TPU v7x, 32 devices: a whole 2x2x4 slice. The times are simulated.
32 devices in a mesh: ep: 8 (over z, y), tp: 4 (over x, core).
Axes of the slice: x: 2, y: 2, z: 4, core: 2. Of those that a mesh axis runs over, the one named last changes fastest.
Arguments:
- q_heads: bfloat16 [8192, 1024], P('ep', 'tp'), may hold values from -200 to 200
- k_heads: bfloat16 [8192, 256], P('ep', 'tp'), may hold values from -6 to 6
- v_heads: bfloat16 [8192, 256], P('ep', 'tp'), may hold values from -6 to 6
- sink_logits: float32 [16], P('tp'), may hold values from 1 to 5
- out_weight: bfloat16 [1024, 2048], P(None, 'tp'), may hold values from -1.5 to 1.5
- tokens_b: bfloat16 [4096, 2048], P('ep'), may hold values from -6 to 6
- moe_gain: float32 [2048], replicated, may hold values from 0.1 to 1.9
- router_group: bfloat16 [2048, 4], replicated, may hold values from -0.125 to 0.125
- router_expert: bfloat16 [2048, 16], replicated, may hold values from -0.125 to 0.125
- route_expert: int32 [4096, 2], P('ep'), may hold values from 0 to 15, as said below
- expert_gate: bfloat16 [16, 2048, 1024], P('ep', None, 'tp'), may hold values from -0.125 to 0.125
- expert_up: bfloat16 [16, 2048, 1024], P('ep', None, 'tp'), may hold values from -0.125 to 0.125
- expert_down: bfloat16 [16, 1024, 2048], P('ep', 'tp'), may hold values from -0.75 to 0.75
Outputs:
- mixer_out: bfloat16 [8192, 2048], P('ep', 'tp')
- moe_out: bfloat16 [4096, 2048], P(('ep', 'tp'))
Inputs may be any that keep to these rules, and one draw needn't show every extreme that they name: `route_expert`: each token names two different experts, in rising order, of one group of 4 consecutive experts. In each aligned block of 128 rows (the rows of one device) no expert is named by more than 32 tokens, in each group one expert is named by exactly 32 tokens of every block, and each group is named by a quarter of every block's tokens.
All inputs are finite; a program needn't handle non-finite values.
Results may differ from a plain program's by a relative error of at most 0.011.
Values may be sent and summed in bfloat16 or wider, within the bound.
No kernel may reach another device: no remote copies, remote signals or barrier semaphores. Data moves between devices by JAX's collectives and lax.ppermute only.
A program may use at most 128 MiB of HBM per device.

v0:
```python
import jax
import jax.numpy as jnp
from jax import lax
from jax.sharding import PartitionSpec as P

HEADS = 16
KV = 4
HD = 64
WINDOW = 128


def shifted(value, axis, steps):
    count = lax.axis_size(axis)
    leading, last = (max(0, -steps), min(count, count - steps))
    return lax.ppermute(value, axis, [(source, source + steps) for source in range(leading, last)])


def normalize(rows_in, gain):
    values = rows_in.astype(jnp.float32)
    scaled = values * lax.rsqrt(jnp.mean(values * values, axis=-1, keepdims=True) + 1e-06) * gain
    return scaled.astype(jnp.bfloat16)


def gate_weights(normed, routes, router_group, router_expert):
    group_logits = jnp.dot(normed, router_group, preferred_element_type=jnp.float32)
    expert_logits = jnp.dot(normed, router_expert, preferred_element_type=jnp.float32)
    group_count = router_group.shape[1]
    expert_count = router_expert.shape[1]
    chosen_group = routes[:, 0] // (expert_count // group_count)
    group_match = chosen_group[:, None] == jnp.arange(group_count, dtype=jnp.int32)[None, :]
    group_share = jnp.sum(
        jnp.where(group_match, jax.nn.softmax(group_logits, axis=-1), 0.0), axis=-1
    )
    expert_match = routes[:, :, None] == jnp.arange(expert_count, dtype=jnp.int32)[None, None, :]
    picked = jnp.sum(jnp.where(expert_match, expert_logits[:, None, :], 0.0), axis=-1)
    return group_share[:, None] * jax.nn.softmax(picked, axis=-1)


def slot_positions(routes, sub_count, expert_count):
    flat_routes = routes.reshape(sub_count, -1)
    onehot = (
        flat_routes[:, :, None] == jnp.arange(expert_count, dtype=jnp.int32)[None, None, :]
    ).astype(jnp.int32)
    places = jnp.sum(onehot * jnp.cumsum(onehot, axis=1), axis=2) - 1
    return (flat_routes, places)


def fill_slots(normed, flat_routes, places, sub_count, expert_count, capacity, exp_local):
    sub_index = jnp.arange(sub_count, dtype=jnp.int32)[:, None]
    target = ((flat_routes * sub_count + sub_index) * capacity + places).reshape(-1)
    source = jnp.repeat(normed, 2, axis=0)
    buffer = jnp.zeros((expert_count * sub_count * capacity, normed.shape[1]), jnp.bfloat16)
    buffer = buffer.at[target].set(source)
    return buffer.reshape(
        expert_count // exp_local, exp_local, sub_count, capacity, normed.shape[1]
    )


def per_device(
    q_heads,
    k_heads,
    v_heads,
    sink_logits,
    out_weight,
    tokens_b,
    moe_gain,
    router_group,
    router_expert,
    route_expert,
    expert_gate,
    expert_up,
    expert_down,
):
    span_len = WINDOW
    row_count = q_heads.shape[0]
    kv_local = k_heads.shape[1] // HD
    group_size = HEADS // KV
    blocks = row_count // span_len
    stacked = jnp.stack([k_heads[row_count - span_len :], v_heads[row_count - span_len :]])
    earlier = shifted(stacked, "ep", 1)

    def make_band(own_rows, prev_rows):
        extended = jnp.concatenate([prev_rows, own_rows], axis=0).reshape(
            blocks + 1, span_len, kv_local, HD
        )
        return jnp.concatenate([extended[:-1], extended[1:]], axis=1)

    key_band = make_band(k_heads, earlier[0])
    value_band = make_band(v_heads, earlier[1])
    query_blocks = q_heads.reshape(blocks, span_len, kv_local, group_size, HD)
    scores = jnp.einsum(
        "nqhgd,nkhd->nhgqk", query_blocks, key_band, preferred_element_type=jnp.float32
    ) * HD ** (-0.5)
    first_row = lax.axis_index("ep") * row_count
    query_index = jnp.arange(span_len, dtype=jnp.int32)[:, None]
    key_index = jnp.arange(2 * span_len, dtype=jnp.int32)[None, :]
    distance = query_index + span_len - key_index
    key_place = (
        first_row
        + jnp.arange(blocks, dtype=jnp.int32)[:, None, None] * span_len
        + key_index[None]
        - span_len
    )
    allowed = (distance >= 0)[None] & (distance < span_len)[None] & (key_place >= 0)
    masked = jnp.where(allowed[:, None, None], scores, -1e30)
    sink_full = sink_logits.reshape(kv_local, group_size)[None, :, :, None]
    row_max = jnp.maximum(jnp.max(masked, axis=-1), sink_full)
    weights_exp = jnp.exp(masked - row_max[..., None])
    denominator = jnp.sum(weights_exp, axis=-1) + jnp.exp(sink_full - row_max)
    probs = (weights_exp / denominator[..., None]).astype(jnp.bfloat16)
    attended = jnp.einsum(
        "nhgqk,nkhd->nqhgd", probs, value_band, preferred_element_type=jnp.float32
    )
    attended = attended.astype(jnp.bfloat16).reshape(row_count, kv_local * group_size * HD)
    mixed = jnp.dot(
        lax.all_gather(attended, "tp", axis=1, tiled=True),
        out_weight,
        preferred_element_type=jnp.float32,
    )
    mixer_out = mixed.astype(jnp.bfloat16)
    tp_count = lax.axis_size("tp")
    tp_index = lax.axis_index("tp")
    exp_local = expert_gate.shape[0]
    expert_count = exp_local * lax.axis_size("ep")
    rows_dev = tokens_b.shape[0] // tp_count
    capacity = min(4 * rows_dev // expert_count, rows_dev // 4)
    own_routes = lax.dynamic_slice_in_dim(route_expert, tp_index * rows_dev, rows_dev, 0)
    own_normed = normalize(
        lax.dynamic_slice_in_dim(tokens_b, tp_index * rows_dev, rows_dev, 0), moe_gain
    )
    flat_routes, places = slot_positions(own_routes, 1, expert_count)
    buffer = fill_slots(own_normed, flat_routes, places, 1, expert_count, capacity, exp_local)
    delivered = lax.all_to_all(buffer, "ep", split_axis=0, concat_axis=0, tiled=True)
    arrived = lax.all_gather(delivered, "tp", axis=2, tiled=True)
    own_flat = flat_routes[0]
    own_places = places[0]
    gates = gate_weights(own_normed, own_routes, router_group, router_expert)
    gate_pre = jnp.einsum(
        "setcd,edf->setcf", arrived, expert_gate, preferred_element_type=jnp.float32
    )
    up_pre = jnp.einsum("setcd,edf->setcf", arrived, expert_up, preferred_element_type=jnp.float32)
    activated = (jax.nn.silu(gate_pre) * up_pre).astype(jnp.bfloat16)
    partial_value = jnp.einsum(
        "setcf,efd->setcd", activated, expert_down, preferred_element_type=jnp.float32
    )
    summed = lax.psum_scatter(
        partial_value.astype(jnp.bfloat16), "tp", scatter_dimension=2, tiled=True
    )
    returned = lax.all_to_all(summed, "ep", split_axis=0, concat_axis=0, tiled=True)
    returned = returned.reshape(expert_count * capacity, returned.shape[-1])
    picked_rows = returned[own_flat * capacity + own_places].reshape(
        rows_dev, 2, returned.shape[-1]
    )
    moe_out = jnp.sum(gates[:, :, None] * picked_rows.astype(jnp.float32), axis=1).astype(
        jnp.bfloat16
    )
    return (mixer_out, moe_out)


def solution(mesh):
    in_specs = (
        P("ep", "tp"),
        P("ep", "tp"),
        P("ep", "tp"),
        P("tp"),
        P(None, "tp"),
        P("ep", None),
        P(),
        P(),
        P(),
        P("ep", None),
        P("ep", None, "tp"),
        P("ep", None, "tp"),
        P("ep", "tp", None),
    )
    out_specs = (P("ep", "tp"), P(("ep", "tp"), None))
    return jax.shard_map(
        per_device, mesh=mesh, in_specs=in_specs, out_specs=out_specs, check_vma=False
    )
```

profile of v0, /device:TPU:0, one launch (start us, length us, event | category | flops | bytes accessed | tf_op | source)
XLA Modules:
  0.0 384.7 jit_solution(17518008943013169215)
XLA Ops:
  9.7 1.2 fusion.24
  10.9 1.3 fusion.26
  12.2 1.6 broadcast_in_dim.34
  13.8 2.3 reshape.383
  16.0 4.4 %scatter_custom_fusion = bf16[512,2048]{1,0:T(8,128)(2,1)} fusion(s32[256]{0:T(256)S(1)} %bitcast.171, bf16[256,2048]{1,0:T(8,128)(2,1)} %reshape.383, bf16[]{:T(256)} %constant.67.clone.1), kind=kCustom, calls=%fused_computation.35 | custom fusion | bytes 2097664 | tf_op jit(solution)/shard_map/scatter | solution.py:53
  20.5 55.5 %all_to_all.10 = bf16[8,2,1,32,2048]{4,3,2,1,0:T(8,128)(2,1)S(1)} all-to-all(bf16[8,2,1,32,2048]{4,3,2,1,0:T(8,128)(2,1)} %bitcast.159), channel_id=1, replica_groups=mesh['ep'=8,'tp'=4] {'ep'}, dimensions={0} | all-to-all | bytes 4194304 | tf_op jit(solution)/shard_map/all_to_all | solution.py:133
  76.0 1.5 copy.69
  77.6 57.4 %all-gather.5.cloned.1.call-done = bf16[8,2,4,32,2048]{4,3,2,0,1:T(8,128)(2,1)} async-done(((bf16[8,2,1,32,2048]{4,3,2,0,1:T(8,128)(2,1)}), bf16[8,2,4,32,2048]{4,3,2,0,1:T(8,128)(2,1)}) %all-gather.5.cloned.1.call-update) | async-done | bytes 8388624 | tf_op jit(solution)/shard_map/all_gather | solution.py:134
  134.9 7.7 %fusion.3 = f32[2,8,4,32,256]{4,3,2,1,0:T(8,128)} fusion(bf16[8,2,4,32,2048]{4,3,2,0,1:T(8,128)(2,1)} %all-gather.5.cloned.1.call-done, bf16[2,2048,256]{2,1,0:T(8,128)(2,1)} %param.24), kind=kOutput, calls=%fused_computation.9 | convolution fusion | flops 2147483648 | bytes 12582912 | tf_op jit(solution)/shard_map/setcd,edf->setcf/dot_general | solution.py:141
  142.6 13.5 %convert_bitcast_fusion = bf16[8,2,4,32,2048]{4,3,2,0,1:T(8,128)(2,1)} fusion(bf16[2,256,2048]{2,1,0:T(8,128)(2,1)S(1)} %copy-done, f32[2,8,4,32,256]{4,3,2,1,0:T(8,128)} %fusion.3, bf16[8,2,4,32,2048]{4,3,2,0,1:T(8,128)(2,1)} %all-gather.5.cloned.1.call-done, bf16[2,2048,256]{2,1,0:T(8,128)(2,1)} %param.23), kind=kOutput, calls=%fused_computation.2 | convolution fusion | flops 4302307328 | bytes 23068672 | tf_op jit(solution)/shard_map/setcf,efd->setcd/dot_general | solution.py:143
  157.1 3.6 collective-permute-start
  162.5 0.9 fusion.1
  163.5 1.1 fusion
  165.4 143.8 %all-reduce.3.cloned.1.call-done = bf16[8,2,4,32,2048]{4,3,2,0,1:T(8,128)(2,1)} async-done(((bf16[8,2,4,32,2048]{4,3,2,0,1:T(8,128)(2,1)}), bf16[8,2,4,32,2048]{4,3,2,0,1:T(8,128)(2,1)}) %all-reduce.3.cloned.1.call-update) | async-done | bytes 8388624
  309.2 2.5 constant_dynamic-slice_fusion
  311.6 1.6 copy.70
  313.2 5.5 %all-to-all-start.1 = ((bf16[8,2,1,32,2048]{4,3,2,1,0:T(8,128)(2,1)}), bf16[8,2,1,32,2048]{4,3,2,1,0:T(8,128)(2,1)S(1)}, u32[]{:S(2)}, u32[]{:S(2)}) async-start(bf16[8,2,1,32,2048]{4,3,2,1,0:T(8,128)(2,1)} %copy.70), calls=%async_computation.1 | async-start | bytes 4194304 | tf_op jit(solution)/shard_map/all_to_all | solution.py:149
  318.8 3.4 fusion.21
  324.3 22.5 %all-gather.3.cloned.1.call-done = bf16[1024,1024]{0,1:T(8,128)(2,1)} async-done(((bf16[1024,256]{0,1:T(8,128)(2,1)}), bf16[1024,1024]{0,1:T(8,128)(2,1)}) %all-gather.3.cloned.1.call-update) | async-done | bytes 2097168 | tf_op jit(solution)/shard_map/all_gather | solution.py:116
  346.8 4.1 %convolution_convert_fusion = bf16[1024,512]{1,0:T(8,128)(2,1)} fusion(bf16[1024,1024]{0,1:T(8,128)(2,1)} %all-gather.3.cloned.1.call-done, bf16[1024,512]{1,0:T(8,128)(2,1)} %param.17), kind=kOutput, calls=%fused_computation.24 | convolution fusion | flops 1074266112 | bytes 4194304 | tf_op jit(solution)/shard_map/dot_general | solution.py:115
  350.9 15.8 %all-to-all-done.1 = bf16[8,2,1,32,2048]{4,3,2,1,0:T(8,128)(2,1)S(1)} async-done(((bf16[8,2,1,32,2048]{4,3,2,1,0:T(8,128)(2,1)}), bf16[8,2,1,32,2048]{4,3,2,1,0:T(8,128)(2,1)S(1)}, u32[]{:S(2)}, u32[]{:S(2)}) %all-to-all-start.1) | async-done | bytes 2097184 | tf_op jit(solution)/shard_map/all_to_all | solution.py:149
  366.7 2.3 gather_fusion
  369.0 3.5 reshape.370
  372.6 5.6 %multiply_reduce_fusion = bf16[128,2048]{1,0:T(8,128)(2,1)} fusion(f32[128,2,2048]{2,1,0:T(2,128)} %reshape.370, f32[128,2]{1,0:T(8,128)S(1)} %copy.62), kind=kLoop, calls=%fused_computation.22 | loop fusion | flops 786432 | bytes 2622464 | tf_op jit(solution)/shard_map/reduce_sum | solution.py:154
  (80 shorter events, 8.1 us)
Async XLA Ops:
  7.2 135.4 %copy-start = (bf16[2,256,2048]{2,1,0:T(8,128)(2,1)S(1)}, bf16[2,256,2048]{2,1,0:T(8,128)(2,1)}, u32[]{:S(2)}) copy-start(bf16[2,256,2048]{2,1,0:T(8,128)(2,1)} %param.25) | copy-start | bytes 6291460
  7.2 127.8 %all-gather.5.cloned.1.call-start = ((), (), s32[]{:S(2)}) async-start(), calls=%async_computation.3 | async-start | bytes 10485760 | tf_op jit(solution)/shard_map/all_gather | solution.py:134
  77.5 231.6 %all-reduce.3.cloned.1.call-start = ((), (), s32[]{:S(2)}) async-start(), calls=%async_computation.4 | async-start | bytes 16777216
  156.1 0.9 copy-start.3
  156.1 1.0 copy-start.4
  156.1 5.1 %copy-start.5 = (bf16[1024,256]{1,0:T(8,128)(2,1)S(1)}, bf16[1024,256]{1,0:T(8,128)(2,1)}, u32[]{:S(2)}) copy-start(bf16[1024,256]{1,0:T(8,128)(2,1)} %param.13) | copy-start | bytes 1572868
  157.1 4.6 %copy-start.9 = (u32[32]{0:T(128)S(1)}, u32[32]{0:T(128)}, u32[]{:S(2)}) copy-start(u32[32]{0:T(128)} %constant.75) | copy-start | bytes 388
  157.1 5.2 %collective-permute-start = (bf16[2,128,64]{1,2,0:T(8,128)(2,1)S(1)}, bf16[2,128,64]{1,2,0:T(8,128)(2,1)S(1)}, u32[]{:S(2)}, u32[]{:S(2)}) collective-permute-start(bf16[2,128,64]{1,2,0:T(8,128)(2,1)S(1)} %pad_maximum_fusion.2), channel_id=1, source_target_pairs={{0,4},{4,8},{8,12},{12,16},{16,20},{20,24},{24,28},{1,5},{5,9},{9,... | collective-permute-start | bytes 98312 | tf_op jit(solution)/shard_map/ppermute | solution.py:15
  162.5 0.9 copy-start.8
  163.4 1.9 copy-start.2
  313.2 53.4 %all-to-all-start.1 = ((bf16[8,2,1,32,2048]{4,3,2,1,0:T(8,128)(2,1)}), bf16[8,2,1,32,2048]{4,3,2,1,0:T(8,128)(2,1)S(1)}, u32[]{:S(2)}, u32[]{:S(2)}) async-start(bf16[8,2,1,32,2048]{4,3,2,1,0:T(8,128)(2,1)} %copy.70), calls=%async_computation.1 | async-start | bytes 4194304 | tf_op jit(solution)/shard_map/all_to_all | solution.py:149
  318.8 28.0 %all-gather.3.cloned.1.call-start = ((), (), s32[]{:S(2)}) async-start(), calls=%async_computation.2 | async-start | bytes 2621440 | tf_op jit(solution)/shard_map/all_gather | solution.py:116
  322.2 1.3 copy-start.6
  322.2 1.6 copy-start.7
  369.0 9.1 %copy-start.1 = (bf16[2,256,2048]{2,1,0:T(8,128)(2,1)S(1)}, bf16[2,256,2048]{2,1,0:T(8,128)(2,1)}, u32[]{:S(2)}) copy-start(bf16[2,256,2048]{2,1,0:T(8,128)(2,1)} %param.25) | copy-start | bytes 6291460
Sparse Core Ops, SparseCore 0:
  77.6 57.2 all-gather.4
  156.3 152.8 all-reduce.2
  323.6 23.1 all-gather.2
where the time goes:
time: 385 us
  waiting for transfers between devices  239 us (62%)
  blocking collectives  55.5 us (14%)
  matrix products  30.1 us (8%)
  local copies, waits for them, and re-layouts  24.9 us (6%)
  between operations  14.1 us (4%)
  other arithmetic  11.5 us (3%)
  starting transfers between devices  9.2 us (2%)
    unnamed x4, waiting for transfers between devices  144 us
    all_gather x1, waiting for transfers between devices, per_device(): arrived = lax.all_gather(delivered, 'tp', axis=2, tiled=True)  57.4 us
    all_to_all x1, blocking collectives, per_device(): lax.all_to_all(buffer, 'ep', split_axis=0, concat_axis=0, tiled=True)  55.5 us
    all_gather x1, waiting for transfers between devices, per_device(): lax.all_gather(attended, 'tp', axis=1, tiled=True)  22.5 us
    all_to_all x1, waiting for transfers between devices, per_device(): lax.all_to_all(summed, 'ep', split_axis=0, concat_axis=0, tiled=True)  15.8 us
    dot_general x1, matrix products, per_device(): jnp.einsum('setcf,efd->setcd', activated, expert_down, preferred_element_...  13.5 us
  transfers between devices with their start and end apart: 5, of which 4 were waited for; matrix products, arithmetic and copies ran while one was open for 3% of the time, Pallas kernels for 0%

commit v1 on v0

v1 whole, which is shorter than its diff:
```python
import functools

import jax
import jax.numpy as jnp
from jax import lax
from jax.experimental import pallas as pl
from jax.experimental.pallas import tpu as pltpu
from jax.sharding import PartitionSpec as P

HEADS = 16
KV = 4
HD = 64
WINDOW = 128
LANES = 128


def shifted(value, axis, steps):
    count = lax.axis_size(axis)
    leading, last = (max(0, -steps), min(count, count - steps))
    return lax.ppermute(value, axis, [(source, source + steps) for source in range(leading, last)])


def flipped(value, axis, bits):
    return lax.ppermute(value, axis, [(i, i ^ bits) for i in range(lax.axis_size(axis))])


def dot_f32(a, b, contract):
    return lax.dot_general(a, b, ((contract[:1], contract[1:]), ((), ())), preferred_element_type=jnp.float32)


def attention_kernel(place_ref, q_ref, kt_ref, vt_ref, halo_ref, sink_ref, out_ref, *, kv_local, group_size):
    span = WINDOW
    rows = q_ref.shape[0]
    query_index = lax.broadcasted_iota(jnp.int32, (span, 2 * span), 0)
    key_index = lax.broadcasted_iota(jnp.int32, (span, 2 * span), 1)
    banded = (key_index > query_index) & (key_index <= query_index + span)
    first_banded = banded & ((key_index >= span) | (place_ref[0] > 0))
    half = kv_local * HD
    for block in range(rows // span):
        here = pl.ds(block * span, span)
        allowed = first_banded if block == 0 else banded
        for kv in range(kv_local):
            heads = pl.ds(kv * HD, HD)
            if block == 0:
                k_band = jnp.concatenate([halo_ref[kv * HD : (kv + 1) * HD, :], kt_ref[heads, here]], axis=1)
                v_band = jnp.concatenate(
                    [halo_ref[half + kv * HD : half + (kv + 1) * HD, :], vt_ref[heads, here]], axis=1
                )
            else:
                k_band = kt_ref[heads, pl.ds((block - 1) * span, 2 * span)]
                v_band = vt_ref[heads, pl.ds((block - 1) * span, 2 * span)]
            mixed = []
            for member in range(group_size):
                head = kv * group_size + member
                scores = dot_f32(q_ref[here, pl.ds(head * HD, HD)], k_band, (1, 0)) * HD ** (-0.5)
                masked = jnp.where(allowed, scores, -1e30)
                sink = sink_ref[head]
                row_max = jnp.maximum(jnp.max(masked, axis=1, keepdims=True), sink)
                weights_exp = jnp.exp(masked - row_max)
                denominator = jnp.sum(weights_exp, axis=1, keepdims=True) + jnp.exp(sink - row_max)
                probs = (weights_exp * (1.0 / denominator)).astype(jnp.bfloat16)
                mixed.append(dot_f32(probs, v_band, (1, 1)))
            out_ref[here, pl.ds(kv * group_size * HD, group_size * HD)] = jnp.concatenate(mixed, axis=1).astype(
                jnp.bfloat16
            )


def attend(place, q_heads, k_t, v_t, halo, sink_logits, kv_local, group_size):
    vmem = pl.BlockSpec(memory_space=pltpu.VMEM)
    smem = pl.BlockSpec(memory_space=pltpu.SMEM)
    return pl.pallas_call(
        functools.partial(attention_kernel, kv_local=kv_local, group_size=group_size),
        out_shape=jax.ShapeDtypeStruct(q_heads.shape, jnp.bfloat16),
        in_specs=[smem, vmem, vmem, vmem, vmem, smem],
        out_specs=vmem,
        cost_estimate=pl.CostEstimate(flops=6_000_000_000, bytes_accessed=2_000_000, transcendentals=0),
        name="attend",
    )(place, q_heads, k_t, v_t, halo, sink_logits)


def projection_kernel(place_ref, *refs):
    *pieces, weight_ref, out_ref = refs
    width = pieces[0].shape[1]
    total = None
    for bits, piece in enumerate(pieces):
        rows = pl.ds(pl.multiple_of((place_ref[1] ^ bits) * width, width), width)
        part = dot_f32(piece[...], weight_ref[rows, :], (1, 0))
        total = part if total is None else total + part
    out_ref[...] = total.astype(jnp.bfloat16)


def project(place, pieces, out_weight):
    rows, width = pieces[0].shape
    tile = rows // 4
    return pl.pallas_call(
        projection_kernel,
        grid_spec=pltpu.PrefetchScalarGridSpec(
            num_scalar_prefetch=1,
            grid=(rows // tile,),
            in_specs=[pl.BlockSpec((tile, width), lambda i, s: (i, 0)) for _ in pieces]
            + [pl.BlockSpec(out_weight.shape, lambda i, s: (0, 0))],
            out_specs=pl.BlockSpec((tile, out_weight.shape[1]), lambda i, s: (i, 0)),
        ),
        out_shape=jax.ShapeDtypeStruct((rows, out_weight.shape[1]), jnp.bfloat16),
        cost_estimate=pl.CostEstimate(flops=2_000_000_000, bytes_accessed=4_000_000, transcendentals=0),
        name="project",
    )(place, *pieces, out_weight)


def dispatch_kernel(place_ref, tokens_ref, gain_ref, group_ref, expert_ref, routes_ref, order_ref, *send_refs):
    groups = group_ref.shape[0]
    experts = expert_ref.shape[0]
    size = experts // groups
    rows, width = tokens_ref.shape
    values = tokens_ref[...].astype(jnp.float32)
    scaled = values * lax.rsqrt(jnp.mean(values * values, axis=-1, keepdims=True) + 1e-06) * gain_ref[...]
    normed = scaled.astype(jnp.bfloat16)
    group_logits = dot_f32(group_ref[...], normed, (1, 1))
    expert_logits = dot_f32(expert_ref[...], normed, (1, 1))
    first = routes_ref[0:1, :]
    second = routes_ref[1:2, :]
    group_index = lax.broadcasted_iota(jnp.int32, (groups, rows), 0)
    in_group = (first >= group_index * size) & (first < (group_index + 1) * size)
    group_exp = jnp.exp(group_logits - jnp.max(group_logits, axis=0, keepdims=True))
    share = jnp.sum(jnp.where(in_group, group_exp, 0.0), axis=0, keepdims=True) / jnp.sum(
        group_exp, axis=0, keepdims=True
    )
    expert_index = lax.broadcasted_iota(jnp.int32, (experts, rows), 0)
    pick_first = jnp.sum(jnp.where(expert_index == first, expert_logits, 0.0), axis=0, keepdims=True)
    pick_second = jnp.sum(jnp.where(expert_index == second, expert_logits, 0.0), axis=0, keepdims=True)
    pick_max = jnp.maximum(pick_first, pick_second)
    exp_first = jnp.exp(pick_first - pick_max)
    exp_second = jnp.exp(pick_second - pick_max)
    pick_sum = exp_first + exp_second
    gate_first = share * (exp_first / pick_sum)
    gate_second = share * (exp_second / pick_sum)
    earlier = lax.broadcasted_iota(jnp.int32, (rows, rows), 0) < lax.broadcasted_iota(jnp.int32, (rows, rows), 1)
    member = jnp.where(in_group, 1.0, 0.0)
    rank = dot_f32(member.astype(jnp.bfloat16), jnp.where(earlier, 1.0, 0.0).astype(jnp.bfloat16), (1, 0))
    chunk = (group_index ^ place_ref[2]) * (rows // groups)
    slot = jnp.sum(member * (chunk.astype(jnp.float32) + rank), axis=0, keepdims=True).astype(jnp.int32)
    order = jnp.where(lax.broadcasted_iota(jnp.int32, (rows, rows), 0) == slot, 1.0, 0.0).astype(jnp.bfloat16)
    order_ref[...] = order
    base = jnp.sum(jnp.where(in_group, group_index * size, 0), axis=0, keepdims=True)
    line = lax.broadcasted_iota(jnp.int32, (LANES, rows), 0)
    local = jnp.where(line < size, line, line - size) + base
    gate = jnp.where(local == first, gate_first, 0.0) + jnp.where(local == second, gate_second, 0.0)
    high = gate.astype(jnp.bfloat16).astype(jnp.float32)
    columns = jnp.where(line < size, high, jnp.where(line < 2 * size, gate - high, 0.0)).astype(jnp.bfloat16)
    moved = dot_f32(order, normed, (1, 0)).astype(jnp.bfloat16)
    moved_gates = dot_f32(order, columns, (1, 1)).astype(jnp.bfloat16)
    step = rows // groups
    for k, send in enumerate(send_refs):
        send[:, :width] = moved[k * step : (k + 1) * step]
        send[:, width:] = moved_gates[k * step : (k + 1) * step]


def dispatch(place, tokens, gain, group_t, expert_t, routes_t, rows):
    width = tokens.shape[1]
    groups = group_t.shape[0]
    step = rows // groups
    whole = lambda shape: pl.BlockSpec(shape, lambda i, s: tuple(0 for _ in shape))
    return pl.pallas_call(
        dispatch_kernel,
        grid_spec=pltpu.PrefetchScalarGridSpec(
            num_scalar_prefetch=1,
            grid=(1,),
            in_specs=[
                pl.BlockSpec((rows, width), lambda i, s: (s[1], 0)),
                whole((1, width)),
                whole(group_t.shape),
                whole(expert_t.shape),
                pl.BlockSpec((2, rows), lambda i, s: (0, s[1])),
            ],
            out_specs=[whole((rows, rows))] + [whole((step, width + LANES)) for _ in range(groups)],
        ),
        out_shape=[jax.ShapeDtypeStruct((rows, rows), jnp.bfloat16)]
        + [jax.ShapeDtypeStruct((step, width + LANES), jnp.bfloat16) for _ in range(groups)],
        cost_estimate=pl.CostEstimate(flops=1_000_000_000, bytes_accessed=2_000_000, transcendentals=0),
        name="dispatch",
    )(place, tokens, gain.reshape(1, width), group_t, expert_t, routes_t)


def experts_kernel(place_ref, *refs, sizes, size, tile):
    count = len(sizes)
    pieces = refs[:count]
    gate_ref, up_ref, down_ref, here_ref, there_ref, rows_ref = refs[count:]
    exp_local, width, hidden = gate_ref.shape
    at = 0
    for piece, rows in zip(pieces, sizes):
        rows_ref[at : at + rows, :] = piece[...]
        at += rows
    half = at // 2
    line = lax.broadcasted_iota(jnp.int32, (tile, LANES), 1)
    for start in range(0, at, tile):
        held = rows_ref[start : start + tile, :width]
        gates = rows_ref[start : start + tile, width:].astype(jnp.float32)
        active = []
        for e in range(exp_local):
            own = place_ref[3] * exp_local + e
            gate = jnp.sum(
                jnp.where((line == own) | (line == own + size), gates, 0.0), axis=1, keepdims=True
            )
            gate_pre = dot_f32(held, gate_ref[e], (1, 0))
            up_pre = dot_f32(held, up_ref[e], (1, 0))
            active.append((jax.nn.silu(gate_pre) * up_pre * gate).astype(jnp.bfloat16))
        result = None
        for e in range(exp_local):
            part = dot_f32(active[e], down_ref[e], (1, 0))
            result = part if result is None else result + part
        result = result.astype(jnp.bfloat16)
        if start < half:
            here_ref[start : start + tile, :] = result
        else:
            there_ref[start - half : start - half + tile, :] = result


def run_experts(place, pieces, expert_gate, expert_up, expert_down, size):
    sizes = tuple(piece.shape[0] for piece in pieces)
    rows = sum(sizes)
    width = expert_gate.shape[1]
    vmem = pl.BlockSpec(memory_space=pltpu.VMEM)
    smem = pl.BlockSpec(memory_space=pltpu.SMEM)
    return pl.pallas_call(
        functools.partial(experts_kernel, sizes=sizes, size=size, tile=min(rows // 2, 256)),
        out_shape=[jax.ShapeDtypeStruct((rows // 2, width), jnp.bfloat16) for _ in range(2)],
        in_specs=[smem] + [vmem] * (len(pieces) + 3),
        out_specs=[vmem, vmem],
        scratch_shapes=[pltpu.VMEM((rows, width + LANES), jnp.bfloat16)],
        cost_estimate=pl.CostEstimate(flops=rows * 7_000_000, bytes_accessed=15_000_000, transcendentals=0),
        name="experts",
    )(place, *pieces, expert_gate, expert_up, expert_down)


def combine_kernel(order_ref, *refs):
    *pieces, out_ref = refs
    rows = jnp.concatenate([piece[...] for piece in pieces], axis=0)
    out_ref[...] = dot_f32(order_ref[...], rows, (0, 0)).astype(jnp.bfloat16)


def combine(order, pieces):
    vmem = pl.BlockSpec(memory_space=pltpu.VMEM)
    return pl.pallas_call(
        combine_kernel,
        out_shape=jax.ShapeDtypeStruct((order.shape[0], pieces[0].shape[1]), jnp.bfloat16),
        in_specs=[vmem] * (len(pieces) + 1),
        out_specs=vmem,
        name="combine",
    )(order, *pieces)


def added(*values):
    return functools.reduce(jnp.add, [v.astype(jnp.float32) for v in values]).astype(jnp.bfloat16)


def gather_plane(own, core_bit, side_bit):
    half = own.shape[0] // 2
    across = flipped(own, "tp", side_bit)
    along = flipped(own, "ep", 1)
    far_low = flipped(across[:half], "ep", 1)
    far_high = flipped(along[half:], "tp", side_bit)
    ours = [own, across, along, far_low, far_high]
    return ours + [flipped(piece, "tp", core_bit) for piece in ours]


def reduce_plane(here, there, core_bit, side_bit):
    step = here.shape[0] // 4
    half = step // 2
    other = flipped(there, "tp", core_bit)
    part = lambda low, high: added(here[low:high], other[low:high])
    far_low = flipped(part(3 * step, 3 * step + half), "ep", 1)
    far_high = flipped(part(3 * step + half, 4 * step), "tp", side_bit)
    across_high = flipped(part(step + half, 2 * step), "tp", side_bit)
    along_low = flipped(part(2 * step, 2 * step + half), "ep", 1)
    across_low = flipped(added(here[step : step + half], other[step : step + half], far_low), "tp", side_bit)
    along_high = flipped(
        added(here[2 * step + half : 3 * step], other[2 * step + half : 3 * step], far_high), "ep", 1
    )
    low = added(here[:half], other[:half], across_low, along_low)
    high = added(here[half:step], other[half:step], across_high, along_high)
    return low, high


def per_device(
    q_heads,
    k_heads,
    v_heads,
    sink_logits,
    out_weight,
    tokens_b,
    moe_gain,
    router_group,
    router_expert,
    route_expert,
    expert_gate,
    expert_up,
    expert_down,
):
    tp_count = lax.axis_size("tp")
    ep_count = lax.axis_size("ep")
    groups = router_group.shape[1]
    experts = router_expert.shape[1]
    exp_local = expert_gate.shape[0]
    members = ep_count // groups
    size = experts // groups
    rows_dev = tokens_b.shape[0] // tp_count
    capacity = min(4 * rows_dev // experts, rows_dev // 4)
    by_group = (
        tp_count == 4
        and members == 2
        and groups & (groups - 1) == 0
        and members * exp_local == size
        and rows_dev // groups <= exp_local * capacity
    )
    ep_index = lax.axis_index("ep")
    tp_index = lax.axis_index("tp")
    place = jnp.stack([ep_index, tp_index, ep_index // members, ep_index % members]).astype(jnp.int32)

    kv_local = k_heads.shape[1] // HD
    k_t = k_heads.T
    v_t = v_heads.T
    last = k_heads.shape[0] - WINDOW
    halo = shifted(jnp.concatenate([k_t[:, last:], v_t[:, last:]], axis=0), "ep", 1)

    if not by_group:
        attended = attend(place, q_heads, k_t, v_t, halo, sink_logits, kv_local, HEADS // KV)
        mixed = jnp.dot(
            lax.all_gather(attended, "tp", axis=1, tiled=True), out_weight, preferred_element_type=jnp.float32
        )
        return (
            mixed.astype(jnp.bfloat16),
            moe_by_slot(
                tokens_b, moe_gain, router_group, router_expert, route_expert, expert_gate, expert_up, expert_down
            ),
        )

    core_bit, side_bit = 1, 2
    order, *sends = dispatch(
        place, tokens_b, moe_gain, router_group.T, router_expert.T, route_expert.T, rows_dev
    )
    arrived = [sends[0]] + [flipped(sends[k], "ep", k * members) for k in range(1, groups)]
    attended = attend(place, q_heads, k_t, v_t, halo, sink_logits, kv_local, HEADS // KV)
    pieces = gather_plane(jnp.concatenate(arrived, axis=0), core_bit, side_bit)
    attended_core = flipped(attended, "tp", core_bit)
    attended_side = flipped(attended, "tp", side_bit)
    attended_both = flipped(attended_side, "tp", core_bit)
    here, there = run_experts(place, pieces, expert_gate, expert_up, expert_down, size)
    low, high = reduce_plane(here, there, core_bit, side_bit)
    mixer_out = project(place, [attended, attended_core, attended_side, attended_both], out_weight)
    step = rows_dev // groups
    totals = jnp.split(low, low.shape[0] // step) + jnp.split(high, high.shape[0] // step)
    returned = [totals[0]] + [flipped(totals[k], "ep", k * members) for k in range(1, groups)]
    return (mixer_out, combine(order, returned))


def normalize(rows_in, gain):
    values = rows_in.astype(jnp.float32)
    scaled = values * lax.rsqrt(jnp.mean(values * values, axis=-1, keepdims=True) + 1e-06) * gain
    return scaled.astype(jnp.bfloat16)


def gate_weights(normed, routes, router_group, router_expert):
    group_logits = jnp.dot(normed, router_group, preferred_element_type=jnp.float32)
    expert_logits = jnp.dot(normed, router_expert, preferred_element_type=jnp.float32)
    group_count = router_group.shape[1]
    expert_count = router_expert.shape[1]
    chosen_group = routes[:, 0] // (expert_count // group_count)
    group_match = chosen_group[:, None] == jnp.arange(group_count, dtype=jnp.int32)[None, :]
    group_share = jnp.sum(jnp.where(group_match, jax.nn.softmax(group_logits, axis=-1), 0.0), axis=-1)
    expert_match = routes[:, :, None] == jnp.arange(expert_count, dtype=jnp.int32)[None, None, :]
    picked = jnp.sum(jnp.where(expert_match, expert_logits[:, None, :], 0.0), axis=-1)
    return group_share[:, None] * jax.nn.softmax(picked, axis=-1)


def moe_by_slot(
    tokens_b, moe_gain, router_group, router_expert, route_expert, expert_gate, expert_up, expert_down
):
    tp_count = lax.axis_size("tp")
    tp_index = lax.axis_index("tp")
    exp_local = expert_gate.shape[0]
    expert_count = exp_local * lax.axis_size("ep")
    rows_dev = tokens_b.shape[0] // tp_count
    width = tokens_b.shape[1]
    capacity = min(4 * rows_dev // expert_count, rows_dev // 4)
    routes = lax.dynamic_slice_in_dim(route_expert, tp_index * rows_dev, rows_dev, 0)
    normed = normalize(lax.dynamic_slice_in_dim(tokens_b, tp_index * rows_dev, rows_dev, 0), moe_gain)
    flat_routes = routes.reshape(-1)
    onehot = (flat_routes[:, None] == jnp.arange(expert_count, dtype=jnp.int32)[None, :]).astype(jnp.int32)
    places = jnp.sum(onehot * jnp.cumsum(onehot, axis=0), axis=1) - 1
    target = flat_routes * capacity + places
    buffer = jnp.zeros((expert_count * capacity, width), jnp.bfloat16)
    buffer = buffer.at[target].set(jnp.repeat(normed, 2, axis=0))
    buffer = buffer.reshape(expert_count // exp_local, exp_local, 1, capacity, width)
    delivered = lax.all_to_all(buffer, "ep", split_axis=0, concat_axis=0, tiled=True)
    arrived = lax.all_gather(delivered, "tp", axis=2, tiled=True)
    gates = gate_weights(normed, routes, router_group, router_expert)
    gate_pre = jnp.einsum("setcd,edf->setcf", arrived, expert_gate, preferred_element_type=jnp.float32)
    up_pre = jnp.einsum("setcd,edf->setcf", arrived, expert_up, preferred_element_type=jnp.float32)
    activated = (jax.nn.silu(gate_pre) * up_pre).astype(jnp.bfloat16)
    partial_value = jnp.einsum("setcf,efd->setcd", activated, expert_down, preferred_element_type=jnp.float32)
    summed = lax.psum_scatter(partial_value.astype(jnp.bfloat16), "tp", scatter_dimension=2, tiled=True)
    returned = lax.all_to_all(summed, "ep", split_axis=0, concat_axis=0, tiled=True)
    picked_rows = returned.reshape(expert_count * capacity, width)[target].reshape(rows_dev, 2, width)
    return jnp.sum(gates[:, :, None] * picked_rows.astype(jnp.float32), axis=1).astype(jnp.bfloat16)


def solution(mesh):
    in_specs = (
        P("ep", "tp"),
        P("ep", "tp"),
        P("ep", "tp"),
        P("tp"),
        P(None, "tp"),
        P("ep", None),
        P(),
        P(),
        P(),
        P("ep", None),
        P("ep", None, "tp"),
        P("ep", None, "tp"),
        P("ep", "tp", None),
    )
    out_specs = (P("ep", "tp"), P(("ep", "tp"), None))
    return jax.shard_map(per_device, mesh=mesh, in_specs=in_specs, out_specs=out_specs, check_vma=False)
```

time: 385 us -> 121 us (0.31)
  waiting for transfers between devices: 239 us -> 46.5 us
  blocking collectives: 55.5 us -> 0 us
  Pallas kernels: 0 us -> 30.2 us
  matrix products: 30.1 us -> 0 us
  starting transfers between devices: 9.2 us -> 28.4 us
  local copies, waits for them, and re-layouts: 24.9 us -> 7.61 us
  between operations: 14.1 us -> 0.87 us
  other arithmetic: 11.5 us -> 6.75 us
    unnamed x4 -> x0, waiting for transfers between devices: 144 us -> none
    all_gather x2 -> x0, waiting for transfers between devices: 79.9 us -> none  [the longest x1 57.4 us: per_device(): arrived = lax.all_gather(delivered, 'tp', axis=2, tiled=True)]
    all_to_all x1 -> x0, blocking collectives: 55.5 us -> none  [per_device(): lax.all_to_all(buffer, 'ep', split_axis=0, concat_axis=0, tiled=True)]
    ppermute x0 -> x25, waiting for transfers between devices: none -> 46.5 us  [flipped(): lax.ppermute(value, axis, [(i, i ^ bits) for i in range(lax.axis_size(axi...]
    pallas_call x0 -> x5, Pallas kernels: none -> 30.2 us  [the longest x1 12.6 us: run_experts(): pl.pallas_call(functools.partial(experts_kernel, sizes=sizes, size=size,...]
    dot_general x7 -> x0, matrix products: 30.1 us -> none  [the longest x1 13.5 us: per_device(): jnp.einsum('setcf,efd->setcd', activated, expert_down, preferred_element_...]
    ppermute x0 -> x25, starting transfers between devices: none -> 25.2 us  [flipped(): lax.ppermute(value, axis, [(i, i ^ bits) for i in range(lax.axis_size(axi...]
    all_to_all x1 -> x0, waiting for transfers between devices: 15.8 us -> none  [per_device(): lax.all_to_all(summed, 'ep', split_axis=0, concat_axis=0, tiled=True)]
  transfers between devices with their start and end apart: 5 -> 26, of which waited for: 4 -> 11; matrix products, arithmetic and copies ran while one was open for 3% -> 6% of each run, Pallas kernels for 0% -> 10%
where the time goes in v1:
time: 121 us; the launch traced here: 120 us
  waiting for transfers between devices  46.5 us (38%)
  Pallas kernels  30.2 us (25%)
  starting transfers between devices  28.4 us (23%)
  local copies, waits for them, and re-layouts  7.61 us (6%)
  other arithmetic  6.75 us (6%)
    ppermute x25, waiting for transfers between devices, flipped(): lax.ppermute(value, axis, [(i, i ^ bits) for i in range(lax.axis_size(axi...  46.5 us
    ppermute x25, starting transfers between devices, flipped(): lax.ppermute(value, axis, [(i, i ^ bits) for i in range(lax.axis_size(axi...  25.2 us
    pallas_call x1, Pallas kernels, run_experts(): pl.pallas_call(functools.partial(experts_kernel, sizes=sizes, size=size,...  12.6 us
    pallas_call x1, Pallas kernels, attend(): pl.pallas_call(functools.partial(attention_kernel, kv_local=kv_local, gro...  6.35 us
    convert_element_type x5, other arithmetic, added(): functools.reduce(jnp.add, [v.astype(jnp.float32) for v in values])  6.15 us
    pallas_call x1, Pallas kernels, project(): pl.pallas_call(projection_kernel, grid_spec=pltpu.PrefetchScalarGridSpec(...  5.62 us
    unnamed x41, local copies, waits for them, and re-layouts  5.42 us
    pallas_call x1, Pallas kernels, dispatch(): pl.pallas_call(dispatch_kernel, grid_spec=pltpu.PrefetchScalarGridSpec(nu...  3.43 us
  transfers between devices with their start and end apart: 26, of which 11 were waited for; matrix products, arithmetic and copies ran while one was open for 6% of the time, Pallas kernels for 10%

profile of v1, /device:TPU:0, one launch (start us, length us, event | category | flops | bytes accessed | tf_op | source)
XLA Modules:
  0.0 120.3 jit_solution(11069307734545104729)
XLA Ops:
  1.2 3.4 %dispatch.1 = (bf16[128,128]{1,0:T(8,128)(2,1)}, bf16[32,2176]{1,0:T(8,128)(2,1)}, bf16[32,2176]{1,0:T(8,128)(2,1)}, bf16[32,2176]{1,0:T(8,128)(2,1)}, bf16[32,2176]{1,0:T(8,128)(2,1)}) custom-call(s32[4]{0:T(128)} %pad_add_fusion.place_ref, bf16[512,2048]{1,0:T(8,128)(2,1)} %tokens_ref.1, f32[1,2048]{1,0:T(1,128)} %bitcast.16, bf16[4,2048]{1,0:T(4,128)(2,1)} %bitcast.15, ...), custom_call_target="tpu_custom_call" | custom-call | flops 1000000000 | bytes 2000000 | tf_op jit(solution)/shard_map/dispatch/pallas_call | solution.py:163
  4.7 3.1 %collective-permute-start.4 = (bf16[32,2176]{1,0:T(8,128)(2,1)}, bf16[32,2176]{1,0:T(8,128)(2,1)S(1)}, u32[]{:S(2)}, u32[]{:S(2)}) collective-permute-start(bf16[32,2176]{1,0:T(8,128)(2,1)} %get-tuple-element.11), channel_id=1, source_target_pairs={{0,8},{4,12},{8,0},{12,4},{16,24},{20,28},{24,16},{28,20},{1,9},{5... | collective-permute-start | bytes 417800 | tf_op jit(solution)/shard_map/ppermute | solution.py:24
  7.7 2.6 %collective-permute-start.5 = (bf16[32,2176]{1,0:T(8,128)(2,1)}, bf16[32,2176]{1,0:T(8,128)(2,1)S(1)}, u32[]{:S(2)}, u32[]{:S(2)}) collective-permute-start(bf16[32,2176]{1,0:T(8,128)(2,1)} %get-tuple-element.12), channel_id=1, source_target_pairs={{0,16},{4,20},{8,24},{12,28},{16,0},{20,4},{24,8},{28,12},{1,17},{... | collective-permute-start | bytes 417800 | tf_op jit(solution)/shard_map/ppermute | solution.py:24
  11.2 2.2 %collective-permute-done.4 = bf16[32,2176]{1,0:T(8,128)(2,1)S(1)} collective-permute-done((bf16[32,2176]{1,0:T(8,128)(2,1)}, bf16[32,2176]{1,0:T(8,128)(2,1)S(1)}, u32[]{:S(2)}, u32[]{:S(2)}) %collective-permute-start.4) | collective-permute-done | bytes 139296 | tf_op jit(solution)/shard_map/ppermute | solution.py:24
  13.4 7.9 %collective-permute-done.5 = bf16[32,2176]{1,0:T(8,128)(2,1)S(1)} collective-permute-done((bf16[32,2176]{1,0:T(8,128)(2,1)}, bf16[32,2176]{1,0:T(8,128)(2,1)S(1)}, u32[]{:S(2)}, u32[]{:S(2)}) %collective-permute-start.5) | collective-permute-done | bytes 139296 | tf_op jit(solution)/shard_map/ppermute | solution.py:24
  21.4 1.6 %collective-permute-start.7 = (bf16[128,2176]{1,0:T(8,128)(2,1)S(1)}, bf16[128,2176]{1,0:T(8,128)(2,1)S(1)}, u32[]{:S(2)}, u32[]{:S(2)}) collective-permute-start(bf16[128,2176]{1,0:T(8,128)(2,1)S(1)} %constant_dynamic-update-slice_fusion.refs_0_), channel_id=1, source_target_pairs={{0,2},{1,3},{2,0},{3,1},{4,6},{5,7},{6,4},{7,5},{8,10},{9,11},{10,... | collective-permute-start | bytes 1671176 | tf_op jit(solution)/shard_map/ppermute | solution.py:24
  24.5 8.9 %collective-permute-done.7.refs_1_ = bf16[128,2176]{1,0:T(8,128)(2,1)S(1)} collective-permute-done((bf16[128,2176]{1,0:T(8,128)(2,1)S(1)}, bf16[128,2176]{1,0:T(8,128)(2,1)S(1)}, u32[]{:S(2)}, u32[]{:S(2)}) %collective-permute-start.7) | collective-permute-done | bytes 557088 | tf_op jit(solution)/shard_map/ppermute | solution.py:24
  33.4 1.6 %collective-permute-start.9 = (bf16[64,2176]{1,0:T(8,128)(2,1)S(1)}, bf16[64,2176]{1,0:T(8,128)(2,1)S(1)}, u32[]{:S(2)}, u32[]{:S(2)}) collective-permute-start(bf16[64,2176]{1,0:T(8,128)(2,1)S(1)} %slice.82), channel_id=1, source_target_pairs={{0,4},{4,0},{8,12},{12,8},{16,20},{20,16},{24,28},{28,24},{1,5},{5... | collective-permute-start | bytes 835592 | tf_op jit(solution)/shard_map/ppermute | solution.py:24
  35.0 1.6 %collective-permute-done.8.refs_2_ = bf16[128,2176]{1,0:T(8,128)(2,1)S(1)} collective-permute-done((bf16[128,2176]{1,0:T(8,128)(2,1)S(1)}, bf16[128,2176]{1,0:T(8,128)(2,1)S(1)}, u32[]{:S(2)}, u32[]{:S(2)}) %collective-permute-start.8) | collective-permute-done | bytes 557088 | tf_op jit(solution)/shard_map/ppermute | solution.py:24
  37.6 3.0 %collective-permute-done.9.refs_3_ = bf16[64,2176]{1,0:T(8,128)(2,1)S(1)} collective-permute-done((bf16[64,2176]{1,0:T(8,128)(2,1)S(1)}, bf16[64,2176]{1,0:T(8,128)(2,1)S(1)}, u32[]{:S(2)}, u32[]{:S(2)}) %collective-permute-start.9) | collective-permute-done | bytes 278560 | tf_op jit(solution)/shard_map/ppermute | solution.py:24
  40.6 2.6 %collective-permute-done.10.refs_4_ = bf16[64,2176]{1,0:T(8,128)(2,1)S(1)} collective-permute-done((bf16[64,2176]{1,0:T(8,128)(2,1)S(1)}, bf16[64,2176]{1,0:T(8,128)(2,1)S(1)}, u32[]{:S(2)}, u32[]{:S(2)}) %collective-permute-start.10) | collective-permute-done | bytes 278560 | tf_op jit(solution)/shard_map/ppermute | solution.py:24
  43.3 1.5 %collective-permute-done.15.refs_9_ = bf16[64,2176]{1,0:T(8,128)(2,1)S(1)} collective-permute-done((bf16[64,2176]{1,0:T(8,128)(2,1)S(1)}, bf16[64,2176]{1,0:T(8,128)(2,1)S(1)}, u32[]{:S(2)}, u32[]{:S(2)}) %collective-permute-start.15) | collective-permute-done | bytes 278560 | tf_op jit(solution)/shard_map/ppermute | solution.py:24
  47.1 12.6 %experts.1 = (bf16[512,2048]{1,0:T(8,128)(2,1)}, bf16[512,2048]{1,0:T(8,128)(2,1)}) custom-call(s32[4]{0:T(128)} %pad_add_fusion.place_ref, bf16[128,2176]{1,0:T(8,128)(2,1)} %copy-done.7, bf16[128,2176]{1,0:T(8,128)(2,1)} %copy-done.2, bf16[128,2176]{1,0:T(8,128)(2,1)} %copy-done.3, bf16[64,2176]{1,0:T(8,128)(2,1)} %copy-done.14, ...), custom_call_target="tpu_custom_call" | custom-call | flops 7168000000 | bytes 15000000 | tf_op jit(solution)/shard_map/experts/pallas_call | solution.py:224
  59.8 4.2 %collective-permute-done.16 = bf16[512,2048]{1,0:T(8,128)(2,1)S(1)} collective-permute-done((bf16[512,2048]{1,0:T(8,128)(2,1)}, bf16[512,2048]{1,0:T(8,128)(2,1)S(1)}, u32[]{:S(2)}, u32[]{:S(2)}) %collective-permute-start.16) | collective-permute-done | bytes 2097184 | tf_op jit(solution)/shard_map/ppermute | solution.py:24
  67.5 3.2 %collective-permute-start = (bf16[128,128]{1,0:T(8,128)(2,1)S(1)}, bf16[128,128]{1,0:T(8,128)(2,1)S(1)}, u32[]{:S(2)}, u32[]{:S(2)}) collective-permute-start(bf16[128,128]{1,0:T(8,128)(2,1)S(1)} %pad_maximum_fusion), channel_id=1, source_target_pairs={{0,4},{4,8},{8,12},{12,16},{16,20},{20,24},{24,28},{1,5},{5,9},{9,... | collective-permute-start | bytes 98312 | tf_op jit(solution)/shard_map/ppermute | solution.py:20
  70.8 2.1 %collective-permute-start.21 = (bf16[64,2048]{1,0:T(8,128)(2,1)S(1)}, bf16[64,2048]{1,0:T(8,128)(2,1)S(1)}, u32[]{:S(2)}, u32[]{:S(2)}) collective-permute-start(bf16[64,2048]{1,0:T(8,128)(2,1)S(1)} %get-tuple-element.19), channel_id=1, source_target_pairs={{0,2},{1,3},{2,0},{3,1},{4,6},{5,7},{6,4},{7,5},{8,10},{9,11},{10,... | collective-permute-start | bytes 786440 | tf_op jit(solution)/shard_map/ppermute | solution.py:24
  72.8 1.9 %collective-permute-done.22 = bf16[64,2048]{1,0:T(8,128)(2,1)S(1)} collective-permute-done((bf16[64,2048]{1,0:T(8,128)(2,1)S(1)}, bf16[64,2048]{1,0:T(8,128)(2,1)S(1)}, u32[]{:S(2)}, u32[]{:S(2)}) %collective-permute-start.22) | collective-permute-done | bytes 262176 | tf_op jit(solution)/shard_map/ppermute | solution.py:24
  77.3 6.3 %attend.1.refs_0_ = bf16[1024,256]{1,0:T(8,128)(2,1)} custom-call(s32[4]{0:T(128)} %pad_add_fusion.place_ref, bf16[1024,256]{1,0:T(8,128)(2,1)} %q_ref.1, bf16[64,1024]{1,0:T(8,128)(2,1)} %bitcast.11, bf16[64,1024]{1,0:T(8,128)(2,1)} %bitcast.13, bf16[128,128]{1,0:T(8,128)(2,1)} %copy-done.18, f32[4]{0:T(128)} %sink_ref.1), custom_call_target="tpu_custom_call" | custom-call | flops 6000000000 | bytes 2000000 | tf_op jit(solution)/shard_map/attend/pallas_call | solution.py:71
  86.4 10.3 %collective-permute-done.2.refs_2_ = bf16[1024,256]{1,0:T(8,128)(2,1)S(1)} collective-permute-done((bf16[1024,256]{1,0:T(8,128)(2,1)}, bf16[1024,256]{1,0:T(8,128)(2,1)S(1)}, u32[]{:S(2)}, u32[]{:S(2)}) %collective-permute-start.2) | collective-permute-done | bytes 524320 | tf_op jit(solution)/shard_map/ppermute | solution.py:24
  98.8 4.3 %collective-permute-start.24 = (bf16[32,2048]{1,0:T(8,128)(2,1)S(1)}, bf16[32,2048]{1,0:T(8,128)(2,1)S(1)}, u32[]{:S(2)}, u32[]{:S(2)}) collective-permute-start(bf16[32,2048]{1,0:T(8,128)(2,1)S(1)} %get-tuple-element.22), channel_id=1, source_target_pairs={{0,16},{4,20},{8,24},{12,28},{16,0},{20,4},{24,8},{28,12},{1,17},{... | collective-permute-start | bytes 393224 | tf_op jit(solution)/shard_map/ppermute | solution.py:24
  103.0 2.4 %collective-permute-done.19 = bf16[64,2048]{1,0:T(8,128)(2,1)S(1)} collective-permute-done((bf16[64,2048]{1,0:T(8,128)(2,1)S(1)}, bf16[64,2048]{1,0:T(8,128)(2,1)S(1)}, u32[]{:S(2)}, u32[]{:S(2)}) %collective-permute-start.19) | collective-permute-done | bytes 262176 | tf_op jit(solution)/shard_map/ppermute | solution.py:24
  105.4 2.3 %collective-permute-start.25 = (bf16[32,2048]{1,0:T(8,128)(2,1)S(1)}, bf16[32,2048]{1,0:T(8,128)(2,1)S(1)}, u32[]{:S(2)}, u32[]{:S(2)}) collective-permute-start(bf16[32,2048]{1,0:T(8,128)(2,1)S(1)} %get-tuple-element.21), channel_id=1, source_target_pairs={{0,24},{4,28},{8,16},{12,20},{16,8},{20,12},{24,0},{28,4},{1,25},{... | collective-permute-start | bytes 393224 | tf_op jit(solution)/shard_map/ppermute | solution.py:24
  111.7 5.6 %project.1 = bf16[1024,512]{1,0:T(8,128)(2,1)} custom-call(s32[4]{0:T(128)} %pad_add_fusion.place_ref, bf16[1024,256]{1,0:T(8,128)(2,1)} %attend.1.refs_0_, bf16[1024,256]{1,0:T(8,128)(2,1)} %copy-done.13, bf16[1024,256]{1,0:T(8,128)(2,1)} %copy-done.12, bf16[1024,256]{1,0:T(8,128)(2,1)} %collective-permute-done.3.refs_3_, bf16[1024,512]{1,0:T(8,128)(2,1)} %refs_4_.1), custom_call_target="tpu_custom_call" | custom-call | flops 2000000000 | bytes 4000000 | tf_op jit(solution)/shard_map/project/pallas_call | solution.py:95
  118.1 2.2 %combine.1 = bf16[128,2048]{1,0:T(8,128)(2,1)} custom-call(bf16[128,128]{1,0:T(8,128)(2,1)} %get-tuple-element.9.order_ref, bf16[32,2048]{1,0:T(8,128)(2,1)} %get-tuple-element.24.refs_0_, bf16[32,2048]{1,0:T(8,128)(2,1)} %copy-done.6, bf16[32,2048]{1,0:T(8,128)(2,1)} %copy-done.4, bf16[32,2048]{1,0:T(8,128)(2,1)} %copy-done.5), custom_call_target="tpu_custom_call" | custom-call | tf_op jit(solution)/shard_map/combine/pallas_call | solution.py:243
  (88 shorter events, 22.2 us)
Async XLA Ops:
  4.7 8.7 %collective-permute-start.4 = (bf16[32,2176]{1,0:T(8,128)(2,1)}, bf16[32,2176]{1,0:T(8,128)(2,1)S(1)}, u32[]{:S(2)}, u32[]{:S(2)}) collective-permute-start(bf16[32,2176]{1,0:T(8,128)(2,1)} %get-tuple-element.11), channel_id=1, source_target_pairs={{0,8},{4,12},{8,0},{12,4},{16,24},{20,28},{24,16},{28,20},{1,9},{5... | collective-permute-start | bytes 417800 | tf_op jit(solution)/shard_map/ppermute | solution.py:24
  7.7 13.6 %collective-permute-start.5 = (bf16[32,2176]{1,0:T(8,128)(2,1)}, bf16[32,2176]{1,0:T(8,128)(2,1)S(1)}, u32[]{:S(2)}, u32[]{:S(2)}) collective-permute-start(bf16[32,2176]{1,0:T(8,128)(2,1)} %get-tuple-element.12), channel_id=1, source_target_pairs={{0,16},{4,20},{8,24},{12,28},{16,0},{20,4},{24,8},{28,12},{1,17},{... | collective-permute-start | bytes 417800 | tf_op jit(solution)/shard_map/ppermute | solution.py:24
  10.3 11.1 %collective-permute-start.6 = (bf16[32,2176]{1,0:T(8,128)(2,1)}, bf16[32,2176]{1,0:T(8,128)(2,1)S(1)}, u32[]{:S(2)}, u32[]{:S(2)}) collective-permute-start(bf16[32,2176]{1,0:T(8,128)(2,1)} %get-tuple-element.13), channel_id=1, source_target_pairs={{0,24},{4,28},{8,16},{12,20},{16,8},{20,12},{24,0},{28,4},{1,25},{... | collective-permute-start | bytes 417800 | tf_op jit(solution)/shard_map/ppermute | solution.py:24
  21.4 12.0 %collective-permute-start.7 = (bf16[128,2176]{1,0:T(8,128)(2,1)S(1)}, bf16[128,2176]{1,0:T(8,128)(2,1)S(1)}, u32[]{:S(2)}, u32[]{:S(2)}) collective-permute-start(bf16[128,2176]{1,0:T(8,128)(2,1)S(1)} %constant_dynamic-update-slice_fusion.refs_0_), channel_id=1, source_target_pairs={{0,2},{1,3},{2,0},{3,1},{4,6},{5,7},{6,4},{7,5},{8,10},{9,11},{10,... | collective-permute-start | bytes 1671176 | tf_op jit(solution)/shard_map/ppermute | solution.py:24
  23.0 13.6 %collective-permute-start.8 = (bf16[128,2176]{1,0:T(8,128)(2,1)S(1)}, bf16[128,2176]{1,0:T(8,128)(2,1)S(1)}, u32[]{:S(2)}, u32[]{:S(2)}) collective-permute-start(bf16[128,2176]{1,0:T(8,128)(2,1)S(1)} %constant_dynamic-update-slice_fusion.refs_0_), channel_id=1, source_target_pairs={{0,4},{4,0},{8,12},{12,8},{16,20},{20,16},{24,28},{28,24},{1,5},{5... | collective-permute-start | bytes 1671176 | tf_op jit(solution)/shard_map/ppermute | solution.py:24
  24.5 18.7 %collective-permute-start.11 = (bf16[128,2176]{1,0:T(8,128)(2,1)S(1)}, bf16[128,2176]{1,0:T(8,128)(2,1)S(1)}, u32[]{:S(2)}, u32[]{:S(2)}) collective-permute-start(bf16[128,2176]{1,0:T(8,128)(2,1)S(1)} %constant_dynamic-update-slice_fusion.refs_0_), channel_id=1, source_target_pairs={{0,1},{1,0},{2,3},{3,2},{4,5},{5,4},{6,7},{7,6},{8,9},{9,8},{10,11... | collective-permute-start | bytes 1671176 | tf_op jit(solution)/shard_map/ppermute | solution.py:24
  33.4 7.1 %collective-permute-start.9 = (bf16[64,2176]{1,0:T(8,128)(2,1)S(1)}, bf16[64,2176]{1,0:T(8,128)(2,1)S(1)}, u32[]{:S(2)}, u32[]{:S(2)}) collective-permute-start(bf16[64,2176]{1,0:T(8,128)(2,1)S(1)} %slice.82), channel_id=1, source_target_pairs={{0,4},{4,0},{8,12},{12,8},{16,20},{20,16},{24,28},{28,24},{1,5},{5... | collective-permute-start | bytes 835592 | tf_op jit(solution)/shard_map/ppermute | solution.py:24
  36.6 6.6 %collective-permute-start.10 = (bf16[64,2176]{1,0:T(8,128)(2,1)S(1)}, bf16[64,2176]{1,0:T(8,128)(2,1)S(1)}, u32[]{:S(2)}, u32[]{:S(2)}) collective-permute-start(bf16[64,2176]{1,0:T(8,128)(2,1)S(1)} %slice.83), channel_id=1, source_target_pairs={{0,2},{1,3},{2,0},{3,1},{4,6},{5,7},{6,4},{7,5},{8,10},{9,11},{10,... | collective-permute-start | bytes 835592 | tf_op jit(solution)/shard_map/ppermute | solution.py:24
  37.1 7.7 %collective-permute-start.12 = (bf16[128,2176]{1,0:T(8,128)(2,1)S(1)}, bf16[128,2176]{1,0:T(8,128)(2,1)S(1)}, u32[]{:S(2)}, u32[]{:S(2)}) collective-permute-start(bf16[128,2176]{1,0:T(8,128)(2,1)S(1)} %collective-permute-done.7.refs_1_), channel_id=1, source_target_pairs={{0,1},{1,0},{2,3},{3,2},{4,5},{5,4},{6,7},{7,6},{8,9},{9,8},{10,11... | collective-permute-start | bytes 1671176 | tf_op jit(solution)/shard_map/ppermute | solution.py:24
  37.1 8.4 %collective-permute-start.13 = (bf16[128,2176]{1,0:T(8,128)(2,1)S(1)}, bf16[128,2176]{1,0:T(8,128)(2,1)S(1)}, u32[]{:S(2)}, u32[]{:S(2)}) collective-permute-start(bf16[128,2176]{1,0:T(8,128)(2,1)S(1)} %collective-permute-done.8.refs_2_), channel_id=1, source_target_pairs={{0,1},{1,0},{2,3},{3,2},{4,5},{5,4},{6,7},{7,6},{8,9},{9,8},{10,11... | collective-permute-start | bytes 1671176 | tf_op jit(solution)/shard_map/ppermute | solution.py:24
  59.7 4.4 %collective-permute-start.16 = (bf16[512,2048]{1,0:T(8,128)(2,1)}, bf16[512,2048]{1,0:T(8,128)(2,1)S(1)}, u32[]{:S(2)}, u32[]{:S(2)}) collective-permute-start(bf16[512,2048]{1,0:T(8,128)(2,1)} %get-tuple-element.15), channel_id=1, source_target_pairs={{0,1},{1,0},{2,3},{3,2},{4,5},{5,4},{6,7},{7,6},{8,9},{9,8},{10,11... | collective-permute-start | bytes 6291464 | tf_op jit(solution)/shard_map/ppermute | solution.py:24
  65.6 9.1 %collective-permute-start.22 = (bf16[64,2048]{1,0:T(8,128)(2,1)S(1)}, bf16[64,2048]{1,0:T(8,128)(2,1)S(1)}, u32[]{:S(2)}, u32[]{:S(2)}) collective-permute-start(bf16[64,2048]{1,0:T(8,128)(2,1)S(1)} %get-tuple-element.20), channel_id=1, source_target_pairs={{0,2},{1,3},{2,0},{3,1},{4,6},{5,7},{6,4},{7,5},{8,10},{9,11},{10,... | collective-permute-start | bytes 786440 | tf_op jit(solution)/shard_map/ppermute | solution.py:24
  67.5 9.2 %collective-permute-start = (bf16[128,128]{1,0:T(8,128)(2,1)S(1)}, bf16[128,128]{1,0:T(8,128)(2,1)S(1)}, u32[]{:S(2)}, u32[]{:S(2)}) collective-permute-start(bf16[128,128]{1,0:T(8,128)(2,1)S(1)} %pad_maximum_fusion), channel_id=1, source_target_pairs={{0,4},{4,8},{8,12},{12,16},{16,20},{20,24},{24,28},{1,5},{5,9},{9,... | collective-permute-start | bytes 98312 | tf_op jit(solution)/shard_map/ppermute | solution.py:20
  70.8 13.5 %collective-permute-start.21 = (bf16[64,2048]{1,0:T(8,128)(2,1)S(1)}, bf16[64,2048]{1,0:T(8,128)(2,1)S(1)}, u32[]{:S(2)}, u32[]{:S(2)}) collective-permute-start(bf16[64,2048]{1,0:T(8,128)(2,1)S(1)} %get-tuple-element.19), channel_id=1, source_target_pairs={{0,2},{1,3},{2,0},{3,1},{4,6},{5,7},{6,4},{7,5},{8,10},{9,11},{10,... | collective-permute-start | bytes 786440 | tf_op jit(solution)/shard_map/ppermute | solution.py:24
  75.8 8.5 %collective-permute-start.23 = (bf16[64,2048]{1,0:T(8,128)(2,1)S(1)}, bf16[64,2048]{1,0:T(8,128)(2,1)S(1)}, u32[]{:S(2)}, u32[]{:S(2)}) collective-permute-start(bf16[64,2048]{1,0:T(8,128)(2,1)S(1)} %add_convert_fusion.1), channel_id=1, source_target_pairs={{0,4},{4,0},{8,12},{12,8},{16,20},{20,16},{24,28},{28,24},{1,5},{5... | collective-permute-start | bytes 786440 | tf_op jit(solution)/shard_map/ppermute | solution.py:24
  83.7 13.0 %collective-permute-start.2 = (bf16[1024,256]{1,0:T(8,128)(2,1)}, bf16[1024,256]{1,0:T(8,128)(2,1)S(1)}, u32[]{:S(2)}, u32[]{:S(2)}) collective-permute-start(bf16[1024,256]{1,0:T(8,128)(2,1)} %attend.1.refs_0_), channel_id=1, source_target_pairs={{0,2},{1,3},{2,0},{3,1},{4,6},{5,7},{6,4},{7,5},{8,10},{9,11},{10,... | collective-permute-start | bytes 1572872 | tf_op jit(solution)/shard_map/ppermute | solution.py:24
  85.7 11.4 %collective-permute-start.17 = (bf16[64,2048]{1,0:T(8,128)(2,1)S(1)}, bf16[64,2048]{1,0:T(8,128)(2,1)S(1)}, u32[]{:S(2)}, u32[]{:S(2)}) collective-permute-start(bf16[64,2048]{1,0:T(8,128)(2,1)S(1)} %get-tuple-element.18), channel_id=1, source_target_pairs={{0,4},{4,0},{8,12},{12,8},{16,20},{20,16},{24,28},{28,24},{1,5},{5... | collective-permute-start | bytes 786440 | tf_op jit(solution)/shard_map/ppermute | solution.py:24
  86.4 24.5 %collective-permute-start.1 = (bf16[1024,256]{1,0:T(8,128)(2,1)S(1)}, bf16[1024,256]{1,0:T(8,128)(2,1)S(1)}, u32[]{:S(2)}, u32[]{:S(2)}) collective-permute-start(bf16[1024,256]{1,0:T(8,128)(2,1)S(1)} %copy-done.11), channel_id=1, source_target_pairs={{0,1},{1,0},{2,3},{3,2},{4,5},{5,4},{6,7},{7,6},{8,9},{9,8},{10,11... | collective-permute-start | bytes 1572872 | tf_op jit(solution)/shard_map/ppermute | solution.py:24
  96.7 14.2 %collective-permute-start.3 = (bf16[1024,256]{1,0:T(8,128)(2,1)S(1)}, bf16[1024,256]{1,0:T(8,128)(2,1)}, u32[]{:S(2)}, u32[]{:S(2)}) collective-permute-start(bf16[1024,256]{1,0:T(8,128)(2,1)S(1)} %collective-permute-done.2.refs_2_), channel_id=1, source_target_pairs={{0,1},{1,0},{2,3},{3,2},{4,5},{5,4},{6,7},{7,6},{8,9},{9,8},{10,11... | collective-permute-start | bytes 1572872 | tf_op jit(solution)/shard_map/ppermute | solution.py:24
  96.7 8.7 %collective-permute-start.19 = (bf16[64,2048]{1,0:T(8,128)(2,1)S(1)}, bf16[64,2048]{1,0:T(8,128)(2,1)S(1)}, u32[]{:S(2)}, u32[]{:S(2)}) collective-permute-start(bf16[64,2048]{1,0:T(8,128)(2,1)S(1)} %get-tuple-element.17), channel_id=1, source_target_pairs={{0,4},{4,0},{8,12},{12,8},{16,20},{20,16},{24,28},{28,24},{1,5},{5... | collective-permute-start | bytes 786440 | tf_op jit(solution)/shard_map/ppermute | solution.py:24
  98.2 9.5 %collective-permute-start.18 = (bf16[64,2048]{1,0:T(8,128)(2,1)S(1)}, bf16[64,2048]{1,0:T(8,128)(2,1)S(1)}, u32[]{:S(2)}, u32[]{:S(2)}) collective-permute-start(bf16[64,2048]{1,0:T(8,128)(2,1)S(1)} %add_convert_fusion.6), channel_id=1, source_target_pairs={{0,2},{1,3},{2,0},{3,1},{4,6},{5,7},{6,4},{7,5},{8,10},{9,11},{10,... | collective-permute-start | bytes 786440 | tf_op jit(solution)/shard_map/ppermute | solution.py:24
  98.8 18.6 %collective-permute-start.24 = (bf16[32,2048]{1,0:T(8,128)(2,1)S(1)}, bf16[32,2048]{1,0:T(8,128)(2,1)S(1)}, u32[]{:S(2)}, u32[]{:S(2)}) collective-permute-start(bf16[32,2048]{1,0:T(8,128)(2,1)S(1)} %get-tuple-element.22), channel_id=1, source_target_pairs={{0,16},{4,20},{8,24},{12,28},{16,0},{20,4},{24,8},{28,12},{1,17},{... | collective-permute-start | bytes 393224 | tf_op jit(solution)/shard_map/ppermute | solution.py:24
  105.4 11.9 %collective-permute-start.25 = (bf16[32,2048]{1,0:T(8,128)(2,1)S(1)}, bf16[32,2048]{1,0:T(8,128)(2,1)S(1)}, u32[]{:S(2)}, u32[]{:S(2)}) collective-permute-start(bf16[32,2048]{1,0:T(8,128)(2,1)S(1)} %get-tuple-element.21), channel_id=1, source_target_pairs={{0,24},{4,28},{8,16},{12,20},{16,8},{20,12},{24,0},{28,4},{1,25},{... | collective-permute-start | bytes 393224 | tf_op jit(solution)/shard_map/ppermute | solution.py:24
  109.5 7.9 %collective-permute-start.20 = (bf16[32,2048]{1,0:T(8,128)(2,1)S(1)}, bf16[32,2048]{1,0:T(8,128)(2,1)S(1)}, u32[]{:S(2)}, u32[]{:S(2)}) collective-permute-start(bf16[32,2048]{1,0:T(8,128)(2,1)S(1)} %get-tuple-element.23), channel_id=1, source_target_pairs={{0,8},{4,12},{8,0},{12,4},{16,24},{20,28},{24,16},{28,20},{1,9},{5... | collective-permute-start | bytes 393224 | tf_op jit(solution)/shard_map/ppermute | solution.py:24
  (21 other events, 101.0 us)

commit v2 on v1

--- a/solution.py
+++ b/solution.py
@@ -7,6 +7,7 @@
 from jax.experimental.pallas import tpu as pltpu
 from jax.sharding import PartitionSpec as P
 
+
 HEADS = 16
 KV = 4
 HD = 64
@@ -24,31 +25,45 @@
     return lax.ppermute(value, axis, [(i, i ^ bits) for i in range(lax.axis_size(axis))])
 
 
+def in_vmem(*values):
+    return [pltpu.with_memory_space_constraint(v, pltpu.VMEM) for v in values]
+
+
+def in_hbm(*values):
+    return [pltpu.with_memory_space_constraint(v, pltpu.HBM) for v in values]
+
+
+def vmem_out(shape, dtype=jnp.bfloat16):
+    return pltpu.VMEM(shape, dtype)
+
+
 def dot_f32(a, b, contract):
     return lax.dot_general(a, b, ((contract[:1], contract[1:]), ((), ())), preferred_element_type=jnp.float32)
 
 
-def attention_kernel(place_ref, q_ref, kt_ref, vt_ref, halo_ref, sink_ref, out_ref, *, kv_local, group_size):
+def attention_kernel(place_ref, q_ref, kt_ref, vt_ref, sink_ref, *refs, first, kv_local, group_size):
+    *halo, out_ref = refs
     span = WINDOW
-    rows = q_ref.shape[0]
     query_index = lax.broadcasted_iota(jnp.int32, (span, 2 * span), 0)
     key_index = lax.broadcasted_iota(jnp.int32, (span, 2 * span), 1)
     banded = (key_index > query_index) & (key_index <= query_index + span)
-    first_banded = banded & ((key_index >= span) | (place_ref[0] > 0))
     half = kv_local * HD
-    for block in range(rows // span):
-        here = pl.ds(block * span, span)
-        allowed = first_banded if block == 0 else banded
+    for block in range(out_ref.shape[0] // span):
+        here = pl.ds((first + block) * span, span)
+        band = pl.ds((first + block - 1) * span, 2 * span)
+        at_start = first + block == 0
+        allowed = banded & ((key_index >= span) | (place_ref[0] > 0)) if at_start else banded
         for kv in range(kv_local):
             heads = pl.ds(kv * HD, HD)
-            if block == 0:
+            if at_start:
+                (halo_ref,) = halo
                 k_band = jnp.concatenate([halo_ref[kv * HD : (kv + 1) * HD, :], kt_ref[heads, here]], axis=1)
                 v_band = jnp.concatenate(
                     [halo_ref[half + kv * HD : half + (kv + 1) * HD, :], vt_ref[heads, here]], axis=1
                 )
             else:
-                k_band = kt_ref[heads, pl.ds((block - 1) * span, 2 * span)]
-                v_band = vt_ref[heads, pl.ds((block - 1) * span, 2 * span)]
+                k_band = kt_ref[heads, band]
+                v_band = vt_ref[heads, band]
             mixed = []
             for member in range(group_size):
                 head = kv * group_size + member
@@ -60,54 +75,74 @@
                 denominator = jnp.sum(weights_exp, axis=1, keepdims=True) + jnp.exp(sink - row_max)
                 probs = (weights_exp * (1.0 / denominator)).astype(jnp.bfloat16)
                 mixed.append(dot_f32(probs, v_band, (1, 1)))
-            out_ref[here, pl.ds(kv * group_size * HD, group_size * HD)] = jnp.concatenate(mixed, axis=1).astype(
-                jnp.bfloat16
+            out_ref[block * span : (block + 1) * span, pl.ds(kv * group_size * HD, group_size * HD)] = (
+                jnp.concatenate(mixed, axis=1).astype(jnp.bfloat16)
             )
 
 
-def attend(place, q_heads, k_t, v_t, halo, sink_logits, kv_local, group_size):
+def attend(place, q_heads, k_t, v_t, sink_logits, first, last, halo):
+    kv_local = k_t.shape[0] // HD
     vmem = pl.BlockSpec(memory_space=pltpu.VMEM)
     smem = pl.BlockSpec(memory_space=pltpu.SMEM)
     return pl.pallas_call(
-        functools.partial(attention_kernel, kv_local=kv_local, group_size=group_size),
-        out_shape=jax.ShapeDtypeStruct(q_heads.shape, jnp.bfloat16),
-        in_specs=[smem, vmem, vmem, vmem, vmem, smem],
+        functools.partial(attention_kernel, first=first, kv_local=kv_local, group_size=HEADS // KV),
+        out_shape=jax.ShapeDtypeStruct(((last - first) * WINDOW, q_heads.shape[1]), jnp.bfloat16),
+        in_specs=[smem, vmem, vmem, vmem, smem] + [vmem] * len(halo),
         out_specs=vmem,
-        cost_estimate=pl.CostEstimate(flops=6_000_000_000, bytes_accessed=2_000_000, transcendentals=0),
+        cost_estimate=pl.CostEstimate(flops=3_000_000_000, bytes_accessed=2_000_000, transcendentals=0),
+        compiler_params=pltpu.CompilerParams(vmem_limit_bytes=12 << 20),
         name="attend",
-    )(place, q_heads, k_t, v_t, halo, sink_logits)
-
-
-def projection_kernel(place_ref, *refs):
-    *pieces, weight_ref, out_ref = refs
-    width = pieces[0].shape[1]
-    total = None
-    for bits, piece in enumerate(pieces):
-        rows = pl.ds(pl.multiple_of((place_ref[1] ^ bits) * width, width), width)
-        part = dot_f32(piece[...], weight_ref[rows, :], (1, 0))
-        total = part if total is None else total + part
-    out_ref[...] = total.astype(jnp.bfloat16)
-
-
-def project(place, pieces, out_weight):
+    )(place, q_heads, k_t, v_t, sink_logits, *halo)
+
+
+def projection_kernel(place_ref, *refs, count, first, steps):
+    pieces, weight_ref = refs[:count], refs[count]
+    out_ref, tile_ref, sems = refs[-3:]
     rows, width = pieces[0].shape
-    tile = rows // 4
+    tile = rows // steps
+    copies = []
+    for i in range(steps):
+        total = None
+        for bits, piece in enumerate(pieces):
+            lines = pl.ds(pl.multiple_of((place_ref[1] ^ bits) * width, width), width)
+            product = dot_f32(piece[i * tile : (i + 1) * tile, :], weight_ref[lines, :], (1, 0))
+            total = product if total is None else total + product
+        tile_ref[i] = total.astype(jnp.bfloat16)
+        copies.append(
+            pltpu.make_async_copy(tile_ref.at[i], out_ref.at[pl.ds(first + i * tile, tile), :], sems.at[i])
+        )
+        copies[-1].start()
+    for copy in copies:
+        copy.wait()
+
+
+def project(place, pieces, out_weight, part, parts, held):
+    rows = pieces[0].shape[0]
+    steps = 2
+    vmem = pl.BlockSpec(memory_space=pltpu.VMEM)
+    operands = [place, *in_vmem(*pieces, out_weight), *held]
     return pl.pallas_call(
-        projection_kernel,
-        grid_spec=pltpu.PrefetchScalarGridSpec(
-            num_scalar_prefetch=1,
-            grid=(rows // tile,),
-            in_specs=[pl.BlockSpec((tile, width), lambda i, s: (i, 0)) for _ in pieces]
-            + [pl.BlockSpec(out_weight.shape, lambda i, s: (0, 0))],
-            out_specs=pl.BlockSpec((tile, out_weight.shape[1]), lambda i, s: (i, 0)),
-        ),
-        out_shape=jax.ShapeDtypeStruct((rows, out_weight.shape[1]), jnp.bfloat16),
-        cost_estimate=pl.CostEstimate(flops=2_000_000_000, bytes_accessed=4_000_000, transcendentals=0),
+        functools.partial(projection_kernel, count=len(pieces), first=part * rows, steps=steps),
+        in_specs=[pl.BlockSpec(memory_space=pltpu.SMEM)]
+        + [vmem] * (len(pieces) + 1)
+        + [pl.BlockSpec(memory_space=pl.ANY) for _ in held],
+        out_specs=pl.BlockSpec(memory_space=pl.ANY),
+        out_shape=pltpu.HBM((rows * parts, out_weight.shape[1]), jnp.bfloat16),
+        scratch_shapes=[
+            pltpu.VMEM((steps, rows // steps, out_weight.shape[1]), jnp.bfloat16),
+            pltpu.SemaphoreType.DMA((steps,)),
+        ],
+        input_output_aliases={len(operands) - 1: 0} if held else {},
+        cost_estimate=pl.CostEstimate(flops=1_000_000_000, bytes_accessed=3_000_000, transcendentals=0),
+        compiler_params=pltpu.CompilerParams(vmem_limit_bytes=8 << 20),
         name="project",
-    )(place, *pieces, out_weight)
-
-
-def dispatch_kernel(place_ref, tokens_ref, gain_ref, group_ref, expert_ref, routes_ref, order_ref, *send_refs):
+    )(*operands)
+
+
+def dispatch_kernel(
+    place_ref, tokens_ref, gain_ref, group_ref, expert_ref, routes_ref, k_ref, v_ref, order_ref, tail_ref, *send_refs
+):
+    tail_ref[...] = jnp.concatenate([k_ref[...], v_ref[...]], axis=0)
     groups = group_ref.shape[0]
     experts = expert_ref.shape[0]
     size = experts // groups
@@ -155,10 +190,11 @@
         send[:, width:] = moved_gates[k * step : (k + 1) * step]
 
 
-def dispatch(place, tokens, gain, group_t, expert_t, routes_t, rows):
+def dispatch(place, tokens, gain, group_t, expert_t, routes_t, k_t, v_t, rows):
     width = tokens.shape[1]
     groups = group_t.shape[0]
     step = rows // groups
+    last = k_t.shape[1] // WINDOW - 1
     whole = lambda shape: pl.BlockSpec(shape, lambda i, s: tuple(0 for _ in shape))
     return pl.pallas_call(
         dispatch_kernel,
@@ -171,48 +207,44 @@
                 whole(group_t.shape),
                 whole(expert_t.shape),
                 pl.BlockSpec((2, rows), lambda i, s: (0, s[1])),
+                pl.BlockSpec((k_t.shape[0], WINDOW), lambda i, s: (0, last)),
+                pl.BlockSpec((v_t.shape[0], WINDOW), lambda i, s: (0, last)),
             ],
-            out_specs=[whole((rows, rows))] + [whole((step, width + LANES)) for _ in range(groups)],
+            out_specs=[whole((rows, rows)), whole((k_t.shape[0] + v_t.shape[0], WINDOW))] + [whole((step, width + LANES)) for _ in range(groups)],
         ),
-        out_shape=[jax.ShapeDtypeStruct((rows, rows), jnp.bfloat16)]
+        out_shape=[
+            jax.ShapeDtypeStruct((rows, rows), jnp.bfloat16),
+            jax.ShapeDtypeStruct((k_t.shape[0] + v_t.shape[0], WINDOW), jnp.bfloat16),
+        ]
         + [jax.ShapeDtypeStruct((step, width + LANES), jnp.bfloat16) for _ in range(groups)],
         cost_estimate=pl.CostEstimate(flops=1_000_000_000, bytes_accessed=2_000_000, transcendentals=0),
+        compiler_params=pltpu.CompilerParams(vmem_limit_bytes=12 << 20),
         name="dispatch",
-    )(place, tokens, gain.reshape(1, width), group_t, expert_t, routes_t)
-
-
-def experts_kernel(place_ref, *refs, sizes, size, tile):
+    )(place, *in_hbm(tokens, gain.reshape(1, width), group_t, expert_t, routes_t, k_t, v_t))
+
+
+def experts_kernel(place_ref, *refs, sizes, size):
     count = len(sizes)
     pieces = refs[:count]
-    gate_ref, up_ref, down_ref, here_ref, there_ref, rows_ref = refs[count:]
-    exp_local, width, hidden = gate_ref.shape
+    gate_ref, up_ref, down_ref, out_ref, rows_ref = refs[count:]
+    exp_local, width, _ = gate_ref.shape
     at = 0
     for piece, rows in zip(pieces, sizes):
         rows_ref[at : at + rows, :] = piece[...]
         at += rows
-    half = at // 2
-    line = lax.broadcasted_iota(jnp.int32, (tile, LANES), 1)
-    for start in range(0, at, tile):
-        held = rows_ref[start : start + tile, :width]
-        gates = rows_ref[start : start + tile, width:].astype(jnp.float32)
-        active = []
-        for e in range(exp_local):
-            own = place_ref[3] * exp_local + e
-            gate = jnp.sum(
-                jnp.where((line == own) | (line == own + size), gates, 0.0), axis=1, keepdims=True
-            )
-            gate_pre = dot_f32(held, gate_ref[e], (1, 0))
-            up_pre = dot_f32(held, up_ref[e], (1, 0))
-            active.append((jax.nn.silu(gate_pre) * up_pre * gate).astype(jnp.bfloat16))
-        result = None
-        for e in range(exp_local):
-            part = dot_f32(active[e], down_ref[e], (1, 0))
-            result = part if result is None else result + part
-        result = result.astype(jnp.bfloat16)
-        if start < half:
-            here_ref[start : start + tile, :] = result
-        else:
-            there_ref[start - half : start - half + tile, :] = result
+    held = rows_ref[:, :width]
+    gates = rows_ref[:, width:].astype(jnp.float32)
+    line = lax.broadcasted_iota(jnp.int32, gates.shape, 1)
+    result = None
+    for e in range(exp_local):
+        own = place_ref[3] * exp_local + e
+        gate = jnp.sum(jnp.where((line == own) | (line == own + size), gates, 0.0), axis=1, keepdims=True)
+        gate_pre = dot_f32(held, gate_ref[e], (1, 0))
+        up_pre = dot_f32(held, up_ref[e], (1, 0))
+        active = (jax.nn.silu(gate_pre) * up_pre * gate).astype(jnp.bfloat16)
+        part = dot_f32(active, down_ref[e], (1, 0))
+        result = part if result is None else result + part
+    out_ref[...] = result.astype(jnp.bfloat16)
 
 
 def run_experts(place, pieces, expert_gate, expert_up, expert_down, size):
@@ -222,14 +254,15 @@
     vmem = pl.BlockSpec(memory_space=pltpu.VMEM)
     smem = pl.BlockSpec(memory_space=pltpu.SMEM)
     return pl.pallas_call(
-        functools.partial(experts_kernel, sizes=sizes, size=size, tile=min(rows // 2, 256)),
-        out_shape=[jax.ShapeDtypeStruct((rows // 2, width), jnp.bfloat16) for _ in range(2)],
+        functools.partial(experts_kernel, sizes=sizes, size=size),
+        out_shape=vmem_out((rows, width)),
         in_specs=[smem] + [vmem] * (len(pieces) + 3),
-        out_specs=[vmem, vmem],
+        out_specs=vmem,
         scratch_shapes=[pltpu.VMEM((rows, width + LANES), jnp.bfloat16)],
         cost_estimate=pl.CostEstimate(flops=rows * 7_000_000, bytes_accessed=15_000_000, transcendentals=0),
+        compiler_params=pltpu.CompilerParams(vmem_limit_bytes=14 << 20),
         name="experts",
-    )(place, *pieces, expert_gate, expert_up, expert_down)
+    )(place, *in_vmem(*pieces, expert_gate, expert_up, expert_down))
 
 
 def combine_kernel(order_ref, *refs):
@@ -245,12 +278,30 @@
         out_shape=jax.ShapeDtypeStruct((order.shape[0], pieces[0].shape[1]), jnp.bfloat16),
         in_specs=[vmem] * (len(pieces) + 1),
         out_specs=vmem,
+        compiler_params=pltpu.CompilerParams(vmem_limit_bytes=8 << 20),
         name="combine",
-    )(order, *pieces)
-
-
-def added(*values):
-    return functools.reduce(jnp.add, [v.astype(jnp.float32) for v in values]).astype(jnp.bfloat16)
+    )(*in_vmem(order, *pieces))
+
+
+def sums_kernel(*refs, plan):
+    values, outs = refs[: len(refs) - len(plan)], refs[len(refs) - len(plan) :]
+    for out, segments in zip(outs, plan):
+        for at, rows, terms in segments:
+            parts = [values[i][start : start + rows, :].astype(jnp.float32) for i, start in terms]
+            out[at : at + rows, :] = functools.reduce(jnp.add, parts).astype(jnp.bfloat16)
+
+
+def sums(plan, *values):
+    vmem = pl.BlockSpec(memory_space=pltpu.VMEM)
+    width = values[0].shape[1]
+    return pl.pallas_call(
+        functools.partial(sums_kernel, plan=plan),
+        out_shape=[vmem_out((sum(rows for _, rows, _ in segments), width)) for segments in plan],
+        in_specs=[vmem] * len(values),
+        out_specs=[vmem] * len(plan),
+        compiler_params=pltpu.CompilerParams(vmem_limit_bytes=4 << 20),
+        name="sums",
+    )(*in_vmem(*values))
 
 
 def gather_plane(own, core_bit, side_bit):
@@ -260,25 +311,41 @@
     far_low = flipped(across[:half], "ep", 1)
     far_high = flipped(along[half:], "tp", side_bit)
     ours = [own, across, along, far_low, far_high]
-    return ours + [flipped(piece, "tp", core_bit) for piece in ours]
-
-
-def reduce_plane(here, there, core_bit, side_bit):
+    return ours, [flipped(piece, "tp", core_bit) for piece in ours]
+
+
+def reduce_plane(here, there, core_bit, side_bit, chunks):
     step = here.shape[0] // 4
     half = step // 2
     other = flipped(there, "tp", core_bit)
-    part = lambda low, high: added(here[low:high], other[low:high])
-    far_low = flipped(part(3 * step, 3 * step + half), "ep", 1)
-    far_high = flipped(part(3 * step + half, 4 * step), "tp", side_bit)
-    across_high = flipped(part(step + half, 2 * step), "tp", side_bit)
-    along_low = flipped(part(2 * step, 2 * step + half), "ep", 1)
-    across_low = flipped(added(here[step : step + half], other[step : step + half], far_low), "tp", side_bit)
-    along_high = flipped(
-        added(here[2 * step + half : 3 * step], other[2 * step + half : 3 * step], far_high), "ep", 1
-    )
-    low = added(here[:half], other[:half], across_low, along_low)
-    high = added(here[half:step], other[half:step], across_high, along_high)
-    return low, high
+    both = lambda at: ((0, at), (1, at))
+    far_low, far_high = sums(
+        (((0, half, both(3 * step)),), ((0, half, both(3 * step + half)),)), here, other
+    )
+    far_low = flipped(far_low, "ep", 1)
+    far_high = flipped(far_high, "tp", side_bit)
+    across, along = sums(
+        (
+            ((0, half, both(step) + ((2, 0),)), (half, half, both(step + half))),
+            ((0, half, both(2 * step)), (half, half, both(2 * step + half) + ((3, 0),))),
+        ),
+        here,
+        other,
+        far_low,
+        far_high,
+    )
+    across = flipped(across, "tp", side_bit)
+    along = flipped(along, "ep", 1)
+    piece = step // chunks
+    return sums(
+        tuple(
+            ((0, piece, both(i * piece) + ((2, i * piece), (3, i * piece))),) for i in range(chunks)
+        ),
+        here,
+        other,
+        across,
+        along,
+    )
 
 
 def per_device(
@@ -316,14 +383,14 @@
     tp_index = lax.axis_index("tp")
     place = jnp.stack([ep_index, tp_index, ep_index // members, ep_index % members]).astype(jnp.int32)
 
-    kv_local = k_heads.shape[1] // HD
     k_t = k_heads.T
     v_t = v_heads.T
+    blocks = k_heads.shape[0] // WINDOW
     last = k_heads.shape[0] - WINDOW
-    halo = shifted(jnp.concatenate([k_t[:, last:], v_t[:, last:]], axis=0), "ep", 1)
 
     if not by_group:
-        attended = attend(place, q_heads, k_t, v_t, halo, sink_logits, kv_local, HEADS // KV)
+        halo = shifted(jnp.concatenate([k_t[:, last:], v_t[:, last:]], axis=0), "ep", 1)
+        attended = attend(place, q_heads, k_t, v_t, sink_logits, 0, blocks, [halo])
         mixed = jnp.dot(
             lax.all_gather(attended, "tp", axis=1, tiled=True), out_weight, preferred_element_type=jnp.float32
         )
@@ -335,22 +402,37 @@
         )
 
     core_bit, side_bit = 1, 2
-    order, *sends = dispatch(
-        place, tokens_b, moe_gain, router_group.T, router_expert.T, route_expert.T, rows_dev
-    )
+    order, tail, *sends = dispatch(
+        place, tokens_b, moe_gain, router_group.T, router_expert.T, route_expert.T, k_t, v_t, rows_dev
+    )
+    halo = shifted(tail, "ep", 1)
+    chunks = ((0, 2), (1, 3)) if groups == 4 else (tuple(range(groups)),)
     arrived = [sends[0]] + [flipped(sends[k], "ep", k * members) for k in range(1, groups)]
-    attended = attend(place, q_heads, k_t, v_t, halo, sink_logits, kv_local, HEADS // KV)
-    pieces = gather_plane(jnp.concatenate(arrived, axis=0), core_bit, side_bit)
-    attended_core = flipped(attended, "tp", core_bit)
-    attended_side = flipped(attended, "tp", side_bit)
-    attended_both = flipped(attended_side, "tp", core_bit)
-    here, there = run_experts(place, pieces, expert_gate, expert_up, expert_down, size)
-    low, high = reduce_plane(here, there, core_bit, side_bit)
-    mixer_out = project(place, [attended, attended_core, attended_side, attended_both], out_weight)
-    step = rows_dev // groups
-    totals = jnp.split(low, low.shape[0] // step) + jnp.split(high, high.shape[0] // step)
-    returned = [totals[0]] + [flipped(totals[k], "ep", k * members) for k in range(1, groups)]
-    return (mixer_out, combine(order, returned))
+    middle = blocks // 2
+    attended = []
+    for first, end in ((0, middle), (middle, blocks)):
+        attended.append(attend(place, q_heads, k_t, v_t, sink_logits, first, end, [halo] if first == 0 else []))
+    results = []
+    for chunk in chunks:
+        own = jnp.concatenate([arrived[k] for k in chunk], axis=0)
+        halves = []
+        for pieces in gather_plane(own, core_bit, side_bit):
+            halves.append(run_experts(place, pieces, expert_gate, expert_up, expert_down, size))
+        results.append(halves)
+    core = [flipped(part, "tp", core_bit) for part in attended]
+    side = [flipped(part, "tp", side_bit) for part in attended]
+    cross = [flipped(part, "tp", core_bit) for part in side]
+    held = []
+    for part in reversed(range(len(attended))):
+        pieces = [attended[part], core[part], side[part], cross[part]]
+        held = [project(place, pieces, out_weight, part, len(attended), held)]
+    (mixer_out,) = held
+    returned = {}
+    for chunk, (here, there) in zip(chunks, results):
+        totals = reduce_plane(here, there, core_bit, side_bit, len(chunk))
+        for k, total in zip(chunk, totals):
+            returned[k] = flipped(total, "ep", k * members) if k else total
+    return (mixer_out, combine(order, [returned[k] for k in range(groups)]))
 
 
 def normalize(rows_in, gain):
@@ -421,4 +503,5 @@
         P("ep", "tp", None),
     )
     out_specs = (P("ep", "tp"), P(("ep", "tp"), None))
+
     return jax.shard_map(per_device, mesh=mesh, in_specs=in_specs, out_specs=out_specs, check_vma=False)

time: 121 us -> 106 us (0.88)
  starting transfers between devices: 28.4 us -> 37.5 us
  Pallas kernels: 30.2 us -> 22.9 us
  other arithmetic: 6.75 us -> 0.08 us
  local copies, waits for them, and re-layouts: 7.61 us -> 1.73 us
  waiting for transfers between devices: 46.5 us -> 42.2 us
    ppermute x25 -> x40, starting transfers between devices: 25.2 us -> 33.8 us  [flipped(): lax.ppermute(value, axis, [(i, i ^ bits) for i in range(lax.axis_size(axi...]
    convert_element_type x5 -> x0, other arithmetic: 6.15 us -> none  [added(): functools.reduce(jnp.add, [v.astype(jnp.float32) for v in values])]
    pallas_call x3 -> x14, Pallas kernels: 24.5 us -> 19 us  [the longest x4 9.76 us: run_experts(): pl.pallas_call(functools.partial(experts_kernel, sizes=sizes, size=size),...]
    ppermute x25 -> x40, waiting for transfers between devices: 46.5 us -> 42.2 us  [flipped(): lax.ppermute(value, axis, [(i, i ^ bits) for i in range(lax.axis_size(axi...]
    unnamed x41 -> x20, local copies, waits for them, and re-layouts: 5.42 us -> 1.65 us
    slice x2 -> x0, local copies, waits for them, and re-layouts: 1.44 us -> none  [the longest x1 0.72 us: per_device(): k_t[:, last:]]
  transfers between devices with their start and end apart: 26 -> 41, of which waited for: 11 -> 14; matrix products, arithmetic and copies ran while one was open for 6% -> 0% of each run, Pallas kernels for 10% -> 18%
where the time goes in v2:
time: 106 us; the launch traced here: 105 us
  waiting for transfers between devices  42.2 us (40%)
  starting transfers between devices  37.5 us (35%)
  Pallas kernels  22.9 us (22%)
  local copies, waits for them, and re-layouts  1.73 us (2%)
    ppermute x40, waiting for transfers between devices, flipped(): lax.ppermute(value, axis, [(i, i ^ bits) for i in range(lax.axis_size(axi...  42.2 us
    ppermute x40, starting transfers between devices, flipped(): lax.ppermute(value, axis, [(i, i ^ bits) for i in range(lax.axis_size(axi...  33.8 us
    pallas_call x4, Pallas kernels, run_experts(): pl.pallas_call(functools.partial(experts_kernel, sizes=sizes, size=size),...  9.76 us
    pallas_call x2, Pallas kernels, attend(): pl.pallas_call(functools.partial(attention_kernel, first=first, kv_local=...  4.56 us
    pallas_call x2, Pallas kernels, project(): pl.pallas_call(functools.partial(projection_kernel, count=len(pieces), fi...  3.95 us
    ppermute x1, starting transfers between devices, shifted(): lax.ppermute(value, axis, [(source, source + steps) for source in range(l...  3.72 us
    pallas_call x1, Pallas kernels, dispatch(): pl.pallas_call(dispatch_kernel, grid_spec=pltpu.PrefetchScalarGridSpec(nu...  2.79 us
  transfers between devices with their start and end apart: 41, of which 14 were waited for; matrix products, arithmetic and copies ran while one was open for 0% of the time, Pallas kernels for 18%

profile of v2, /device:TPU:0, one launch (start us, length us, event | category | flops | bytes accessed | tf_op | source)
XLA Modules:
  0.0 105.3 jit_solution(9502227690186992790)
XLA Ops:
  0.7 2.8 %dispatch.1 = (bf16[128,128]{1,0:T(8,128)(2,1)S(1)}, bf16[128,128]{1,0:T(8,128)(2,1)S(1)}, bf16[32,2176]{1,0:T(8,128)(2,1)S(1)}, bf16[32,2176]{1,0:T(8,128)(2,1)...) custom-call(s32[4]{0:T(128)S(1)} %pad_add_fusion.place_ref, bf16[512,2048]{1,0:T(8,128)(2,1)} %tokens_ref.1, ...), custom_call_target="tpu_custom_call" | custom-call | flops 1000000000 | bytes 2000000 | tf_op jit(solution)/shard_map/dispatch/pallas_call | solution.py:199
  3.5 3.1 %collective-permute-start.22 = (bf16[32,2176]{1,0:T(8,128)(2,1)S(1)}, bf16[32,2176]{1,0:T(8,128)(2,1)S(1)}, u32[]{:S(2)}, u32[]{:S(2)}) collective-permute-start(bf16[32,2176]{1,0:T(8,128)(2,1)S(1)} %get-tuple-element.29), channel_id=1, source_target_pairs={{0,8},{4,12},{8,0},{12,4},{16,24},{20,28},{24,16},{28,20},{1,9},{5... | collective-permute-start | bytes 417800 | tf_op jit(solution)/shard_map/ppermute | solution.py:25
  6.6 2.5 %collective-permute-start.23 = (bf16[32,2176]{1,0:T(8,128)(2,1)S(1)}, bf16[32,2176]{1,0:T(8,128)(2,1)S(1)}, u32[]{:S(2)}, u32[]{:S(2)}) collective-permute-start(bf16[32,2176]{1,0:T(8,128)(2,1)S(1)} %get-tuple-element.30), channel_id=1, source_target_pairs={{0,24},{4,28},{8,16},{12,20},{16,8},{20,12},{24,0},{28,4},{1,25},{... | collective-permute-start | bytes 417800 | tf_op jit(solution)/shard_map/ppermute | solution.py:25
  10.4 6.3 %collective-permute-done.23 = bf16[32,2176]{1,0:T(8,128)(2,1)S(1)} collective-permute-done((bf16[32,2176]{1,0:T(8,128)(2,1)S(1)}, bf16[32,2176]{1,0:T(8,128)(2,1)S(1)}, u32[]{:S(2)}, u32[]{:S(2)}) %collective-permute-start.23) | collective-permute-done | bytes 139296 | tf_op jit(solution)/shard_map/ppermute | solution.py:25
  26.5 4.3 %collective-permute-done.8.refs_1_ = bf16[64,2176]{1,0:T(8,128)(2,1)S(1)} collective-permute-done((bf16[64,2176]{1,0:T(8,128)(2,1)S(1)}, bf16[64,2176]{1,0:T(8,128)(2,1)S(1)}, u32[]{:S(2)}, u32[]{:S(2)}) %collective-permute-start.8) | collective-permute-done | bytes 278560 | tf_op jit(solution)/shard_map/ppermute | solution.py:25
  32.9 2.7 %collective-permute-done.26.refs_3_ = bf16[32,2176]{1,0:T(8,128)(2,1)S(1)} collective-permute-done((bf16[32,2176]{1,0:T(8,128)(2,1)S(1)}, bf16[32,2176]{1,0:T(8,128)(2,1)S(1)}, u32[]{:S(2)}, u32[]{:S(2)}) %collective-permute-start.26) | collective-permute-done | bytes 139296 | tf_op jit(solution)/shard_map/ppermute | solution.py:25
  38.2 2.5 %collective-permute-done.11.refs_4_ = bf16[32,2176]{1,0:T(8,128)(2,1)S(1)} collective-permute-done((bf16[32,2176]{1,0:T(8,128)(2,1)S(1)}, bf16[32,2176]{1,0:T(8,128)(2,1)S(1)}, u32[]{:S(2)}, u32[]{:S(2)}) %collective-permute-start.11) | collective-permute-done | bytes 139296 | tf_op jit(solution)/shard_map/ppermute | solution.py:25
  43.4 2.4 %experts.7 = bf16[256,2048]{1,0:T(8,128)(2,1)S(1)} custom-call(s32[4]{0:T(128)S(1)} %pad_add_fusion.place_ref, bf16[64,2176]{1,0:T(8,128)(2,1)S(1)} %collective-permute-done.28.refs_0_, bf16[64,2176]{1,0:T(8,128)(2,1)S(1)} %collective-permute-done.29.refs_1_, bf16[64,2176]{1,0:T(8,128)(2,1)S(1)} %collective-permute-done.30.refs_2_, ...), custom_call_target="tpu_custom_call" | custom-call | flops 1792000000 | bytes 15000000 | tf_op jit(solution)/shard_map/experts/pallas_call | solution.py:256
  46.5 2.4 %experts.5 = bf16[256,2048]{1,0:T(8,128)(2,1)S(1)} custom-call(s32[4]{0:T(128)S(1)} %pad_add_fusion.place_ref, bf16[64,2176]{1,0:T(8,128)(2,1)S(1)} %collective-permute-done.12.refs_0_, bf16[64,2176]{1,0:T(8,128)(2,1)S(1)} %collective-permute-done.13.refs_1_, bf16[64,2176]{1,0:T(8,128)(2,1)S(1)} %collective-permute-done.14.refs_2_, ...), custom_call_target="tpu_custom_call" | custom-call | flops 1792000000 | bytes 15000000 | tf_op jit(solution)/shard_map/experts/pallas_call | solution.py:256
  49.1 2.3 %attend.3.refs_0_ = bf16[512,256]{1,0:T(8,128)(2,1)S(1)} custom-call(s32[4]{0:T(128)S(1)} %pad_add_fusion.place_ref, bf16[1024,256]{1,0:T(8,128)(2,1)S(1)} %copy-done.5, bf16[64,1024]{1,0:T(8,128)(2,1)S(1)} %bitcast.11, bf16[64,1024]{1,0:T(8,128)(2,1)S(1)} %bitcast.14, f32[4]{0:T(128)S(1)} %copy-done.8), custom_call_target="tpu_custom_call" | custom-call | flops 3000000000 | bytes 2000000 | tf_op jit(solution)/shard_map/attend/pallas_call | solution.py:87
  52.0 3.7 %collective-permute-start = (bf16[128,128]{1,0:T(8,128)(2,1)S(1)}, bf16[128,128]{1,0:T(8,128)(2,1)S(1)}, u32[]{:S(2)}, u32[]{:S(2)}) collective-permute-start(bf16[128,128]{1,0:T(8,128)(2,1)S(1)} %get-tuple-element.20), channel_id=1, source_target_pairs={{0,4},{4,8},{8,12},{12,16},{16,20},{20,24},{24,28},{1,5},{5,9},{9,... | collective-permute-start | bytes 98312 | tf_op jit(solution)/shard_map/ppermute | solution.py:21
  55.7 2.4 %experts.6.refs_0_ = bf16[256,2048]{1,0:T(8,128)(2,1)S(1)} custom-call(s32[4]{0:T(128)S(1)} %pad_add_fusion.place_ref, bf16[64,2176]{1,0:T(8,128)(2,1)S(1)} %constant_dynamic-update-slice_fusion.2.refs_0_, bf16[64,2176]{1,0:T(8,128)(2,1)S(1)} %collective-permute-done.24.refs_1_, bf16[64,2176]{1,0:T(8,128)(2,1)S(1)} %collective-permute-done.25.refs_2_, ...), custom_call_target="tpu_custom_call" | custom-call | flops 1792000000 | bytes 15000000 | tf_op jit(solution)/shard_map/experts/pallas_call | solution.py:256
  58.1 2.4 %experts.4.refs_0_ = bf16[256,2048]{1,0:T(8,128)(2,1)S(1)} custom-call(s32[4]{0:T(128)S(1)} %pad_add_fusion.place_ref, bf16[64,2176]{1,0:T(8,128)(2,1)S(1)} %constant_dynamic-update-slice_fusion.refs_0_, bf16[64,2176]{1,0:T(8,128)(2,1)S(1)} %collective-permute-done.8.refs_1_, bf16[64,2176]{1,0:T(8,128)(2,1)S(1)} %collective-permute-done.9.refs_2_, ...), custom_call_target="tpu_custom_call" | custom-call | flops 1792000000 | bytes 15000000 | tf_op jit(solution)/shard_map/experts/pallas_call | solution.py:256
  60.7 2.4 %collective-permute-start.34 = (bf16[32,2048]{1,0:T(8,128)(2,1)S(1)}, bf16[32,2048]{1,0:T(8,128)(2,1)S(1)}, u32[]{:S(2)}, u32[]{:S(2)}) collective-permute-start(bf16[32,2048]{1,0:T(8,128)(2,1)S(1)} %get-tuple-element.31), channel_id=1, source_target_pairs={{0,4},{4,0},{8,12},{12,8},{16,20},{20,16},{24,28},{28,24},{1,5},{5... | collective-permute-start | bytes 393224 | tf_op jit(solution)/shard_map/ppermute | solution.py:25
  63.1 2.0 %collective-permute-start.35 = (bf16[32,2048]{1,0:T(8,128)(2,1)S(1)}, bf16[32,2048]{1,0:T(8,128)(2,1)S(1)}, u32[]{:S(2)}, u32[]{:S(2)}) collective-permute-start(bf16[32,2048]{1,0:T(8,128)(2,1)S(1)} %get-tuple-element.32), channel_id=1, source_target_pairs={{0,2},{1,3},{2,0},{3,1},{4,6},{5,7},{6,4},{7,5},{8,10},{9,11},{10,... | collective-permute-start | bytes 393224 | tf_op jit(solution)/shard_map/ppermute | solution.py:25
  65.3 2.3 %attend.2.refs_0_ = bf16[512,256]{1,0:T(8,128)(2,1)S(1)} custom-call(s32[4]{0:T(128)S(1)} %pad_add_fusion.place_ref, bf16[1024,256]{1,0:T(8,128)(2,1)S(1)} %copy-done.5, bf16[64,1024]{1,0:T(8,128)(2,1)S(1)} %bitcast.12, bf16[64,1024]{1,0:T(8,128)(2,1)S(1)} %bitcast.15, f32[4]{0:T(128)S(1)} %copy-done.8, bf16[128,128]{1,0:T(8,128)(2,1)S(1)} %collective-permute-done.refs_0_), custom_call_target="tpu_custom_call" | custom-call | flops 3000000000 | bytes 2000000 | tf_op jit(solution)/shard_map/attend/pallas_call | solution.py:87
  67.6 2.1 %collective-permute-start.2 = (bf16[512,256]{1,0:T(8,128)(2,1)S(1)}, bf16[512,256]{1,0:T(8,128)(2,1)S(1)}, u32[]{:S(2)}, u32[]{:S(2)}) collective-permute-start(bf16[512,256]{1,0:T(8,128)(2,1)S(1)} %attend.2.refs_0_), channel_id=1, source_target_pairs={{0,2},{1,3},{2,0},{3,1},{4,6},{5,7},{6,4},{7,5},{8,10},{9,11},{10,... | collective-permute-start | bytes 786440 | tf_op jit(solution)/shard_map/ppermute | solution.py:25
  72.4 2.1 %collective-permute-start.20 = (bf16[64,2048]{1,0:T(8,128)(2,1)S(1)}, bf16[64,2048]{1,0:T(8,128)(2,1)S(1)}, u32[]{:S(2)}, u32[]{:S(2)}) collective-permute-start(bf16[64,2048]{1,0:T(8,128)(2,1)S(1)} %get-tuple-element.26), channel_id=1, source_target_pairs={{0,2},{1,3},{2,0},{3,1},{4,6},{5,7},{6,4},{7,5},{8,10},{9,11},{10,... | collective-permute-start | bytes 786440 | tf_op jit(solution)/shard_map/ppermute | solution.py:25
  74.5 3.4 %collective-permute-done.2.refs_2_ = bf16[512,256]{1,0:T(8,128)(2,1)S(1)} collective-permute-done((bf16[512,256]{1,0:T(8,128)(2,1)S(1)}, bf16[512,256]{1,0:T(8,128)(2,1)S(1)}, u32[]{:S(2)}, u32[]{:S(2)}) %collective-permute-start.2) | collective-permute-done | bytes 262176 | tf_op jit(solution)/shard_map/ppermute | solution.py:25
  77.9 5.6 %collective-permute-done.36.refs_2_ = bf16[64,2048]{1,0:T(8,128)(2,1)S(1)} collective-permute-done((bf16[64,2048]{1,0:T(8,128)(2,1)S(1)}, bf16[64,2048]{1,0:T(8,128)(2,1)S(1)}, u32[]{:S(2)}, u32[]{:S(2)}) %collective-permute-start.36) | collective-permute-done | bytes 262176 | tf_op jit(solution)/shard_map/ppermute | solution.py:25
  84.0 4.0 %collective-permute-done.20.refs_2_ = bf16[64,2048]{1,0:T(8,128)(2,1)S(1)} collective-permute-done((bf16[64,2048]{1,0:T(8,128)(2,1)S(1)}, bf16[64,2048]{1,0:T(8,128)(2,1)S(1)}, u32[]{:S(2)}, u32[]{:S(2)}) %collective-permute-start.20) | collective-permute-done | bytes 262176 | tf_op jit(solution)/shard_map/ppermute | solution.py:25
  90.2 2.3 %collective-permute-start.40 = (bf16[32,2048]{1,0:T(8,128)(2,1)S(1)}, bf16[32,2048]{1,0:T(8,128)(2,1)S(1)}, u32[]{:S(2)}, u32[]{:S(2)}) collective-permute-start(bf16[32,2048]{1,0:T(8,128)(2,1)S(1)} %get-tuple-element.37), channel_id=1, source_target_pairs={{0,24},{4,28},{8,16},{12,20},{16,8},{20,12},{24,0},{28,4},{1,25},{... | collective-permute-start | bytes 393224 | tf_op jit(solution)/shard_map/ppermute | solution.py:25
  96.5 3.0 %collective-permute-done.40.refs_3_ = bf16[32,2048]{1,0:T(8,128)(2,1)S(1)} collective-permute-done((bf16[32,2048]{1,0:T(8,128)(2,1)S(1)}, bf16[32,2048]{1,0:T(8,128)(2,1)S(1)}, u32[]{:S(2)}, u32[]{:S(2)}) %collective-permute-start.40) | collective-permute-done | bytes 131104 | tf_op jit(solution)/shard_map/ppermute | solution.py:25
  99.5 4.7 %collective-permute-done.39.refs_2_ = bf16[32,2048]{1,0:T(8,128)(2,1)S(1)} collective-permute-done((bf16[32,2048]{1,0:T(8,128)(2,1)S(1)}, bf16[32,2048]{1,0:T(8,128)(2,1)S(1)}, u32[]{:S(2)}, u32[]{:S(2)}) %collective-permute-start.39) | collective-permute-done | bytes 131104 | tf_op jit(solution)/shard_map/ppermute | solution.py:25
  (101 shorter events, 30.6 us)
Async XLA Ops:
  6.6 10.1 %collective-permute-start.23 = (bf16[32,2176]{1,0:T(8,128)(2,1)S(1)}, bf16[32,2176]{1,0:T(8,128)(2,1)S(1)}, u32[]{:S(2)}, u32[]{:S(2)}) collective-permute-start(bf16[32,2176]{1,0:T(8,128)(2,1)S(1)} %get-tuple-element.30), channel_id=1, source_target_pairs={{0,24},{4,28},{8,16},{12,20},{16,8},{20,12},{24,0},{28,4},{1,25},{... | collective-permute-start | bytes 417800 | tf_op jit(solution)/shard_map/ppermute | solution.py:25
  9.1 12.5 %collective-permute-start.7 = (bf16[32,2176]{1,0:T(8,128)(2,1)S(1)}, bf16[32,2176]{1,0:T(8,128)(2,1)S(1)}, u32[]{:S(2)}, u32[]{:S(2)}) collective-permute-start(bf16[32,2176]{1,0:T(8,128)(2,1)S(1)} %get-tuple-element.23), channel_id=1, source_target_pairs={{0,16},{4,20},{8,24},{12,28},{16,0},{20,4},{24,8},{28,12},{1,17},{... | collective-permute-start | bytes 417800 | tf_op jit(solution)/shard_map/ppermute | solution.py:25
  21.6 9.2 %collective-permute-start.8 = (bf16[64,2176]{1,0:T(8,128)(2,1)S(1)}, bf16[64,2176]{1,0:T(8,128)(2,1)S(1)}, u32[]{:S(2)}, u32[]{:S(2)}) collective-permute-start(bf16[64,2176]{1,0:T(8,128)(2,1)S(1)} %constant_dynamic-update-slice_fusion.refs_0_), channel_id=1, source_target_pairs={{0,2},{1,3},{2,0},{3,1},{4,6},{5,7},{6,4},{7,5},{8,10},{9,11},{10,... | collective-permute-start | bytes 835592 | tf_op jit(solution)/shard_map/ppermute | solution.py:25
  23.2 9.2 %collective-permute-start.28 = (bf16[64,2176]{1,0:T(8,128)(2,1)S(1)}, bf16[64,2176]{1,0:T(8,128)(2,1)S(1)}, u32[]{:S(2)}, u32[]{:S(2)}) collective-permute-start(bf16[64,2176]{1,0:T(8,128)(2,1)S(1)} %constant_dynamic-update-slice_fusion.2.refs_0_), channel_id=1, source_target_pairs={{0,1},{1,0},{2,3},{3,2},{4,5},{5,4},{6,7},{7,6},{8,9},{9,8},{10,11... | collective-permute-start | bytes 835592 | tf_op jit(solution)/shard_map/ppermute | solution.py:25
  23.2 9.5 %collective-permute-start.9 = (bf16[64,2176]{1,0:T(8,128)(2,1)S(1)}, bf16[64,2176]{1,0:T(8,128)(2,1)S(1)}, u32[]{:S(2)}, u32[]{:S(2)}) collective-permute-start(bf16[64,2176]{1,0:T(8,128)(2,1)S(1)} %constant_dynamic-update-slice_fusion.refs_0_), channel_id=1, source_target_pairs={{0,4},{4,0},{8,12},{12,8},{16,20},{20,16},{24,28},{28,24},{1,5},{5... | collective-permute-start | bytes 835592 | tf_op jit(solution)/shard_map/ppermute | solution.py:25
  24.7 11.0 %collective-permute-start.26 = (bf16[32,2176]{1,0:T(8,128)(2,1)S(1)}, bf16[32,2176]{1,0:T(8,128)(2,1)S(1)}, u32[]{:S(2)}, u32[]{:S(2)}) collective-permute-start(bf16[32,2176]{1,0:T(8,128)(2,1)S(1)} %slice.18), channel_id=1, source_target_pairs={{0,4},{4,0},{8,12},{12,8},{16,20},{20,16},{24,28},{28,24},{1,5},{5... | collective-permute-start | bytes 417800 | tf_op jit(solution)/shard_map/ppermute | solution.py:25
  25.3 10.9 %collective-permute-start.27 = (bf16[32,2176]{1,0:T(8,128)(2,1)S(1)}, bf16[32,2176]{1,0:T(8,128)(2,1)S(1)}, u32[]{:S(2)}, u32[]{:S(2)}) collective-permute-start(bf16[32,2176]{1,0:T(8,128)(2,1)S(1)} %slice.19), channel_id=1, source_target_pairs={{0,2},{1,3},{2,0},{3,1},{4,6},{5,7},{6,4},{7,5},{8,10},{9,11},{10,... | collective-permute-start | bytes 417800 | tf_op jit(solution)/shard_map/ppermute | solution.py:25
  32.4 8.9 %collective-permute-start.29 = (bf16[64,2176]{1,0:T(8,128)(2,1)S(1)}, bf16[64,2176]{1,0:T(8,128)(2,1)S(1)}, u32[]{:S(2)}, u32[]{:S(2)}) collective-permute-start(bf16[64,2176]{1,0:T(8,128)(2,1)S(1)} %collective-permute-done.24.refs_1_), channel_id=1, source_target_pairs={{0,1},{1,0},{2,3},{3,2},{4,5},{5,4},{6,7},{7,6},{8,9},{9,8},{10,11... | collective-permute-start | bytes 835592 | tf_op jit(solution)/shard_map/ppermute | solution.py:25
  32.7 9.1 %collective-permute-start.30 = (bf16[64,2176]{1,0:T(8,128)(2,1)S(1)}, bf16[64,2176]{1,0:T(8,128)(2,1)S(1)}, u32[]{:S(2)}, u32[]{:S(2)}) collective-permute-start(bf16[64,2176]{1,0:T(8,128)(2,1)S(1)} %collective-permute-done.25.refs_2_), channel_id=1, source_target_pairs={{0,1},{1,0},{2,3},{3,2},{4,5},{5,4},{6,7},{7,6},{8,9},{9,8},{10,11... | collective-permute-start | bytes 835592 | tf_op jit(solution)/shard_map/ppermute | solution.py:25
  45.9 14.7 %collective-permute-start.33 = (bf16[256,2048]{1,0:T(8,128)(2,1)S(1)}, bf16[256,2048]{1,0:T(8,128)(2,1)S(1)}, u32[]{:S(2)}, u32[]{:S(2)}) collective-permute-start(bf16[256,2048]{1,0:T(8,128)(2,1)S(1)} %experts.7), channel_id=1, source_target_pairs={{0,1},{1,0},{2,3},{3,2},{4,5},{5,4},{6,7},{7,6},{8,9},{9,8},{10,11... | collective-permute-start | bytes 3145736 | tf_op jit(solution)/shard_map/ppermute | solution.py:25
  48.9 16.1 %collective-permute-start.17 = (bf16[256,2048]{1,0:T(8,128)(2,1)S(1)}, bf16[256,2048]{1,0:T(8,128)(2,1)S(1)}, u32[]{:S(2)}, u32[]{:S(2)}) collective-permute-start(bf16[256,2048]{1,0:T(8,128)(2,1)S(1)} %experts.5), channel_id=1, source_target_pairs={{0,1},{1,0},{2,3},{3,2},{4,5},{5,4},{6,7},{7,6},{8,9},{9,8},{10,11... | collective-permute-start | bytes 3145736 | tf_op jit(solution)/shard_map/ppermute | solution.py:25
  51.4 23.1 %collective-permute-start.5 = (bf16[512,256]{1,0:T(8,128)(2,1)S(1)}, bf16[512,256]{1,0:T(8,128)(2,1)S(1)}, u32[]{:S(2)}, u32[]{:S(2)}) collective-permute-start(bf16[512,256]{1,0:T(8,128)(2,1)S(1)} %attend.3.refs_0_), channel_id=1, source_target_pairs={{0,2},{1,3},{2,0},{3,1},{4,6},{5,7},{6,4},{7,5},{8,10},{9,11},{10,... | collective-permute-start | bytes 786440 | tf_op jit(solution)/shard_map/ppermute | solution.py:25
  52.0 13.3 %collective-permute-start = (bf16[128,128]{1,0:T(8,128)(2,1)S(1)}, bf16[128,128]{1,0:T(8,128)(2,1)S(1)}, u32[]{:S(2)}, u32[]{:S(2)}) collective-permute-start(bf16[128,128]{1,0:T(8,128)(2,1)S(1)} %get-tuple-element.20), channel_id=1, source_target_pairs={{0,4},{4,8},{8,12},{12,16},{16,20},{20,24},{24,28},{1,5},{5,9},{9,... | collective-permute-start | bytes 98312 | tf_op jit(solution)/shard_map/ppermute | solution.py:21
  67.6 10.2 %collective-permute-start.2 = (bf16[512,256]{1,0:T(8,128)(2,1)S(1)}, bf16[512,256]{1,0:T(8,128)(2,1)S(1)}, u32[]{:S(2)}, u32[]{:S(2)}) collective-permute-start(bf16[512,256]{1,0:T(8,128)(2,1)S(1)} %attend.2.refs_0_), channel_id=1, source_target_pairs={{0,2},{1,3},{2,0},{3,1},{4,6},{5,7},{6,4},{7,5},{8,10},{9,11},{10,... | collective-permute-start | bytes 786440 | tf_op jit(solution)/shard_map/ppermute | solution.py:25
  69.8 13.6 %collective-permute-start.36 = (bf16[64,2048]{1,0:T(8,128)(2,1)S(1)}, bf16[64,2048]{1,0:T(8,128)(2,1)S(1)}, u32[]{:S(2)}, u32[]{:S(2)}) collective-permute-start(bf16[64,2048]{1,0:T(8,128)(2,1)S(1)} %get-tuple-element.33), channel_id=1, source_target_pairs={{0,2},{1,3},{2,0},{3,1},{4,6},{5,7},{6,4},{7,5},{8,10},{9,11},{10,... | collective-permute-start | bytes 786440 | tf_op jit(solution)/shard_map/ppermute | solution.py:25
  71.7 11.8 %collective-permute-start.37 = (bf16[64,2048]{1,0:T(8,128)(2,1)S(1)}, bf16[64,2048]{1,0:T(8,128)(2,1)S(1)}, u32[]{:S(2)}, u32[]{:S(2)}) collective-permute-start(bf16[64,2048]{1,0:T(8,128)(2,1)S(1)} %get-tuple-element.34), channel_id=1, source_target_pairs={{0,4},{4,0},{8,12},{12,8},{16,20},{20,16},{24,28},{28,24},{1,5},{5... | collective-permute-start | bytes 786440 | tf_op jit(solution)/shard_map/ppermute | solution.py:25
  72.4 15.6 %collective-permute-start.20 = (bf16[64,2048]{1,0:T(8,128)(2,1)S(1)}, bf16[64,2048]{1,0:T(8,128)(2,1)S(1)}, u32[]{:S(2)}, u32[]{:S(2)}) collective-permute-start(bf16[64,2048]{1,0:T(8,128)(2,1)S(1)} %get-tuple-element.26), channel_id=1, source_target_pairs={{0,2},{1,3},{2,0},{3,1},{4,6},{5,7},{6,4},{7,5},{8,10},{9,11},{10,... | collective-permute-start | bytes 786440 | tf_op jit(solution)/shard_map/ppermute | solution.py:25
  74.5 13.7 %collective-permute-start.21 = (bf16[64,2048]{1,0:T(8,128)(2,1)S(1)}, bf16[64,2048]{1,0:T(8,128)(2,1)S(1)}, u32[]{:S(2)}, u32[]{:S(2)}) collective-permute-start(bf16[64,2048]{1,0:T(8,128)(2,1)S(1)} %get-tuple-element.27), channel_id=1, source_target_pairs={{0,4},{4,0},{8,12},{12,8},{16,20},{20,16},{24,28},{28,24},{1,5},{5... | collective-permute-start | bytes 786440 | tf_op jit(solution)/shard_map/ppermute | solution.py:25
  77.9 12.3 %collective-permute-start.4 = (bf16[512,256]{1,0:T(8,128)(2,1)S(1)}, bf16[512,256]{1,0:T(8,128)(2,1)S(1)}, u32[]{:S(2)}, u32[]{:S(2)}) collective-permute-start(bf16[512,256]{1,0:T(8,128)(2,1)S(1)} %attend.3.refs_0_), channel_id=1, source_target_pairs={{0,1},{1,0},{2,3},{3,2},{4,5},{5,4},{6,7},{7,6},{8,9},{9,8},{10,11... | collective-permute-start | bytes 786440 | tf_op jit(solution)/shard_map/ppermute | solution.py:25
  83.5 9.0 %collective-permute-start.6 = (bf16[512,256]{1,0:T(8,128)(2,1)S(1)}, bf16[512,256]{1,0:T(8,128)(2,1)S(1)}, u32[]{:S(2)}, u32[]{:S(2)}) collective-permute-start(bf16[512,256]{1,0:T(8,128)(2,1)S(1)} %collective-permute-done.5.refs_2_), channel_id=1, source_target_pairs={{0,1},{1,0},{2,3},{3,2},{4,5},{5,4},{6,7},{7,6},{8,9},{9,8},{10,11... | collective-permute-start | bytes 786440 | tf_op jit(solution)/shard_map/ppermute | solution.py:25
  83.5 11.0 %collective-permute-start.1 = (bf16[512,256]{1,0:T(8,128)(2,1)S(1)}, bf16[512,256]{1,0:T(8,128)(2,1)S(1)}, u32[]{:S(2)}, u32[]{:S(2)}) collective-permute-start(bf16[512,256]{1,0:T(8,128)(2,1)S(1)} %attend.2.refs_0_), channel_id=1, source_target_pairs={{0,1},{1,0},{2,3},{3,2},{4,5},{5,4},{6,7},{7,6},{8,9},{9,8},{10,11... | collective-permute-start | bytes 786440 | tf_op jit(solution)/shard_map/ppermute | solution.py:25
  88.2 8.3 %collective-permute-start.38 = (bf16[32,2048]{1,0:T(8,128)(2,1)S(1)}, bf16[32,2048]{1,0:T(8,128)(2,1)S(1)}, u32[]{:S(2)}, u32[]{:S(2)}) collective-permute-start(bf16[32,2048]{1,0:T(8,128)(2,1)S(1)} %get-tuple-element.35), channel_id=1, source_target_pairs={{0,8},{4,12},{8,0},{12,4},{16,24},{20,28},{24,16},{28,20},{1,9},{5... | collective-permute-start | bytes 393224 | tf_op jit(solution)/shard_map/ppermute | solution.py:25
  90.2 9.3 %collective-permute-start.40 = (bf16[32,2048]{1,0:T(8,128)(2,1)S(1)}, bf16[32,2048]{1,0:T(8,128)(2,1)S(1)}, u32[]{:S(2)}, u32[]{:S(2)}) collective-permute-start(bf16[32,2048]{1,0:T(8,128)(2,1)S(1)} %get-tuple-element.37), channel_id=1, source_target_pairs={{0,24},{4,28},{8,16},{12,20},{16,8},{20,12},{24,0},{28,4},{1,25},{... | collective-permute-start | bytes 393224 | tf_op jit(solution)/shard_map/ppermute | solution.py:25
  92.5 11.8 %collective-permute-start.39 = (bf16[32,2048]{1,0:T(8,128)(2,1)S(1)}, bf16[32,2048]{1,0:T(8,128)(2,1)S(1)}, u32[]{:S(2)}, u32[]{:S(2)}) collective-permute-start(bf16[32,2048]{1,0:T(8,128)(2,1)S(1)} %get-tuple-element.36), channel_id=1, source_target_pairs={{0,16},{4,20},{8,24},{12,28},{16,0},{20,4},{24,8},{28,12},{1,17},{... | collective-permute-start | bytes 393224 | tf_op jit(solution)/shard_map/ppermute | solution.py:25
  (26 other events, 221.9 us)

commit v3 on v2

--- a/solution.py
+++ b/solution.py
@@ -265,19 +265,33 @@
     )(place, *in_vmem(*pieces, expert_gate, expert_up, expert_down))
 
 
-def combine_kernel(order_ref, *refs):
-    *pieces, out_ref = refs
+def combine_kernel(order_ref, *refs, steps):
+    *pieces, out_ref, tile_ref, sems = refs
     rows = jnp.concatenate([piece[...] for piece in pieces], axis=0)
-    out_ref[...] = dot_f32(order_ref[...], rows, (0, 0)).astype(jnp.bfloat16)
+    width = rows.shape[1] // steps
+    copies = []
+    for i in range(steps):
+        tile_ref[i] = dot_f32(order_ref[...], rows[:, i * width : (i + 1) * width], (0, 0)).astype(jnp.bfloat16)
+        copies.append(
+            pltpu.make_async_copy(tile_ref.at[i], out_ref.at[:, pl.ds(i * width, width)], sems.at[i])
+        )
+        copies[-1].start()
+    for copy in copies:
+        copy.wait()
 
 
 def combine(order, pieces):
     vmem = pl.BlockSpec(memory_space=pltpu.VMEM)
+    rows, width, steps = order.shape[0], pieces[0].shape[1], 4
     return pl.pallas_call(
-        combine_kernel,
-        out_shape=jax.ShapeDtypeStruct((order.shape[0], pieces[0].shape[1]), jnp.bfloat16),
+        functools.partial(combine_kernel, steps=steps),
+        out_shape=pltpu.HBM((rows, width), jnp.bfloat16),
         in_specs=[vmem] * (len(pieces) + 1),
-        out_specs=vmem,
+        out_specs=pl.BlockSpec(memory_space=pl.ANY),
+        scratch_shapes=[
+            pltpu.VMEM((steps, rows, width // steps), jnp.bfloat16),
+            pltpu.SemaphoreType.DMA((steps,)),
+        ],
         compiler_params=pltpu.CompilerParams(vmem_limit_bytes=8 << 20),
         name="combine",
     )(*in_vmem(order, *pieces))
@@ -319,33 +333,34 @@
     half = step // 2
     other = flipped(there, "tp", core_bit)
     both = lambda at: ((0, at), (1, at))
-    far_low, far_high = sums(
-        (((0, half, both(3 * step)),), ((0, half, both(3 * step + half)),)), here, other
-    )
-    far_low = flipped(far_low, "ep", 1)
-    far_high = flipped(far_high, "tp", side_bit)
-    across, along = sums(
+    first_side, first_along = sums(
         (
-            ((0, half, both(step) + ((2, 0),)), (half, half, both(step + half))),
-            ((0, half, both(2 * step)), (half, half, both(2 * step + half) + ((3, 0),))),
+            ((0, half, both(3 * step + half)), (half, half, both(step + half))),
+            ((0, half, both(3 * step)), (half, half, both(2 * step))),
         ),
         here,
         other,
-        far_low,
-        far_high,
     )
-    across = flipped(across, "tp", side_bit)
-    along = flipped(along, "ep", 1)
-    piece = step // chunks
-    return sums(
-        tuple(
-            ((0, piece, both(i * piece) + ((2, i * piece), (3, i * piece))),) for i in range(chunks)
-        ),
+    first_side = flipped(first_side, "tp", side_bit)
+    first_along = flipped(first_along, "ep", 1)
+    second_side, second_along = sums(
+        (((0, half, both(step) + ((2, 0),)),), ((0, half, both(2 * step + half) + ((3, 0),)),)),
         here,
         other,
-        across,
-        along,
+        first_along,
+        first_side,
     )
+    second_side = flipped(second_side, "tp", side_bit)
+    second_along = flipped(second_along, "ep", 1)
+    piece = step // chunks
+    plan = []
+    for at in range(0, step, piece):
+        if at < half:
+            far = ((2, at), (5, half + at))
+        else:
+            far = ((4, at), (3, at - half))
+        plan.append(((0, piece, both(at) + far),))
+    return sums(tuple(plan), here, other, second_side, second_along, first_side, first_along)
 
 
 def per_device(
@@ -432,7 +447,8 @@
         totals = reduce_plane(here, there, core_bit, side_bit, len(chunk))
         for k, total in zip(chunk, totals):
             returned[k] = flipped(total, "ep", k * members) if k else total
-    return (mixer_out, combine(order, [returned[k] for k in range(groups)]))
+    moe_out = combine(order, [returned[k] for k in range(groups)])
+    return (mixer_out, moe_out)
 
 
 def normalize(rows_in, gain):

time: 106 us -> 108 us (1.019)
  starting transfers between devices: 37.5 us -> 38.9 us
  waiting for transfers between devices: 42.2 us -> 43.5 us
    ppermute x40, starting transfers between devices: 33.8 us -> 35.2 us  [flipped(): lax.ppermute(value, axis, [(i, i ^ bits) for i in range(lax.axis_size(axi...]
    ppermute x40, waiting for transfers between devices: 42.2 us -> 43.5 us  [flipped(): lax.ppermute(value, axis, [(i, i ^ bits) for i in range(lax.axis_size(axi...]
  transfers between devices with their start and end apart: 41 -> 41, of which waited for: 14 -> 17; matrix products, arithmetic and copies ran while one was open for 0% -> 0% of each run, Pallas kernels for 18% -> 18%
where the time goes in v3:
time: 108 us
  waiting for transfers between devices  43.5 us (40%)
  starting transfers between devices  38.9 us (36%)
  Pallas kernels  22.8 us (21%)
  local copies, waits for them, and re-layouts  1.73 us (2%)
  between operations  1.08 us (1%)
    ppermute x40, waiting for transfers between devices, flipped(): lax.ppermute(value, axis, [(i, i ^ bits) for i in range(lax.axis_size(axi...  43.5 us
    ppermute x40, starting transfers between devices, flipped(): lax.ppermute(value, axis, [(i, i ^ bits) for i in range(lax.axis_size(axi...  35.2 us
    pallas_call x4, Pallas kernels, run_experts(): pl.pallas_call(functools.partial(experts_kernel, sizes=sizes, size=size),...  9.76 us
    pallas_call x2, Pallas kernels, attend(): pl.pallas_call(functools.partial(attention_kernel, first=first, kv_local=...  4.56 us
    pallas_call x2, Pallas kernels, project(): pl.pallas_call(functools.partial(projection_kernel, count=len(pieces), fi...  3.95 us
    ppermute x1, starting transfers between devices, shifted(): lax.ppermute(value, axis, [(source, source + steps) for source in range(l...  3.72 us
    pallas_call x1, Pallas kernels, dispatch(): pl.pallas_call(dispatch_kernel, grid_spec=pltpu.PrefetchScalarGridSpec(nu...  2.79 us
  transfers between devices with their start and end apart: 41, of which 17 were waited for; matrix products, arithmetic and copies ran while one was open for 0% of the time, Pallas kernels for 18%

profile of v3, /device:TPU:0, one launch (start us, length us, event | category | flops | bytes accessed | tf_op | source)
XLA Modules:
  0.0 108.1 jit_solution(9827427580515875878)
XLA Ops:
  0.7 2.8 %dispatch.1 = (bf16[128,128]{1,0:T(8,128)(2,1)S(1)}, bf16[128,128]{1,0:T(8,128)(2,1)S(1)}, bf16[32,2176]{1,0:T(8,128)(2,1)S(1)}, bf16[32,2176]{1,0:T(8,128)(2,1)...) custom-call(s32[4]{0:T(128)S(1)} %pad_add_fusion.place_ref, bf16[512,2048]{1,0:T(8,128)(2,1)} %tokens_ref.1, ...), custom_call_target="tpu_custom_call" | custom-call | flops 1000000000 | bytes 2000000 | tf_op jit(solution)/shard_map/dispatch/pallas_call | solution.py:199
  3.5 3.1 %collective-permute-start.22 = (bf16[32,2176]{1,0:T(8,128)(2,1)S(1)}, bf16[32,2176]{1,0:T(8,128)(2,1)S(1)}, u32[]{:S(2)}, u32[]{:S(2)}) collective-permute-start(bf16[32,2176]{1,0:T(8,128)(2,1)S(1)} %get-tuple-element.29), channel_id=1, source_target_pairs={{0,8},{4,12},{8,0},{12,4},{16,24},{20,28},{24,16},{28,20},{1,9},{5... | collective-permute-start | bytes 417800 | tf_op jit(solution)/shard_map/ppermute | solution.py:25
  6.6 2.5 %collective-permute-start.23 = (bf16[32,2176]{1,0:T(8,128)(2,1)S(1)}, bf16[32,2176]{1,0:T(8,128)(2,1)S(1)}, u32[]{:S(2)}, u32[]{:S(2)}) collective-permute-start(bf16[32,2176]{1,0:T(8,128)(2,1)S(1)} %get-tuple-element.30), channel_id=1, source_target_pairs={{0,24},{4,28},{8,16},{12,20},{16,8},{20,12},{24,0},{28,4},{1,25},{... | collective-permute-start | bytes 417800 | tf_op jit(solution)/shard_map/ppermute | solution.py:25
  10.4 6.3 %collective-permute-done.23 = bf16[32,2176]{1,0:T(8,128)(2,1)S(1)} collective-permute-done((bf16[32,2176]{1,0:T(8,128)(2,1)S(1)}, bf16[32,2176]{1,0:T(8,128)(2,1)S(1)}, u32[]{:S(2)}, u32[]{:S(2)}) %collective-permute-start.23) | collective-permute-done | bytes 139296 | tf_op jit(solution)/shard_map/ppermute | solution.py:25
  26.5 4.3 %collective-permute-done.8.refs_1_ = bf16[64,2176]{1,0:T(8,128)(2,1)S(1)} collective-permute-done((bf16[64,2176]{1,0:T(8,128)(2,1)S(1)}, bf16[64,2176]{1,0:T(8,128)(2,1)S(1)}, u32[]{:S(2)}, u32[]{:S(2)}) %collective-permute-start.8) | collective-permute-done | bytes 278560 | tf_op jit(solution)/shard_map/ppermute | solution.py:25
  32.9 2.7 %collective-permute-done.26.refs_3_ = bf16[32,2176]{1,0:T(8,128)(2,1)S(1)} collective-permute-done((bf16[32,2176]{1,0:T(8,128)(2,1)S(1)}, bf16[32,2176]{1,0:T(8,128)(2,1)S(1)}, u32[]{:S(2)}, u32[]{:S(2)}) %collective-permute-start.26) | collective-permute-done | bytes 139296 | tf_op jit(solution)/shard_map/ppermute | solution.py:25
  38.2 2.5 %collective-permute-done.11.refs_4_ = bf16[32,2176]{1,0:T(8,128)(2,1)S(1)} collective-permute-done((bf16[32,2176]{1,0:T(8,128)(2,1)S(1)}, bf16[32,2176]{1,0:T(8,128)(2,1)S(1)}, u32[]{:S(2)}, u32[]{:S(2)}) %collective-permute-start.11) | collective-permute-done | bytes 139296 | tf_op jit(solution)/shard_map/ppermute | solution.py:25
  43.4 2.4 %experts.7 = bf16[256,2048]{1,0:T(8,128)(2,1)S(1)} custom-call(s32[4]{0:T(128)S(1)} %pad_add_fusion.place_ref, bf16[64,2176]{1,0:T(8,128)(2,1)S(1)} %collective-permute-done.28.refs_0_, bf16[64,2176]{1,0:T(8,128)(2,1)S(1)} %collective-permute-done.29.refs_1_, bf16[64,2176]{1,0:T(8,128)(2,1)S(1)} %collective-permute-done.30.refs_2_, ...), custom_call_target="tpu_custom_call" | custom-call | flops 1792000000 | bytes 15000000 | tf_op jit(solution)/shard_map/experts/pallas_call | solution.py:256
  46.5 2.4 %experts.5 = bf16[256,2048]{1,0:T(8,128)(2,1)S(1)} custom-call(s32[4]{0:T(128)S(1)} %pad_add_fusion.place_ref, bf16[64,2176]{1,0:T(8,128)(2,1)S(1)} %collective-permute-done.12.refs_0_, bf16[64,2176]{1,0:T(8,128)(2,1)S(1)} %collective-permute-done.13.refs_1_, bf16[64,2176]{1,0:T(8,128)(2,1)S(1)} %collective-permute-done.14.refs_2_, ...), custom_call_target="tpu_custom_call" | custom-call | flops 1792000000 | bytes 15000000 | tf_op jit(solution)/shard_map/experts/pallas_call | solution.py:256
  49.1 2.3 %attend.3.refs_0_ = bf16[512,256]{1,0:T(8,128)(2,1)S(1)} custom-call(s32[4]{0:T(128)S(1)} %pad_add_fusion.place_ref, bf16[1024,256]{1,0:T(8,128)(2,1)S(1)} %copy-done.5, bf16[64,1024]{1,0:T(8,128)(2,1)S(1)} %bitcast.11, bf16[64,1024]{1,0:T(8,128)(2,1)S(1)} %bitcast.14, f32[4]{0:T(128)S(1)} %copy-done.8), custom_call_target="tpu_custom_call" | custom-call | flops 3000000000 | bytes 2000000 | tf_op jit(solution)/shard_map/attend/pallas_call | solution.py:87
  52.0 3.7 %collective-permute-start = (bf16[128,128]{1,0:T(8,128)(2,1)S(1)}, bf16[128,128]{1,0:T(8,128)(2,1)S(1)}, u32[]{:S(2)}, u32[]{:S(2)}) collective-permute-start(bf16[128,128]{1,0:T(8,128)(2,1)S(1)} %get-tuple-element.20), channel_id=1, source_target_pairs={{0,4},{4,8},{8,12},{12,16},{16,20},{20,24},{24,28},{1,5},{5,9},{9,... | collective-permute-start | bytes 98312 | tf_op jit(solution)/shard_map/ppermute | solution.py:21
  55.7 2.4 %experts.6.refs_0_ = bf16[256,2048]{1,0:T(8,128)(2,1)S(1)} custom-call(s32[4]{0:T(128)S(1)} %pad_add_fusion.place_ref, bf16[64,2176]{1,0:T(8,128)(2,1)S(1)} %constant_dynamic-update-slice_fusion.2.refs_0_, bf16[64,2176]{1,0:T(8,128)(2,1)S(1)} %collective-permute-done.24.refs_1_, bf16[64,2176]{1,0:T(8,128)(2,1)S(1)} %collective-permute-done.25.refs_2_, ...), custom_call_target="tpu_custom_call" | custom-call | flops 1792000000 | bytes 15000000 | tf_op jit(solution)/shard_map/experts/pallas_call | solution.py:256
  58.1 2.4 %experts.4.refs_0_ = bf16[256,2048]{1,0:T(8,128)(2,1)S(1)} custom-call(s32[4]{0:T(128)S(1)} %pad_add_fusion.place_ref, bf16[64,2176]{1,0:T(8,128)(2,1)S(1)} %constant_dynamic-update-slice_fusion.refs_0_, bf16[64,2176]{1,0:T(8,128)(2,1)S(1)} %collective-permute-done.8.refs_1_, bf16[64,2176]{1,0:T(8,128)(2,1)S(1)} %collective-permute-done.9.refs_2_, ...), custom_call_target="tpu_custom_call" | custom-call | flops 1792000000 | bytes 15000000 | tf_op jit(solution)/shard_map/experts/pallas_call | solution.py:256
  60.7 2.4 %collective-permute-start.34 = (bf16[64,2048]{1,0:T(8,128)(2,1)S(1)}, bf16[64,2048]{1,0:T(8,128)(2,1)S(1)}, u32[]{:S(2)}, u32[]{:S(2)}) collective-permute-start(bf16[64,2048]{1,0:T(8,128)(2,1)S(1)} %get-tuple-element.31), channel_id=1, source_target_pairs={{0,4},{4,0},{8,12},{12,8},{16,20},{20,16},{24,28},{28,24},{1,5},{5... | collective-permute-start | bytes 786440 | tf_op jit(solution)/shard_map/ppermute | solution.py:25
  63.1 2.0 %collective-permute-start.35 = (bf16[64,2048]{1,0:T(8,128)(2,1)S(1)}, bf16[64,2048]{1,0:T(8,128)(2,1)S(1)}, u32[]{:S(2)}, u32[]{:S(2)}) collective-permute-start(bf16[64,2048]{1,0:T(8,128)(2,1)S(1)} %get-tuple-element.32), channel_id=1, source_target_pairs={{0,2},{1,3},{2,0},{3,1},{4,6},{5,7},{6,4},{7,5},{8,10},{9,11},{10,... | collective-permute-start | bytes 786440 | tf_op jit(solution)/shard_map/ppermute | solution.py:25
  65.4 2.3 %attend.2.refs_0_ = bf16[512,256]{1,0:T(8,128)(2,1)S(1)} custom-call(s32[4]{0:T(128)S(1)} %pad_add_fusion.place_ref, bf16[1024,256]{1,0:T(8,128)(2,1)S(1)} %copy-done.5, bf16[64,1024]{1,0:T(8,128)(2,1)S(1)} %bitcast.12, bf16[64,1024]{1,0:T(8,128)(2,1)S(1)} %bitcast.15, f32[4]{0:T(128)S(1)} %copy-done.8, bf16[128,128]{1,0:T(8,128)(2,1)S(1)} %collective-permute-done.refs_0_), custom_call_target="tpu_custom_call" | custom-call | flops 3000000000 | bytes 2000000 | tf_op jit(solution)/shard_map/attend/pallas_call | solution.py:87
  67.7 2.6 %collective-permute-done.34.refs_2_.refs_5_ = bf16[64,2048]{1,0:T(8,128)(2,1)S(1)} collective-permute-done((bf16[64,2048]{1,0:T(8,128)(2,1)S(1)}, bf16[64,2048]{1,0:T(8,128)(2,1)S(1)}, u32[]{:S(2)}, u32[]{:S(2)}) %collective-permute-start.34) | collective-permute-done | bytes 262176 | tf_op jit(solution)/shard_map/ppermute | solution.py:25
  70.3 2.0 %collective-permute-start.2 = (bf16[512,256]{1,0:T(8,128)(2,1)S(1)}, bf16[512,256]{1,0:T(8,128)(2,1)S(1)}, u32[]{:S(2)}, u32[]{:S(2)}) collective-permute-start(bf16[512,256]{1,0:T(8,128)(2,1)S(1)} %attend.2.refs_0_), channel_id=1, source_target_pairs={{0,2},{1,3},{2,0},{3,1},{4,6},{5,7},{6,4},{7,5},{8,10},{9,11},{10,... | collective-permute-start | bytes 786440 | tf_op jit(solution)/shard_map/ppermute | solution.py:25
  72.4 2.1 %collective-permute-start.36 = (bf16[32,2048]{1,0:T(8,128)(2,1)S(1)}, bf16[32,2048]{1,0:T(8,128)(2,1)S(1)}, u32[]{:S(2)}, u32[]{:S(2)}) collective-permute-start(bf16[32,2048]{1,0:T(8,128)(2,1)S(1)} %get-tuple-element.33), channel_id=1, source_target_pairs={{0,2},{1,3},{2,0},{3,1},{4,6},{5,7},{6,4},{7,5},{8,10},{9,11},{10,... | collective-permute-start | bytes 393224 | tf_op jit(solution)/shard_map/ppermute | solution.py:25
  78.0 2.1 %collective-permute-start.20 = (bf16[32,2048]{1,0:T(8,128)(2,1)S(1)}, bf16[32,2048]{1,0:T(8,128)(2,1)S(1)}, u32[]{:S(2)}, u32[]{:S(2)}) collective-permute-start(bf16[32,2048]{1,0:T(8,128)(2,1)S(1)} %get-tuple-element.26), channel_id=1, source_target_pairs={{0,2},{1,3},{2,0},{3,1},{4,6},{5,7},{6,4},{7,5},{8,10},{9,11},{10,... | collective-permute-start | bytes 393224 | tf_op jit(solution)/shard_map/ppermute | solution.py:25
  80.1 3.5 %collective-permute-done.2.refs_2_ = bf16[512,256]{1,0:T(8,128)(2,1)S(1)} collective-permute-done((bf16[512,256]{1,0:T(8,128)(2,1)S(1)}, bf16[512,256]{1,0:T(8,128)(2,1)S(1)}, u32[]{:S(2)}, u32[]{:S(2)}) %collective-permute-start.2) | collective-permute-done | bytes 262176 | tf_op jit(solution)/shard_map/ppermute | solution.py:25
  83.5 2.8 %collective-permute-done.36.refs_2_ = bf16[32,2048]{1,0:T(8,128)(2,1)S(1)} collective-permute-done((bf16[32,2048]{1,0:T(8,128)(2,1)S(1)}, bf16[32,2048]{1,0:T(8,128)(2,1)S(1)}, u32[]{:S(2)}, u32[]{:S(2)}) %collective-permute-start.36) | collective-permute-done | bytes 131104 | tf_op jit(solution)/shard_map/ppermute | solution.py:25
  88.6 4.5 %collective-permute-done.21.refs_3_ = bf16[32,2048]{1,0:T(8,128)(2,1)S(1)} collective-permute-done((bf16[32,2048]{1,0:T(8,128)(2,1)S(1)}, bf16[32,2048]{1,0:T(8,128)(2,1)S(1)}, u32[]{:S(2)}, u32[]{:S(2)}) %collective-permute-start.21) | collective-permute-done | bytes 131104 | tf_op jit(solution)/shard_map/ppermute | solution.py:25
  102.7 4.3 %collective-permute-done.39.refs_2_ = bf16[32,2048]{1,0:T(8,128)(2,1)S(1)} collective-permute-done((bf16[32,2048]{1,0:T(8,128)(2,1)S(1)}, bf16[32,2048]{1,0:T(8,128)(2,1)S(1)}, u32[]{:S(2)}, u32[]{:S(2)}) %collective-permute-start.39) | collective-permute-done | bytes 131104 | tf_op jit(solution)/shard_map/ppermute | solution.py:25
  (101 shorter events, 36.7 us)
Async XLA Ops:
  6.6 10.1 %collective-permute-start.23 = (bf16[32,2176]{1,0:T(8,128)(2,1)S(1)}, bf16[32,2176]{1,0:T(8,128)(2,1)S(1)}, u32[]{:S(2)}, u32[]{:S(2)}) collective-permute-start(bf16[32,2176]{1,0:T(8,128)(2,1)S(1)} %get-tuple-element.30), channel_id=1, source_target_pairs={{0,24},{4,28},{8,16},{12,20},{16,8},{20,12},{24,0},{28,4},{1,25},{... | collective-permute-start | bytes 417800 | tf_op jit(solution)/shard_map/ppermute | solution.py:25
  9.1 12.5 %collective-permute-start.7 = (bf16[32,2176]{1,0:T(8,128)(2,1)S(1)}, bf16[32,2176]{1,0:T(8,128)(2,1)S(1)}, u32[]{:S(2)}, u32[]{:S(2)}) collective-permute-start(bf16[32,2176]{1,0:T(8,128)(2,1)S(1)} %get-tuple-element.23), channel_id=1, source_target_pairs={{0,16},{4,20},{8,24},{12,28},{16,0},{20,4},{24,8},{28,12},{1,17},{... | collective-permute-start | bytes 417800 | tf_op jit(solution)/shard_map/ppermute | solution.py:25
  21.6 9.2 %collective-permute-start.8 = (bf16[64,2176]{1,0:T(8,128)(2,1)S(1)}, bf16[64,2176]{1,0:T(8,128)(2,1)S(1)}, u32[]{:S(2)}, u32[]{:S(2)}) collective-permute-start(bf16[64,2176]{1,0:T(8,128)(2,1)S(1)} %constant_dynamic-update-slice_fusion.refs_0_), channel_id=1, source_target_pairs={{0,2},{1,3},{2,0},{3,1},{4,6},{5,7},{6,4},{7,5},{8,10},{9,11},{10,... | collective-permute-start | bytes 835592 | tf_op jit(solution)/shard_map/ppermute | solution.py:25
  23.2 9.2 %collective-permute-start.28 = (bf16[64,2176]{1,0:T(8,128)(2,1)S(1)}, bf16[64,2176]{1,0:T(8,128)(2,1)S(1)}, u32[]{:S(2)}, u32[]{:S(2)}) collective-permute-start(bf16[64,2176]{1,0:T(8,128)(2,1)S(1)} %constant_dynamic-update-slice_fusion.2.refs_0_), channel_id=1, source_target_pairs={{0,1},{1,0},{2,3},{3,2},{4,5},{5,4},{6,7},{7,6},{8,9},{9,8},{10,11... | collective-permute-start | bytes 835592 | tf_op jit(solution)/shard_map/ppermute | solution.py:25
  23.2 9.5 %collective-permute-start.9 = (bf16[64,2176]{1,0:T(8,128)(2,1)S(1)}, bf16[64,2176]{1,0:T(8,128)(2,1)S(1)}, u32[]{:S(2)}, u32[]{:S(2)}) collective-permute-start(bf16[64,2176]{1,0:T(8,128)(2,1)S(1)} %constant_dynamic-update-slice_fusion.refs_0_), channel_id=1, source_target_pairs={{0,4},{4,0},{8,12},{12,8},{16,20},{20,16},{24,28},{28,24},{1,5},{5... | collective-permute-start | bytes 835592 | tf_op jit(solution)/shard_map/ppermute | solution.py:25
  24.7 11.0 %collective-permute-start.26 = (bf16[32,2176]{1,0:T(8,128)(2,1)S(1)}, bf16[32,2176]{1,0:T(8,128)(2,1)S(1)}, u32[]{:S(2)}, u32[]{:S(2)}) collective-permute-start(bf16[32,2176]{1,0:T(8,128)(2,1)S(1)} %slice.18), channel_id=1, source_target_pairs={{0,4},{4,0},{8,12},{12,8},{16,20},{20,16},{24,28},{28,24},{1,5},{5... | collective-permute-start | bytes 417800 | tf_op jit(solution)/shard_map/ppermute | solution.py:25
  25.3 10.9 %collective-permute-start.27 = (bf16[32,2176]{1,0:T(8,128)(2,1)S(1)}, bf16[32,2176]{1,0:T(8,128)(2,1)S(1)}, u32[]{:S(2)}, u32[]{:S(2)}) collective-permute-start(bf16[32,2176]{1,0:T(8,128)(2,1)S(1)} %slice.19), channel_id=1, source_target_pairs={{0,2},{1,3},{2,0},{3,1},{4,6},{5,7},{6,4},{7,5},{8,10},{9,11},{10,... | collective-permute-start | bytes 417800 | tf_op jit(solution)/shard_map/ppermute | solution.py:25
  45.9 14.7 %collective-permute-start.33 = (bf16[256,2048]{1,0:T(8,128)(2,1)S(1)}, bf16[256,2048]{1,0:T(8,128)(2,1)S(1)}, u32[]{:S(2)}, u32[]{:S(2)}) collective-permute-start(bf16[256,2048]{1,0:T(8,128)(2,1)S(1)} %experts.7), channel_id=1, source_target_pairs={{0,1},{1,0},{2,3},{3,2},{4,5},{5,4},{6,7},{7,6},{8,9},{9,8},{10,11... | collective-permute-start | bytes 3145736 | tf_op jit(solution)/shard_map/ppermute | solution.py:25
  48.9 16.2 %collective-permute-start.17 = (bf16[256,2048]{1,0:T(8,128)(2,1)S(1)}, bf16[256,2048]{1,0:T(8,128)(2,1)S(1)}, u32[]{:S(2)}, u32[]{:S(2)}) collective-permute-start(bf16[256,2048]{1,0:T(8,128)(2,1)S(1)} %experts.5), channel_id=1, source_target_pairs={{0,1},{1,0},{2,3},{3,2},{4,5},{5,4},{6,7},{7,6},{8,9},{9,8},{10,11... | collective-permute-start | bytes 3145736 | tf_op jit(solution)/shard_map/ppermute | solution.py:25
  51.4 28.7 %collective-permute-start.5 = (bf16[512,256]{1,0:T(8,128)(2,1)S(1)}, bf16[512,256]{1,0:T(8,128)(2,1)S(1)}, u32[]{:S(2)}, u32[]{:S(2)}) collective-permute-start(bf16[512,256]{1,0:T(8,128)(2,1)S(1)} %attend.3.refs_0_), channel_id=1, source_target_pairs={{0,2},{1,3},{2,0},{3,1},{4,6},{5,7},{6,4},{7,5},{8,10},{9,11},{10,... | collective-permute-start | bytes 786440 | tf_op jit(solution)/shard_map/ppermute | solution.py:25
  52.0 13.4 %collective-permute-start = (bf16[128,128]{1,0:T(8,128)(2,1)S(1)}, bf16[128,128]{1,0:T(8,128)(2,1)S(1)}, u32[]{:S(2)}, u32[]{:S(2)}) collective-permute-start(bf16[128,128]{1,0:T(8,128)(2,1)S(1)} %get-tuple-element.20), channel_id=1, source_target_pairs={{0,4},{4,8},{8,12},{12,16},{16,20},{20,24},{24,28},{1,5},{5,9},{9,... | collective-permute-start | bytes 98312 | tf_op jit(solution)/shard_map/ppermute | solution.py:21
  60.7 9.5 %collective-permute-start.34 = (bf16[64,2048]{1,0:T(8,128)(2,1)S(1)}, bf16[64,2048]{1,0:T(8,128)(2,1)S(1)}, u32[]{:S(2)}, u32[]{:S(2)}) collective-permute-start(bf16[64,2048]{1,0:T(8,128)(2,1)S(1)} %get-tuple-element.31), channel_id=1, source_target_pairs={{0,4},{4,0},{8,12},{12,8},{16,20},{20,16},{24,28},{28,24},{1,5},{5... | collective-permute-start | bytes 786440 | tf_op jit(solution)/shard_map/ppermute | solution.py:25
  63.1 9.2 %collective-permute-start.35 = (bf16[64,2048]{1,0:T(8,128)(2,1)S(1)}, bf16[64,2048]{1,0:T(8,128)(2,1)S(1)}, u32[]{:S(2)}, u32[]{:S(2)}) collective-permute-start(bf16[64,2048]{1,0:T(8,128)(2,1)S(1)} %get-tuple-element.32), channel_id=1, source_target_pairs={{0,2},{1,3},{2,0},{3,1},{4,6},{5,7},{6,4},{7,5},{8,10},{9,11},{10,... | collective-permute-start | bytes 786440 | tf_op jit(solution)/shard_map/ppermute | solution.py:25
  65.2 10.1 %collective-permute-start.18 = (bf16[64,2048]{1,0:T(8,128)(2,1)S(1)}, bf16[64,2048]{1,0:T(8,128)(2,1)S(1)}, u32[]{:S(2)}, u32[]{:S(2)}) collective-permute-start(bf16[64,2048]{1,0:T(8,128)(2,1)S(1)} %get-tuple-element.24), channel_id=1, source_target_pairs={{0,4},{4,0},{8,12},{12,8},{16,20},{20,16},{24,28},{28,24},{1,5},{5... | collective-permute-start | bytes 786440 | tf_op jit(solution)/shard_map/ppermute | solution.py:25
  65.4 12.5 %collective-permute-start.19 = (bf16[64,2048]{1,0:T(8,128)(2,1)S(1)}, bf16[64,2048]{1,0:T(8,128)(2,1)S(1)}, u32[]{:S(2)}, u32[]{:S(2)}) collective-permute-start(bf16[64,2048]{1,0:T(8,128)(2,1)S(1)} %get-tuple-element.25), channel_id=1, source_target_pairs={{0,2},{1,3},{2,0},{3,1},{4,6},{5,7},{6,4},{7,5},{8,10},{9,11},{10,... | collective-permute-start | bytes 786440 | tf_op jit(solution)/shard_map/ppermute | solution.py:25
  70.3 13.3 %collective-permute-start.2 = (bf16[512,256]{1,0:T(8,128)(2,1)S(1)}, bf16[512,256]{1,0:T(8,128)(2,1)S(1)}, u32[]{:S(2)}, u32[]{:S(2)}) collective-permute-start(bf16[512,256]{1,0:T(8,128)(2,1)S(1)} %attend.2.refs_0_), channel_id=1, source_target_pairs={{0,2},{1,3},{2,0},{3,1},{4,6},{5,7},{6,4},{7,5},{8,10},{9,11},{10,... | collective-permute-start | bytes 786440 | tf_op jit(solution)/shard_map/ppermute | solution.py:25
  72.4 13.9 %collective-permute-start.36 = (bf16[32,2048]{1,0:T(8,128)(2,1)S(1)}, bf16[32,2048]{1,0:T(8,128)(2,1)S(1)}, u32[]{:S(2)}, u32[]{:S(2)}) collective-permute-start(bf16[32,2048]{1,0:T(8,128)(2,1)S(1)} %get-tuple-element.33), channel_id=1, source_target_pairs={{0,2},{1,3},{2,0},{3,1},{4,6},{5,7},{6,4},{7,5},{8,10},{9,11},{10,... | collective-permute-start | bytes 393224 | tf_op jit(solution)/shard_map/ppermute | solution.py:25
  75.4 11.0 %collective-permute-start.37 = (bf16[32,2048]{1,0:T(8,128)(2,1)S(1)}, bf16[32,2048]{1,0:T(8,128)(2,1)S(1)}, u32[]{:S(2)}, u32[]{:S(2)}) collective-permute-start(bf16[32,2048]{1,0:T(8,128)(2,1)S(1)} %get-tuple-element.34), channel_id=1, source_target_pairs={{0,4},{4,0},{8,12},{12,8},{16,20},{20,16},{24,28},{28,24},{1,5},{5... | collective-permute-start | bytes 393224 | tf_op jit(solution)/shard_map/ppermute | solution.py:25
  78.0 10.0 %collective-permute-start.20 = (bf16[32,2048]{1,0:T(8,128)(2,1)S(1)}, bf16[32,2048]{1,0:T(8,128)(2,1)S(1)}, u32[]{:S(2)}, u32[]{:S(2)}) collective-permute-start(bf16[32,2048]{1,0:T(8,128)(2,1)S(1)} %get-tuple-element.26), channel_id=1, source_target_pairs={{0,2},{1,3},{2,0},{3,1},{4,6},{5,7},{6,4},{7,5},{8,10},{9,11},{10,... | collective-permute-start | bytes 393224 | tf_op jit(solution)/shard_map/ppermute | solution.py:25
  80.1 14.9 %collective-permute-start.4 = (bf16[512,256]{1,0:T(8,128)(2,1)S(1)}, bf16[512,256]{1,0:T(8,128)(2,1)S(1)}, u32[]{:S(2)}, u32[]{:S(2)}) collective-permute-start(bf16[512,256]{1,0:T(8,128)(2,1)S(1)} %attend.3.refs_0_), channel_id=1, source_target_pairs={{0,1},{1,0},{2,3},{3,2},{4,5},{5,4},{6,7},{7,6},{8,9},{9,8},{10,11... | collective-permute-start | bytes 786440 | tf_op jit(solution)/shard_map/ppermute | solution.py:25
  83.5 13.1 %collective-permute-start.6 = (bf16[512,256]{1,0:T(8,128)(2,1)S(1)}, bf16[512,256]{1,0:T(8,128)(2,1)S(1)}, u32[]{:S(2)}, u32[]{:S(2)}) collective-permute-start(bf16[512,256]{1,0:T(8,128)(2,1)S(1)} %collective-permute-done.5.refs_2_), channel_id=1, source_target_pairs={{0,1},{1,0},{2,3},{3,2},{4,5},{5,4},{6,7},{7,6},{8,9},{9,8},{10,11... | collective-permute-start | bytes 786440 | tf_op jit(solution)/shard_map/ppermute | solution.py:25
  86.3 12.4 %collective-permute-start.1 = (bf16[512,256]{1,0:T(8,128)(2,1)S(1)}, bf16[512,256]{1,0:T(8,128)(2,1)S(1)}, u32[]{:S(2)}, u32[]{:S(2)}) collective-permute-start(bf16[512,256]{1,0:T(8,128)(2,1)S(1)} %attend.2.refs_0_), channel_id=1, source_target_pairs={{0,1},{1,0},{2,3},{3,2},{4,5},{5,4},{6,7},{7,6},{8,9},{9,8},{10,11... | collective-permute-start | bytes 786440 | tf_op jit(solution)/shard_map/ppermute | solution.py:25
  86.4 12.4 %collective-permute-start.3 = (bf16[512,256]{1,0:T(8,128)(2,1)S(1)}, bf16[512,256]{1,0:T(8,128)(2,1)S(1)}, u32[]{:S(2)}, u32[]{:S(2)}) collective-permute-start(bf16[512,256]{1,0:T(8,128)(2,1)S(1)} %collective-permute-done.2.refs_2_), channel_id=1, source_target_pairs={{0,1},{1,0},{2,3},{3,2},{4,5},{5,4},{6,7},{7,6},{8,9},{9,8},{10,11... | collective-permute-start | bytes 786440 | tf_op jit(solution)/shard_map/ppermute | solution.py:25
  96.7 10.3 %collective-permute-start.39 = (bf16[32,2048]{1,0:T(8,128)(2,1)S(1)}, bf16[32,2048]{1,0:T(8,128)(2,1)S(1)}, u32[]{:S(2)}, u32[]{:S(2)}) collective-permute-start(bf16[32,2048]{1,0:T(8,128)(2,1)S(1)} %get-tuple-element.36), channel_id=1, source_target_pairs={{0,16},{4,20},{8,24},{12,28},{16,0},{20,4},{24,8},{28,12},{1,17},{... | collective-permute-start | bytes 393224 | tf_op jit(solution)/shard_map/ppermute | solution.py:25
  (26 other events, 216.9 us)

commit v4 on v3

--- a/solution.py
+++ b/solution.py
@@ -227,7 +227,7 @@
     count = len(sizes)
     pieces = refs[:count]
     gate_ref, up_ref, down_ref, out_ref, rows_ref = refs[count:]
-    exp_local, width, _ = gate_ref.shape
+    exp_local, width, hidden = gate_ref.shape
     at = 0
     for piece, rows in zip(pieces, sizes):
         rows_ref[at : at + rows, :] = piece[...]
@@ -235,16 +235,15 @@
     held = rows_ref[:, :width]
     gates = rows_ref[:, width:].astype(jnp.float32)
     line = lax.broadcasted_iota(jnp.int32, gates.shape, 1)
-    result = None
+    active = []
     for e in range(exp_local):
         own = place_ref[3] * exp_local + e
         gate = jnp.sum(jnp.where((line == own) | (line == own + size), gates, 0.0), axis=1, keepdims=True)
         gate_pre = dot_f32(held, gate_ref[e], (1, 0))
         up_pre = dot_f32(held, up_ref[e], (1, 0))
-        active = (jax.nn.silu(gate_pre) * up_pre * gate).astype(jnp.bfloat16)
-        part = dot_f32(active, down_ref[e], (1, 0))
-        result = part if result is None else result + part
-    out_ref[...] = result.astype(jnp.bfloat16)
+        active.append((jax.nn.silu(gate_pre) * up_pre * gate).astype(jnp.bfloat16))
+    down = down_ref[...].reshape(exp_local * hidden, width)
+    out_ref[...] = dot_f32(jnp.concatenate(active, axis=1), down, (1, 0)).astype(jnp.bfloat16)
 
 
 def run_experts(place, pieces, expert_gate, expert_up, expert_down, size):
@@ -421,7 +420,7 @@
         place, tokens_b, moe_gain, router_group.T, router_expert.T, route_expert.T, k_t, v_t, rows_dev
     )
     halo = shifted(tail, "ep", 1)
-    chunks = ((0, 2), (1, 3)) if groups == 4 else (tuple(range(groups)),)
+    chunks = ((0, 3), (1, 2)) if groups == 4 else (tuple(range(groups)),)
     arrived = [sends[0]] + [flipped(sends[k], "ep", k * members) for k in range(1, groups)]
     middle = blocks // 2
     attended = []

time: 108 us -> 107 us (level)
  starting transfers between devices: 38.9 us -> 34.5 us
  waiting for transfers between devices: 43.5 us -> 46.5 us
    ppermute x40, starting transfers between devices: 35.2 us -> 30.2 us  [flipped(): lax.ppermute(value, axis, [(i, i ^ bits) for i in range(lax.axis_size(axi...]
    ppermute x40, waiting for transfers between devices: 43.5 us -> 46.5 us  [flipped(): lax.ppermute(value, axis, [(i, i ^ bits) for i in range(lax.axis_size(axi...]
where the time goes in v4:
time: 107 us; the launch traced here: 106 us
  waiting for transfers between devices  46.5 us (43%)
  starting transfers between devices  34.5 us (32%)
  Pallas kernels  22.5 us (21%)
  local copies, waits for them, and re-layouts  1.73 us (2%)
  between operations  1.11 us (1%)
    ppermute x40, waiting for transfers between devices, flipped(): lax.ppermute(value, axis, [(i, i ^ bits) for i in range(lax.axis_size(axi...  46.5 us
    ppermute x40, starting transfers between devices, flipped(): lax.ppermute(value, axis, [(i, i ^ bits) for i in range(lax.axis_size(axi...  30.2 us
    pallas_call x4, Pallas kernels, run_experts(): pl.pallas_call(functools.partial(experts_kernel, sizes=sizes, size=size),...  9.46 us
    pallas_call x2, Pallas kernels, attend(): pl.pallas_call(functools.partial(attention_kernel, first=first, kv_local=...  4.56 us
    ppermute x1, starting transfers between devices, shifted(): lax.ppermute(value, axis, [(source, source + steps) for source in range(l...  4.32 us
    pallas_call x2, Pallas kernels, project(): pl.pallas_call(functools.partial(projection_kernel, count=len(pieces), fi...  3.95 us
    pallas_call x1, Pallas kernels, dispatch(): pl.pallas_call(dispatch_kernel, grid_spec=pltpu.PrefetchScalarGridSpec(nu...  2.79 us
  transfers between devices with their start and end apart: 41, of which 17 were waited for; matrix products, arithmetic and copies ran while one was open for 0% of the time, Pallas kernels for 18%

profile of v4, /device:TPU:0, one launch (start us, length us, event | category | flops | bytes accessed | tf_op | source)
XLA Modules:
  0.0 106.4 jit_solution(7216481315376068090)
XLA Ops:
  0.7 2.8 %dispatch.1 = (bf16[128,128]{1,0:T(8,128)(2,1)S(1)}, bf16[128,128]{1,0:T(8,128)(2,1)S(1)}, bf16[32,2176]{1,0:T(8,128)(2,1)S(1)}, bf16[32,2176]{1,0:T(8,128)(2,1)...) custom-call(s32[4]{0:T(128)S(1)} %pad_add_fusion.place_ref, bf16[512,2048]{1,0:T(8,128)(2,1)} %tokens_ref.1, ...), custom_call_target="tpu_custom_call" | custom-call | flops 1000000000 | bytes 2000000 | tf_op jit(solution)/shard_map/dispatch/pallas_call | solution.py:199
  3.5 3.1 %collective-permute-start.22 = (bf16[32,2176]{1,0:T(8,128)(2,1)S(1)}, bf16[32,2176]{1,0:T(8,128)(2,1)S(1)}, u32[]{:S(2)}, u32[]{:S(2)}) collective-permute-start(bf16[32,2176]{1,0:T(8,128)(2,1)S(1)} %get-tuple-element.29), channel_id=1, source_target_pairs={{0,8},{4,12},{8,0},{12,4},{16,24},{20,28},{24,16},{28,20},{1,9},{5... | collective-permute-start | bytes 417800 | tf_op jit(solution)/shard_map/ppermute | solution.py:25
  6.6 2.6 %collective-permute-start.23 = (bf16[32,2176]{1,0:T(8,128)(2,1)S(1)}, bf16[32,2176]{1,0:T(8,128)(2,1)S(1)}, u32[]{:S(2)}, u32[]{:S(2)}) collective-permute-start(bf16[32,2176]{1,0:T(8,128)(2,1)S(1)} %get-tuple-element.30), channel_id=1, source_target_pairs={{0,16},{4,20},{8,24},{12,28},{16,0},{20,4},{24,8},{28,12},{1,17},{... | collective-permute-start | bytes 417800 | tf_op jit(solution)/shard_map/ppermute | solution.py:25
  9.3 2.9 %collective-permute-done.22 = bf16[32,2176]{1,0:T(8,128)(2,1)S(1)} collective-permute-done((bf16[32,2176]{1,0:T(8,128)(2,1)S(1)}, bf16[32,2176]{1,0:T(8,128)(2,1)S(1)}, u32[]{:S(2)}, u32[]{:S(2)}) %collective-permute-start.22) | collective-permute-done | bytes 139296 | tf_op jit(solution)/shard_map/ppermute | solution.py:25
  12.1 7.9 %collective-permute-done.23 = bf16[32,2176]{1,0:T(8,128)(2,1)S(1)} collective-permute-done((bf16[32,2176]{1,0:T(8,128)(2,1)S(1)}, bf16[32,2176]{1,0:T(8,128)(2,1)S(1)}, u32[]{:S(2)}, u32[]{:S(2)}) %collective-permute-start.23) | collective-permute-done | bytes 139296 | tf_op jit(solution)/shard_map/ppermute | solution.py:25
  24.3 2.4 %collective-permute-done.24.refs_1_ = bf16[64,2176]{1,0:T(8,128)(2,1)S(1)} collective-permute-done((bf16[64,2176]{1,0:T(8,128)(2,1)S(1)}, bf16[64,2176]{1,0:T(8,128)(2,1)S(1)}, u32[]{:S(2)}, u32[]{:S(2)}) %collective-permute-start.24) | collective-permute-done | bytes 278560 | tf_op jit(solution)/shard_map/ppermute | solution.py:25
  32.8 2.7 %collective-permute-done.9.refs_2_ = bf16[64,2176]{1,0:T(8,128)(2,1)S(1)} collective-permute-done((bf16[64,2176]{1,0:T(8,128)(2,1)S(1)}, bf16[64,2176]{1,0:T(8,128)(2,1)S(1)}, u32[]{:S(2)}, u32[]{:S(2)}) %collective-permute-start.9) | collective-permute-done | bytes 278560 | tf_op jit(solution)/shard_map/ppermute | solution.py:25
  35.5 2.9 %collective-permute-done.26.refs_3_ = bf16[32,2176]{1,0:T(8,128)(2,1)S(1)} collective-permute-done((bf16[32,2176]{1,0:T(8,128)(2,1)S(1)}, bf16[32,2176]{1,0:T(8,128)(2,1)S(1)}, u32[]{:S(2)}, u32[]{:S(2)}) %collective-permute-start.26) | collective-permute-done | bytes 139296 | tf_op jit(solution)/shard_map/ppermute | solution.py:25
  40.1 3.4 %collective-permute-done.11.refs_4_ = bf16[32,2176]{1,0:T(8,128)(2,1)S(1)} collective-permute-done((bf16[32,2176]{1,0:T(8,128)(2,1)S(1)}, bf16[32,2176]{1,0:T(8,128)(2,1)S(1)}, u32[]{:S(2)}, u32[]{:S(2)}) %collective-permute-start.11) | collective-permute-done | bytes 139296 | tf_op jit(solution)/shard_map/ppermute | solution.py:25
  46.2 2.4 %experts.7 = bf16[256,2048]{1,0:T(8,128)(2,1)S(1)} custom-call(s32[4]{0:T(128)S(1)} %pad_add_fusion.place_ref, bf16[64,2176]{1,0:T(8,128)(2,1)S(1)} %collective-permute-done.28.refs_0_, bf16[64,2176]{1,0:T(8,128)(2,1)S(1)} %collective-permute-done.29.refs_1_, bf16[64,2176]{1,0:T(8,128)(2,1)S(1)} %collective-permute-done.30.refs_2_, ...), custom_call_target="tpu_custom_call" | custom-call | flops 1792000000 | bytes 15000000 | tf_op jit(solution)/shard_map/experts/pallas_call | solution.py:255
  49.1 2.4 %experts.5 = bf16[256,2048]{1,0:T(8,128)(2,1)S(1)} custom-call(s32[4]{0:T(128)S(1)} %pad_add_fusion.place_ref, bf16[64,2176]{1,0:T(8,128)(2,1)S(1)} %collective-permute-done.12.refs_0_, bf16[64,2176]{1,0:T(8,128)(2,1)S(1)} %collective-permute-done.13.refs_1_, bf16[64,2176]{1,0:T(8,128)(2,1)S(1)} %collective-permute-done.14.refs_2_, ...), custom_call_target="tpu_custom_call" | custom-call | flops 1792000000 | bytes 15000000 | tf_op jit(solution)/shard_map/experts/pallas_call | solution.py:255
  51.7 2.3 %attend.3.refs_0_ = bf16[512,256]{1,0:T(8,128)(2,1)S(1)} custom-call(s32[4]{0:T(128)S(1)} %pad_add_fusion.place_ref, bf16[1024,256]{1,0:T(8,128)(2,1)S(1)} %copy-done.5, bf16[64,1024]{1,0:T(8,128)(2,1)S(1)} %bitcast.11, bf16[64,1024]{1,0:T(8,128)(2,1)S(1)} %bitcast.14, f32[4]{0:T(128)S(1)} %copy-done.8), custom_call_target="tpu_custom_call" | custom-call | flops 3000000000 | bytes 2000000 | tf_op jit(solution)/shard_map/attend/pallas_call | solution.py:87
  54.1 4.3 %collective-permute-start = (bf16[128,128]{1,0:T(8,128)(2,1)S(1)}, bf16[128,128]{1,0:T(8,128)(2,1)S(1)}, u32[]{:S(2)}, u32[]{:S(2)}) collective-permute-start(bf16[128,128]{1,0:T(8,128)(2,1)S(1)} %get-tuple-element.20), channel_id=1, source_target_pairs={{0,4},{4,8},{8,12},{12,16},{16,20},{20,24},{24,28},{1,5},{5,9},{9,... | collective-permute-start | bytes 98312 | tf_op jit(solution)/shard_map/ppermute | solution.py:21
  58.4 2.4 %experts.6.refs_0_ = bf16[256,2048]{1,0:T(8,128)(2,1)S(1)} custom-call(s32[4]{0:T(128)S(1)} %pad_add_fusion.place_ref, bf16[64,2176]{1,0:T(8,128)(2,1)S(1)} %constant_dynamic-update-slice_fusion.2.refs_0_, bf16[64,2176]{1,0:T(8,128)(2,1)S(1)} %collective-permute-done.24.refs_1_, bf16[64,2176]{1,0:T(8,128)(2,1)S(1)} %collective-permute-done.25.refs_2_, ...), custom_call_target="tpu_custom_call" | custom-call | flops 1792000000 | bytes 15000000 | tf_op jit(solution)/shard_map/experts/pallas_call | solution.py:255
  60.8 2.4 %experts.4.refs_0_ = bf16[256,2048]{1,0:T(8,128)(2,1)S(1)} custom-call(s32[4]{0:T(128)S(1)} %pad_add_fusion.place_ref, bf16[64,2176]{1,0:T(8,128)(2,1)S(1)} %constant_dynamic-update-slice_fusion.refs_0_, bf16[64,2176]{1,0:T(8,128)(2,1)S(1)} %collective-permute-done.8.refs_1_, bf16[64,2176]{1,0:T(8,128)(2,1)S(1)} %collective-permute-done.9.refs_2_, ...), custom_call_target="tpu_custom_call" | custom-call | flops 1792000000 | bytes 15000000 | tf_op jit(solution)/shard_map/experts/pallas_call | solution.py:255
  65.2 2.0 %collective-permute-start.18 = (bf16[64,2048]{1,0:T(8,128)(2,1)S(1)}, bf16[64,2048]{1,0:T(8,128)(2,1)S(1)}, u32[]{:S(2)}, u32[]{:S(2)}) collective-permute-start(bf16[64,2048]{1,0:T(8,128)(2,1)S(1)} %get-tuple-element.24), channel_id=1, source_target_pairs={{0,4},{4,0},{8,12},{12,8},{16,20},{20,16},{24,28},{28,24},{1,5},{5... | collective-permute-start | bytes 786440 | tf_op jit(solution)/shard_map/ppermute | solution.py:25
  67.6 2.3 %attend.2.refs_0_ = bf16[512,256]{1,0:T(8,128)(2,1)S(1)} custom-call(s32[4]{0:T(128)S(1)} %pad_add_fusion.place_ref, bf16[1024,256]{1,0:T(8,128)(2,1)S(1)} %copy-done.5, bf16[64,1024]{1,0:T(8,128)(2,1)S(1)} %bitcast.12, bf16[64,1024]{1,0:T(8,128)(2,1)S(1)} %bitcast.15, f32[4]{0:T(128)S(1)} %copy-done.8, bf16[128,128]{1,0:T(8,128)(2,1)S(1)} %collective-permute-done.refs_0_), custom_call_target="tpu_custom_call" | custom-call | flops 3000000000 | bytes 2000000 | tf_op jit(solution)/shard_map/attend/pallas_call | solution.py:87
  69.9 2.6 %collective-permute-done.34.refs_2_.refs_5_ = bf16[64,2048]{1,0:T(8,128)(2,1)S(1)} collective-permute-done((bf16[64,2048]{1,0:T(8,128)(2,1)S(1)}, bf16[64,2048]{1,0:T(8,128)(2,1)S(1)}, u32[]{:S(2)}, u32[]{:S(2)}) %collective-permute-start.34) | collective-permute-done | bytes 262176 | tf_op jit(solution)/shard_map/ppermute | solution.py:25
  74.7 2.3 %collective-permute-done.18.refs_2_.refs_5_ = bf16[64,2048]{1,0:T(8,128)(2,1)S(1)} collective-permute-done((bf16[64,2048]{1,0:T(8,128)(2,1)S(1)}, bf16[64,2048]{1,0:T(8,128)(2,1)S(1)}, u32[]{:S(2)}, u32[]{:S(2)}) %collective-permute-start.18) | collective-permute-done | bytes 262176 | tf_op jit(solution)/shard_map/ppermute | solution.py:25
  80.0 3.8 %collective-permute-done.2.refs_2_ = bf16[512,256]{1,0:T(8,128)(2,1)S(1)} collective-permute-done((bf16[512,256]{1,0:T(8,128)(2,1)S(1)}, bf16[512,256]{1,0:T(8,128)(2,1)S(1)}, u32[]{:S(2)}, u32[]{:S(2)}) %collective-permute-start.2) | collective-permute-done | bytes 262176 | tf_op jit(solution)/shard_map/ppermute | solution.py:25
  83.8 2.8 %collective-permute-done.36.refs_2_ = bf16[32,2048]{1,0:T(8,128)(2,1)S(1)} collective-permute-done((bf16[32,2048]{1,0:T(8,128)(2,1)S(1)}, bf16[32,2048]{1,0:T(8,128)(2,1)S(1)}, u32[]{:S(2)}, u32[]{:S(2)}) %collective-permute-start.36) | collective-permute-done | bytes 131104 | tf_op jit(solution)/shard_map/ppermute | solution.py:25
  90.2 3.2 %collective-permute-done.21.refs_3_ = bf16[32,2048]{1,0:T(8,128)(2,1)S(1)} collective-permute-done((bf16[32,2048]{1,0:T(8,128)(2,1)S(1)}, bf16[32,2048]{1,0:T(8,128)(2,1)S(1)}, u32[]{:S(2)}, u32[]{:S(2)}) %collective-permute-start.21) | collective-permute-done | bytes 131104 | tf_op jit(solution)/shard_map/ppermute | solution.py:25
  93.5 2.9 %collective-permute-start.39 = (bf16[32,2048]{1,0:T(8,128)(2,1)S(1)}, bf16[32,2048]{1,0:T(8,128)(2,1)S(1)}, u32[]{:S(2)}, u32[]{:S(2)}) collective-permute-start(bf16[32,2048]{1,0:T(8,128)(2,1)S(1)} %get-tuple-element.36), channel_id=1, source_target_pairs={{0,16},{4,20},{8,24},{12,28},{16,0},{20,4},{24,8},{28,12},{1,17},{... | collective-permute-start | bytes 393224 | tf_op jit(solution)/shard_map/ppermute | solution.py:25
  101.9 3.3 %collective-permute-done.39.refs_2_ = bf16[32,2048]{1,0:T(8,128)(2,1)S(1)} collective-permute-done((bf16[32,2048]{1,0:T(8,128)(2,1)S(1)}, bf16[32,2048]{1,0:T(8,128)(2,1)S(1)}, u32[]{:S(2)}, u32[]{:S(2)}) %collective-permute-start.39) | collective-permute-done | bytes 131104 | tf_op jit(solution)/shard_map/ppermute | solution.py:25
  (101 shorter events, 33.3 us)
Async XLA Ops:
  6.6 13.4 %collective-permute-start.23 = (bf16[32,2176]{1,0:T(8,128)(2,1)S(1)}, bf16[32,2176]{1,0:T(8,128)(2,1)S(1)}, u32[]{:S(2)}, u32[]{:S(2)}) collective-permute-start(bf16[32,2176]{1,0:T(8,128)(2,1)S(1)} %get-tuple-element.30), channel_id=1, source_target_pairs={{0,16},{4,20},{8,24},{12,28},{16,0},{20,4},{24,8},{28,12},{1,17},{... | collective-permute-start | bytes 417800 | tf_op jit(solution)/shard_map/ppermute | solution.py:25
  9.2 13.9 %collective-permute-start.7 = (bf16[32,2176]{1,0:T(8,128)(2,1)S(1)}, bf16[32,2176]{1,0:T(8,128)(2,1)S(1)}, u32[]{:S(2)}, u32[]{:S(2)}) collective-permute-start(bf16[32,2176]{1,0:T(8,128)(2,1)S(1)} %get-tuple-element.23), channel_id=1, source_target_pairs={{0,24},{4,28},{8,16},{12,20},{16,8},{20,12},{24,0},{28,4},{1,25},{... | collective-permute-start | bytes 417800 | tf_op jit(solution)/shard_map/ppermute | solution.py:25
  23.8 11.7 %collective-permute-start.9 = (bf16[64,2176]{1,0:T(8,128)(2,1)S(1)}, bf16[64,2176]{1,0:T(8,128)(2,1)S(1)}, u32[]{:S(2)}, u32[]{:S(2)}) collective-permute-start(bf16[64,2176]{1,0:T(8,128)(2,1)S(1)} %constant_dynamic-update-slice_fusion.refs_0_), channel_id=1, source_target_pairs={{0,4},{4,0},{8,12},{12,8},{16,20},{20,16},{24,28},{28,24},{1,5},{5... | collective-permute-start | bytes 835592 | tf_op jit(solution)/shard_map/ppermute | solution.py:25
  26.7 11.7 %collective-permute-start.26 = (bf16[32,2176]{1,0:T(8,128)(2,1)S(1)}, bf16[32,2176]{1,0:T(8,128)(2,1)S(1)}, u32[]{:S(2)}, u32[]{:S(2)}) collective-permute-start(bf16[32,2176]{1,0:T(8,128)(2,1)S(1)} %slice.18), channel_id=1, source_target_pairs={{0,4},{4,0},{8,12},{12,8},{16,20},{20,16},{24,28},{28,24},{1,5},{5... | collective-permute-start | bytes 417800 | tf_op jit(solution)/shard_map/ppermute | solution.py:25
  31.1 9.1 %collective-permute-start.10 = (bf16[32,2176]{1,0:T(8,128)(2,1)S(1)}, bf16[32,2176]{1,0:T(8,128)(2,1)S(1)}, u32[]{:S(2)}, u32[]{:S(2)}) collective-permute-start(bf16[32,2176]{1,0:T(8,128)(2,1)S(1)} %slice.16), channel_id=1, source_target_pairs={{0,4},{4,0},{8,12},{12,8},{16,20},{20,16},{24,28},{28,24},{1,5},{5... | collective-permute-start | bytes 417800 | tf_op jit(solution)/shard_map/ppermute | solution.py:25
  32.8 11.3 %collective-permute-start.29 = (bf16[64,2176]{1,0:T(8,128)(2,1)S(1)}, bf16[64,2176]{1,0:T(8,128)(2,1)S(1)}, u32[]{:S(2)}, u32[]{:S(2)}) collective-permute-start(bf16[64,2176]{1,0:T(8,128)(2,1)S(1)} %collective-permute-done.24.refs_1_), channel_id=1, source_target_pairs={{0,1},{1,0},{2,3},{3,2},{4,5},{5,4},{6,7},{7,6},{8,9},{9,8},{10,11... | collective-permute-start | bytes 835592 | tf_op jit(solution)/shard_map/ppermute | solution.py:25
  35.5 9.0 %collective-permute-start.30 = (bf16[64,2176]{1,0:T(8,128)(2,1)S(1)}, bf16[64,2176]{1,0:T(8,128)(2,1)S(1)}, u32[]{:S(2)}, u32[]{:S(2)}) collective-permute-start(bf16[64,2176]{1,0:T(8,128)(2,1)S(1)} %collective-permute-done.25.refs_2_), channel_id=1, source_target_pairs={{0,1},{1,0},{2,3},{3,2},{4,5},{5,4},{6,7},{7,6},{8,9},{9,8},{10,11... | collective-permute-start | bytes 835592 | tf_op jit(solution)/shard_map/ppermute | solution.py:25
  48.6 14.5 %collective-permute-start.33 = (bf16[256,2048]{1,0:T(8,128)(2,1)S(1)}, bf16[256,2048]{1,0:T(8,128)(2,1)S(1)}, u32[]{:S(2)}, u32[]{:S(2)}) collective-permute-start(bf16[256,2048]{1,0:T(8,128)(2,1)S(1)} %experts.7), channel_id=1, source_target_pairs={{0,1},{1,0},{2,3},{3,2},{4,5},{5,4},{6,7},{7,6},{8,9},{9,8},{10,11... | collective-permute-start | bytes 3145736 | tf_op jit(solution)/shard_map/ppermute | solution.py:25
  51.5 13.5 %collective-permute-start.17 = (bf16[256,2048]{1,0:T(8,128)(2,1)S(1)}, bf16[256,2048]{1,0:T(8,128)(2,1)S(1)}, u32[]{:S(2)}, u32[]{:S(2)}) collective-permute-start(bf16[256,2048]{1,0:T(8,128)(2,1)S(1)} %experts.5), channel_id=1, source_target_pairs={{0,1},{1,0},{2,3},{3,2},{4,5},{5,4},{6,7},{7,6},{8,9},{9,8},{10,11... | collective-permute-start | bytes 3145736 | tf_op jit(solution)/shard_map/ppermute | solution.py:25
  54.0 26.0 %collective-permute-start.5 = (bf16[512,256]{1,0:T(8,128)(2,1)S(1)}, bf16[512,256]{1,0:T(8,128)(2,1)S(1)}, u32[]{:S(2)}, u32[]{:S(2)}) collective-permute-start(bf16[512,256]{1,0:T(8,128)(2,1)S(1)} %attend.3.refs_0_), channel_id=1, source_target_pairs={{0,2},{1,3},{2,0},{3,1},{4,6},{5,7},{6,4},{7,5},{8,10},{9,11},{10,... | collective-permute-start | bytes 786440 | tf_op jit(solution)/shard_map/ppermute | solution.py:25
  54.1 13.1 %collective-permute-start = (bf16[128,128]{1,0:T(8,128)(2,1)S(1)}, bf16[128,128]{1,0:T(8,128)(2,1)S(1)}, u32[]{:S(2)}, u32[]{:S(2)}) collective-permute-start(bf16[128,128]{1,0:T(8,128)(2,1)S(1)} %get-tuple-element.20), channel_id=1, source_target_pairs={{0,4},{4,8},{8,12},{12,16},{16,20},{20,24},{24,28},{1,5},{5,9},{9,... | collective-permute-start | bytes 98312 | tf_op jit(solution)/shard_map/ppermute | solution.py:21
  63.3 9.2 %collective-permute-start.34 = (bf16[64,2048]{1,0:T(8,128)(2,1)S(1)}, bf16[64,2048]{1,0:T(8,128)(2,1)S(1)}, u32[]{:S(2)}, u32[]{:S(2)}) collective-permute-start(bf16[64,2048]{1,0:T(8,128)(2,1)S(1)} %get-tuple-element.31), channel_id=1, source_target_pairs={{0,4},{4,0},{8,12},{12,8},{16,20},{20,16},{24,28},{28,24},{1,5},{5... | collective-permute-start | bytes 786440 | tf_op jit(solution)/shard_map/ppermute | solution.py:25
  63.4 10.8 %collective-permute-start.35 = (bf16[64,2048]{1,0:T(8,128)(2,1)S(1)}, bf16[64,2048]{1,0:T(8,128)(2,1)S(1)}, u32[]{:S(2)}, u32[]{:S(2)}) collective-permute-start(bf16[64,2048]{1,0:T(8,128)(2,1)S(1)} %get-tuple-element.32), channel_id=1, source_target_pairs={{0,2},{1,3},{2,0},{3,1},{4,6},{5,7},{6,4},{7,5},{8,10},{9,11},{10,... | collective-permute-start | bytes 786440 | tf_op jit(solution)/shard_map/ppermute | solution.py:25
  65.2 11.9 %collective-permute-start.18 = (bf16[64,2048]{1,0:T(8,128)(2,1)S(1)}, bf16[64,2048]{1,0:T(8,128)(2,1)S(1)}, u32[]{:S(2)}, u32[]{:S(2)}) collective-permute-start(bf16[64,2048]{1,0:T(8,128)(2,1)S(1)} %get-tuple-element.24), channel_id=1, source_target_pairs={{0,4},{4,0},{8,12},{12,8},{16,20},{20,16},{24,28},{28,24},{1,5},{5... | collective-permute-start | bytes 786440 | tf_op jit(solution)/shard_map/ppermute | solution.py:25
  67.2 11.0 %collective-permute-start.19 = (bf16[64,2048]{1,0:T(8,128)(2,1)S(1)}, bf16[64,2048]{1,0:T(8,128)(2,1)S(1)}, u32[]{:S(2)}, u32[]{:S(2)}) collective-permute-start(bf16[64,2048]{1,0:T(8,128)(2,1)S(1)} %get-tuple-element.25), channel_id=1, source_target_pairs={{0,2},{1,3},{2,0},{3,1},{4,6},{5,7},{6,4},{7,5},{8,10},{9,11},{10,... | collective-permute-start | bytes 786440 | tf_op jit(solution)/shard_map/ppermute | solution.py:25
  72.5 11.3 %collective-permute-start.2 = (bf16[512,256]{1,0:T(8,128)(2,1)S(1)}, bf16[512,256]{1,0:T(8,128)(2,1)S(1)}, u32[]{:S(2)}, u32[]{:S(2)}) collective-permute-start(bf16[512,256]{1,0:T(8,128)(2,1)S(1)} %attend.2.refs_0_), channel_id=1, source_target_pairs={{0,2},{1,3},{2,0},{3,1},{4,6},{5,7},{6,4},{7,5},{8,10},{9,11},{10,... | collective-permute-start | bytes 786440 | tf_op jit(solution)/shard_map/ppermute | solution.py:25
  74.2 12.4 %collective-permute-start.36 = (bf16[32,2048]{1,0:T(8,128)(2,1)S(1)}, bf16[32,2048]{1,0:T(8,128)(2,1)S(1)}, u32[]{:S(2)}, u32[]{:S(2)}) collective-permute-start(bf16[32,2048]{1,0:T(8,128)(2,1)S(1)} %get-tuple-element.33), channel_id=1, source_target_pairs={{0,2},{1,3},{2,0},{3,1},{4,6},{5,7},{6,4},{7,5},{8,10},{9,11},{10,... | collective-permute-start | bytes 393224 | tf_op jit(solution)/shard_map/ppermute | solution.py:25
  77.0 9.6 %collective-permute-start.37 = (bf16[32,2048]{1,0:T(8,128)(2,1)S(1)}, bf16[32,2048]{1,0:T(8,128)(2,1)S(1)}, u32[]{:S(2)}, u32[]{:S(2)}) collective-permute-start(bf16[32,2048]{1,0:T(8,128)(2,1)S(1)} %get-tuple-element.34), channel_id=1, source_target_pairs={{0,4},{4,0},{8,12},{12,8},{16,20},{20,16},{24,28},{28,24},{1,5},{5... | collective-permute-start | bytes 393224 | tf_op jit(solution)/shard_map/ppermute | solution.py:25
  78.3 10.0 %collective-permute-start.20 = (bf16[32,2048]{1,0:T(8,128)(2,1)S(1)}, bf16[32,2048]{1,0:T(8,128)(2,1)S(1)}, u32[]{:S(2)}, u32[]{:S(2)}) collective-permute-start(bf16[32,2048]{1,0:T(8,128)(2,1)S(1)} %get-tuple-element.26), channel_id=1, source_target_pairs={{0,2},{1,3},{2,0},{3,1},{4,6},{5,7},{6,4},{7,5},{8,10},{9,11},{10,... | collective-permute-start | bytes 393224 | tf_op jit(solution)/shard_map/ppermute | solution.py:25
  80.0 13.5 %collective-permute-start.4 = (bf16[512,256]{1,0:T(8,128)(2,1)S(1)}, bf16[512,256]{1,0:T(8,128)(2,1)S(1)}, u32[]{:S(2)}, u32[]{:S(2)}) collective-permute-start(bf16[512,256]{1,0:T(8,128)(2,1)S(1)} %attend.3.refs_0_), channel_id=1, source_target_pairs={{0,1},{1,0},{2,3},{3,2},{4,5},{5,4},{6,7},{7,6},{8,9},{9,8},{10,11... | collective-permute-start | bytes 786440 | tf_op jit(solution)/shard_map/ppermute | solution.py:25
  83.8 12.5 %collective-permute-start.6 = (bf16[512,256]{1,0:T(8,128)(2,1)S(1)}, bf16[512,256]{1,0:T(8,128)(2,1)S(1)}, u32[]{:S(2)}, u32[]{:S(2)}) collective-permute-start(bf16[512,256]{1,0:T(8,128)(2,1)S(1)} %collective-permute-done.5.refs_2_), channel_id=1, source_target_pairs={{0,1},{1,0},{2,3},{3,2},{4,5},{5,4},{6,7},{7,6},{8,9},{9,8},{10,11... | collective-permute-start | bytes 786440 | tf_op jit(solution)/shard_map/ppermute | solution.py:25
  86.6 13.3 %collective-permute-start.1 = (bf16[512,256]{1,0:T(8,128)(2,1)S(1)}, bf16[512,256]{1,0:T(8,128)(2,1)S(1)}, u32[]{:S(2)}, u32[]{:S(2)}) collective-permute-start(bf16[512,256]{1,0:T(8,128)(2,1)S(1)} %attend.2.refs_0_), channel_id=1, source_target_pairs={{0,1},{1,0},{2,3},{3,2},{4,5},{5,4},{6,7},{7,6},{8,9},{9,8},{10,11... | collective-permute-start | bytes 786440 | tf_op jit(solution)/shard_map/ppermute | solution.py:25
  86.6 13.3 %collective-permute-start.3 = (bf16[512,256]{1,0:T(8,128)(2,1)S(1)}, bf16[512,256]{1,0:T(8,128)(2,1)S(1)}, u32[]{:S(2)}, u32[]{:S(2)}) collective-permute-start(bf16[512,256]{1,0:T(8,128)(2,1)S(1)} %collective-permute-done.2.refs_2_), channel_id=1, source_target_pairs={{0,1},{1,0},{2,3},{3,2},{4,5},{5,4},{6,7},{7,6},{8,9},{9,8},{10,11... | collective-permute-start | bytes 786440 | tf_op jit(solution)/shard_map/ppermute | solution.py:25
  93.5 11.7 %collective-permute-start.39 = (bf16[32,2048]{1,0:T(8,128)(2,1)S(1)}, bf16[32,2048]{1,0:T(8,128)(2,1)S(1)}, u32[]{:S(2)}, u32[]{:S(2)}) collective-permute-start(bf16[32,2048]{1,0:T(8,128)(2,1)S(1)} %get-tuple-element.36), channel_id=1, source_target_pairs={{0,16},{4,20},{8,24},{12,28},{16,0},{20,4},{24,8},{28,12},{1,17},{... | collective-permute-start | bytes 393224 | tf_op jit(solution)/shard_map/ppermute | solution.py:25
  (26 other events, 227.0 us)

commit v5 on v4

--- a/solution.py
+++ b/solution.py
@@ -118,7 +118,7 @@
 
 def project(place, pieces, out_weight, part, parts, held):
     rows = pieces[0].shape[0]
-    steps = 2
+    steps = 1
     vmem = pl.BlockSpec(memory_space=pltpu.VMEM)
     operands = [place, *in_vmem(*pieces, out_weight), *held]
     return pl.pallas_call(
@@ -150,8 +150,9 @@
     values = tokens_ref[...].astype(jnp.float32)
     scaled = values * lax.rsqrt(jnp.mean(values * values, axis=-1, keepdims=True) + 1e-06) * gain_ref[...]
     normed = scaled.astype(jnp.bfloat16)
-    group_logits = dot_f32(group_ref[...], normed, (1, 1))
-    expert_logits = dot_f32(expert_ref[...], normed, (1, 1))
+    logits = dot_f32(jnp.concatenate([expert_ref[...], group_ref[...]], axis=0), normed, (1, 1))
+    expert_logits = logits[:experts]
+    group_logits = logits[experts:]
     first = routes_ref[0:1, :]
     second = routes_ref[1:2, :]
     group_index = lax.broadcasted_iota(jnp.int32, (groups, rows), 0)
@@ -226,14 +227,10 @@
 def experts_kernel(place_ref, *refs, sizes, size):
     count = len(sizes)
     pieces = refs[:count]
-    gate_ref, up_ref, down_ref, out_ref, rows_ref = refs[count:]
+    gate_ref, up_ref, down_ref, out_ref = refs[count:]
     exp_local, width, hidden = gate_ref.shape
-    at = 0
-    for piece, rows in zip(pieces, sizes):
-        rows_ref[at : at + rows, :] = piece[...]
-        at += rows
-    held = rows_ref[:, :width]
-    gates = rows_ref[:, width:].astype(jnp.float32)
+    held = jnp.concatenate([piece[:, :width] for piece in pieces], axis=0)
+    gates = jnp.concatenate([piece[:, width:] for piece in pieces], axis=0).astype(jnp.float32)
     line = lax.broadcasted_iota(jnp.int32, gates.shape, 1)
     active = []
     for e in range(exp_local):
@@ -257,7 +254,6 @@
         out_shape=vmem_out((rows, width)),
         in_specs=[smem] + [vmem] * (len(pieces) + 3),
         out_specs=vmem,
-        scratch_shapes=[pltpu.VMEM((rows, width + LANES), jnp.bfloat16)],
         cost_estimate=pl.CostEstimate(flops=rows * 7_000_000, bytes_accessed=15_000_000, transcendentals=0),
         compiler_params=pltpu.CompilerParams(vmem_limit_bytes=14 << 20),
         name="experts",

time: 107 us -> 106 us (level)
  no operation moved by 1% of the time
where the time goes in v5:
time: 106 us
  waiting for transfers between devices  46.3 us (44%)
  starting transfers between devices  34.5 us (33%)
  Pallas kernels  22.4 us (21%)
  local copies, waits for them, and re-layouts  1.73 us (2%)
  between operations  1.11 us (1%)
    ppermute x40, waiting for transfers between devices, flipped(): lax.ppermute(value, axis, [(i, i ^ bits) for i in range(lax.axis_size(axi...  46.3 us
    ppermute x40, starting transfers between devices, flipped(): lax.ppermute(value, axis, [(i, i ^ bits) for i in range(lax.axis_size(axi...  30.2 us
    pallas_call x4, Pallas kernels, run_experts(): pl.pallas_call(functools.partial(experts_kernel, sizes=sizes, size=size),...  9.36 us
    pallas_call x2, Pallas kernels, attend(): pl.pallas_call(functools.partial(attention_kernel, first=first, kv_local=...  4.56 us
    ppermute x1, starting transfers between devices, shifted(): lax.ppermute(value, axis, [(source, source + steps) for source in range(l...  4.3 us
    pallas_call x2, Pallas kernels, project(): pl.pallas_call(functools.partial(projection_kernel, count=len(pieces), fi...  4.11 us
    pallas_call x1, Pallas kernels, dispatch(): pl.pallas_call(dispatch_kernel, grid_spec=pltpu.PrefetchScalarGridSpec(nu...  2.67 us
  transfers between devices with their start and end apart: 41, of which 17 were waited for; matrix products, arithmetic and copies ran while one was open for 0% of the time, Pallas kernels for 18%

profile of v5, /device:TPU:0, one launch (start us, length us, event | category | flops | bytes accessed | tf_op | source)
XLA Modules:
  0.0 106.2 jit_solution(18174533152544677105)
XLA Ops:
  0.7 2.7 %dispatch.1 = (bf16[128,128]{1,0:T(8,128)(2,1)S(1)}, bf16[128,128]{1,0:T(8,128)(2,1)S(1)}, bf16[32,2176]{1,0:T(8,128)(2,1)S(1)}, bf16[32,2176]{1,0:T(8,128)(2,1)...) custom-call(s32[4]{0:T(128)S(1)} %pad_add_fusion.place_ref, bf16[512,2048]{1,0:T(8,128)(2,1)} %tokens_ref.1, ...), custom_call_target="tpu_custom_call" | custom-call | flops 1000000000 | bytes 2000000 | tf_op jit(solution)/shard_map/dispatch/pallas_call | solution.py:200
  3.4 3.1 %collective-permute-start.22 = (bf16[32,2176]{1,0:T(8,128)(2,1)S(1)}, bf16[32,2176]{1,0:T(8,128)(2,1)S(1)}, u32[]{:S(2)}, u32[]{:S(2)}) collective-permute-start(bf16[32,2176]{1,0:T(8,128)(2,1)S(1)} %get-tuple-element.29), channel_id=1, source_target_pairs={{0,8},{4,12},{8,0},{12,4},{16,24},{20,28},{24,16},{28,20},{1,9},{5... | collective-permute-start | bytes 417800 | tf_op jit(solution)/shard_map/ppermute | solution.py:25
  6.5 2.6 %collective-permute-start.23 = (bf16[32,2176]{1,0:T(8,128)(2,1)S(1)}, bf16[32,2176]{1,0:T(8,128)(2,1)S(1)}, u32[]{:S(2)}, u32[]{:S(2)}) collective-permute-start(bf16[32,2176]{1,0:T(8,128)(2,1)S(1)} %get-tuple-element.30), channel_id=1, source_target_pairs={{0,16},{4,20},{8,24},{12,28},{16,0},{20,4},{24,8},{28,12},{1,17},{... | collective-permute-start | bytes 417800 | tf_op jit(solution)/shard_map/ppermute | solution.py:25
  9.1 2.9 %collective-permute-done.22 = bf16[32,2176]{1,0:T(8,128)(2,1)S(1)} collective-permute-done((bf16[32,2176]{1,0:T(8,128)(2,1)S(1)}, bf16[32,2176]{1,0:T(8,128)(2,1)S(1)}, u32[]{:S(2)}, u32[]{:S(2)}) %collective-permute-start.22) | collective-permute-done | bytes 139296 | tf_op jit(solution)/shard_map/ppermute | solution.py:25
  12.0 7.9 %collective-permute-done.23 = bf16[32,2176]{1,0:T(8,128)(2,1)S(1)} collective-permute-done((bf16[32,2176]{1,0:T(8,128)(2,1)S(1)}, bf16[32,2176]{1,0:T(8,128)(2,1)S(1)}, u32[]{:S(2)}, u32[]{:S(2)}) %collective-permute-start.23) | collective-permute-done | bytes 139296 | tf_op jit(solution)/shard_map/ppermute | solution.py:25
  24.2 2.4 %collective-permute-done.24.refs_1_ = bf16[64,2176]{1,0:T(8,128)(2,1)S(1)} collective-permute-done((bf16[64,2176]{1,0:T(8,128)(2,1)S(1)}, bf16[64,2176]{1,0:T(8,128)(2,1)S(1)}, u32[]{:S(2)}, u32[]{:S(2)}) %collective-permute-start.24) | collective-permute-done | bytes 278560 | tf_op jit(solution)/shard_map/ppermute | solution.py:25
  32.7 2.7 %collective-permute-done.9.refs_2_ = bf16[64,2176]{1,0:T(8,128)(2,1)S(1)} collective-permute-done((bf16[64,2176]{1,0:T(8,128)(2,1)S(1)}, bf16[64,2176]{1,0:T(8,128)(2,1)S(1)}, u32[]{:S(2)}, u32[]{:S(2)}) %collective-permute-start.9) | collective-permute-done | bytes 278560 | tf_op jit(solution)/shard_map/ppermute | solution.py:25
  35.4 2.9 %collective-permute-done.26.refs_3_ = bf16[32,2176]{1,0:T(8,128)(2,1)S(1)} collective-permute-done((bf16[32,2176]{1,0:T(8,128)(2,1)S(1)}, bf16[32,2176]{1,0:T(8,128)(2,1)S(1)}, u32[]{:S(2)}, u32[]{:S(2)}) %collective-permute-start.26) | collective-permute-done | bytes 139296 | tf_op jit(solution)/shard_map/ppermute | solution.py:25
  40.0 3.4 %collective-permute-done.11.refs_4_ = bf16[32,2176]{1,0:T(8,128)(2,1)S(1)} collective-permute-done((bf16[32,2176]{1,0:T(8,128)(2,1)S(1)}, bf16[32,2176]{1,0:T(8,128)(2,1)S(1)}, u32[]{:S(2)}, u32[]{:S(2)}) %collective-permute-start.11) | collective-permute-done | bytes 139296 | tf_op jit(solution)/shard_map/ppermute | solution.py:25
  46.1 2.3 %experts.7 = bf16[256,2048]{1,0:T(8,128)(2,1)S(1)} custom-call(s32[4]{0:T(128)S(1)} %pad_add_fusion.place_ref, bf16[64,2176]{1,0:T(8,128)(2,1)S(1)} %collective-permute-done.28.refs_0_, bf16[64,2176]{1,0:T(8,128)(2,1)S(1)} %collective-permute-done.29.refs_1_, bf16[64,2176]{1,0:T(8,128)(2,1)S(1)} %collective-permute-done.30.refs_2_, ...), custom_call_target="tpu_custom_call" | custom-call | flops 1792000000 | bytes 15000000 | tf_op jit(solution)/shard_map/experts/pallas_call | solution.py:252
  49.0 2.3 %experts.5 = bf16[256,2048]{1,0:T(8,128)(2,1)S(1)} custom-call(s32[4]{0:T(128)S(1)} %pad_add_fusion.place_ref, bf16[64,2176]{1,0:T(8,128)(2,1)S(1)} %collective-permute-done.12.refs_0_, bf16[64,2176]{1,0:T(8,128)(2,1)S(1)} %collective-permute-done.13.refs_1_, bf16[64,2176]{1,0:T(8,128)(2,1)S(1)} %collective-permute-done.14.refs_2_, ...), custom_call_target="tpu_custom_call" | custom-call | flops 1792000000 | bytes 15000000 | tf_op jit(solution)/shard_map/experts/pallas_call | solution.py:252
  51.5 2.3 %attend.3.refs_0_ = bf16[512,256]{1,0:T(8,128)(2,1)S(1)} custom-call(s32[4]{0:T(128)S(1)} %pad_add_fusion.place_ref, bf16[1024,256]{1,0:T(8,128)(2,1)S(1)} %copy-done.5, bf16[64,1024]{1,0:T(8,128)(2,1)S(1)} %bitcast.11, bf16[64,1024]{1,0:T(8,128)(2,1)S(1)} %bitcast.14, f32[4]{0:T(128)S(1)} %copy-done.8), custom_call_target="tpu_custom_call" | custom-call | flops 3000000000 | bytes 2000000 | tf_op jit(solution)/shard_map/attend/pallas_call | solution.py:87
  53.9 4.3 %collective-permute-start = (bf16[128,128]{1,0:T(8,128)(2,1)S(1)}, bf16[128,128]{1,0:T(8,128)(2,1)S(1)}, u32[]{:S(2)}, u32[]{:S(2)}) collective-permute-start(bf16[128,128]{1,0:T(8,128)(2,1)S(1)} %get-tuple-element.20), channel_id=1, source_target_pairs={{0,4},{4,8},{8,12},{12,16},{16,20},{20,24},{24,28},{1,5},{5,9},{9,... | collective-permute-start | bytes 98312 | tf_op jit(solution)/shard_map/ppermute | solution.py:21
  58.2 2.3 %experts.6.refs_0_ = bf16[256,2048]{1,0:T(8,128)(2,1)S(1)} custom-call(s32[4]{0:T(128)S(1)} %pad_add_fusion.place_ref, bf16[64,2176]{1,0:T(8,128)(2,1)S(1)} %constant_dynamic-update-slice_fusion.2.refs_0_, bf16[64,2176]{1,0:T(8,128)(2,1)S(1)} %collective-permute-done.24.refs_1_, bf16[64,2176]{1,0:T(8,128)(2,1)S(1)} %collective-permute-done.25.refs_2_, ...), custom_call_target="tpu_custom_call" | custom-call | flops 1792000000 | bytes 15000000 | tf_op jit(solution)/shard_map/experts/pallas_call | solution.py:252
  60.6 2.3 %experts.4.refs_0_ = bf16[256,2048]{1,0:T(8,128)(2,1)S(1)} custom-call(s32[4]{0:T(128)S(1)} %pad_add_fusion.place_ref, bf16[64,2176]{1,0:T(8,128)(2,1)S(1)} %constant_dynamic-update-slice_fusion.refs_0_, bf16[64,2176]{1,0:T(8,128)(2,1)S(1)} %collective-permute-done.8.refs_1_, bf16[64,2176]{1,0:T(8,128)(2,1)S(1)} %collective-permute-done.9.refs_2_, ...), custom_call_target="tpu_custom_call" | custom-call | flops 1792000000 | bytes 15000000 | tf_op jit(solution)/shard_map/experts/pallas_call | solution.py:252
  67.4 2.3 %attend.2.refs_0_ = bf16[512,256]{1,0:T(8,128)(2,1)S(1)} custom-call(s32[4]{0:T(128)S(1)} %pad_add_fusion.place_ref, bf16[1024,256]{1,0:T(8,128)(2,1)S(1)} %copy-done.5, bf16[64,1024]{1,0:T(8,128)(2,1)S(1)} %bitcast.12, bf16[64,1024]{1,0:T(8,128)(2,1)S(1)} %bitcast.15, f32[4]{0:T(128)S(1)} %copy-done.8, bf16[128,128]{1,0:T(8,128)(2,1)S(1)} %collective-permute-done.refs_0_), custom_call_target="tpu_custom_call" | custom-call | flops 3000000000 | bytes 2000000 | tf_op jit(solution)/shard_map/attend/pallas_call | solution.py:87
  69.6 2.6 %collective-permute-done.34.refs_2_.refs_5_ = bf16[64,2048]{1,0:T(8,128)(2,1)S(1)} collective-permute-done((bf16[64,2048]{1,0:T(8,128)(2,1)S(1)}, bf16[64,2048]{1,0:T(8,128)(2,1)S(1)}, u32[]{:S(2)}, u32[]{:S(2)}) %collective-permute-start.34) | collective-permute-done | bytes 262176 | tf_op jit(solution)/shard_map/ppermute | solution.py:25
  74.5 2.3 %collective-permute-done.18.refs_2_.refs_5_ = bf16[64,2048]{1,0:T(8,128)(2,1)S(1)} collective-permute-done((bf16[64,2048]{1,0:T(8,128)(2,1)S(1)}, bf16[64,2048]{1,0:T(8,128)(2,1)S(1)}, u32[]{:S(2)}, u32[]{:S(2)}) %collective-permute-start.18) | collective-permute-done | bytes 262176 | tf_op jit(solution)/shard_map/ppermute | solution.py:25
  79.8 3.8 %collective-permute-done.2.refs_2_ = bf16[512,256]{1,0:T(8,128)(2,1)S(1)} collective-permute-done((bf16[512,256]{1,0:T(8,128)(2,1)S(1)}, bf16[512,256]{1,0:T(8,128)(2,1)S(1)}, u32[]{:S(2)}, u32[]{:S(2)}) %collective-permute-start.2) | collective-permute-done | bytes 262176 | tf_op jit(solution)/shard_map/ppermute | solution.py:25
  83.6 2.8 %collective-permute-done.36.refs_2_ = bf16[32,2048]{1,0:T(8,128)(2,1)S(1)} collective-permute-done((bf16[32,2048]{1,0:T(8,128)(2,1)S(1)}, bf16[32,2048]{1,0:T(8,128)(2,1)S(1)}, u32[]{:S(2)}, u32[]{:S(2)}) %collective-permute-start.36) | collective-permute-done | bytes 131104 | tf_op jit(solution)/shard_map/ppermute | solution.py:25
  89.9 3.2 %collective-permute-done.21.refs_3_ = bf16[32,2048]{1,0:T(8,128)(2,1)S(1)} collective-permute-done((bf16[32,2048]{1,0:T(8,128)(2,1)S(1)}, bf16[32,2048]{1,0:T(8,128)(2,1)S(1)}, u32[]{:S(2)}, u32[]{:S(2)}) %collective-permute-start.21) | collective-permute-done | bytes 131104 | tf_op jit(solution)/shard_map/ppermute | solution.py:25
  93.3 2.9 %collective-permute-start.39 = (bf16[32,2048]{1,0:T(8,128)(2,1)S(1)}, bf16[32,2048]{1,0:T(8,128)(2,1)S(1)}, u32[]{:S(2)}, u32[]{:S(2)}) collective-permute-start(bf16[32,2048]{1,0:T(8,128)(2,1)S(1)} %get-tuple-element.36), channel_id=1, source_target_pairs={{0,16},{4,20},{8,24},{12,28},{16,0},{20,4},{24,8},{28,12},{1,17},{... | collective-permute-start | bytes 393224 | tf_op jit(solution)/shard_map/ppermute | solution.py:25
  99.8 2.1 %project.3 = bf16[1024,512]{1,0:T(8,128)(2,1)} custom-call(s32[4]{0:T(128)S(1)} %pad_add_fusion.place_ref, bf16[512,256]{1,0:T(8,128)(2,1)S(1)} %attend.2.refs_0_, bf16[512,256]{1,0:T(8,128)(2,1)S(1)} %collective-permute-done.1.refs_1_, bf16[512,256]{1,0:T(8,128)(2,1)S(1)} %collective-permute-done.2.refs_2_, ...), custom_call_target="tpu_custom_call", output_to_operand_aliasing={{}: (6, {})} | custom-call | flops 1000000000 | bytes 3000000 | tf_op jit(solution)/shard_map/project/pallas_call | solution.py:124
  101.9 3.1 %collective-permute-done.39.refs_2_ = bf16[32,2048]{1,0:T(8,128)(2,1)S(1)} collective-permute-done((bf16[32,2048]{1,0:T(8,128)(2,1)S(1)}, bf16[32,2048]{1,0:T(8,128)(2,1)S(1)}, u32[]{:S(2)}, u32[]{:S(2)}) %collective-permute-start.39) | collective-permute-done | bytes 131104 | tf_op jit(solution)/shard_map/ppermute | solution.py:25
  (101 shorter events, 33.4 us)
Async XLA Ops:
  6.5 13.4 %collective-permute-start.23 = (bf16[32,2176]{1,0:T(8,128)(2,1)S(1)}, bf16[32,2176]{1,0:T(8,128)(2,1)S(1)}, u32[]{:S(2)}, u32[]{:S(2)}) collective-permute-start(bf16[32,2176]{1,0:T(8,128)(2,1)S(1)} %get-tuple-element.30), channel_id=1, source_target_pairs={{0,16},{4,20},{8,24},{12,28},{16,0},{20,4},{24,8},{28,12},{1,17},{... | collective-permute-start | bytes 417800 | tf_op jit(solution)/shard_map/ppermute | solution.py:25
  9.1 13.9 %collective-permute-start.7 = (bf16[32,2176]{1,0:T(8,128)(2,1)S(1)}, bf16[32,2176]{1,0:T(8,128)(2,1)S(1)}, u32[]{:S(2)}, u32[]{:S(2)}) collective-permute-start(bf16[32,2176]{1,0:T(8,128)(2,1)S(1)} %get-tuple-element.23), channel_id=1, source_target_pairs={{0,24},{4,28},{8,16},{12,20},{16,8},{20,12},{24,0},{28,4},{1,25},{... | collective-permute-start | bytes 417800 | tf_op jit(solution)/shard_map/ppermute | solution.py:25
  23.7 11.7 %collective-permute-start.9 = (bf16[64,2176]{1,0:T(8,128)(2,1)S(1)}, bf16[64,2176]{1,0:T(8,128)(2,1)S(1)}, u32[]{:S(2)}, u32[]{:S(2)}) collective-permute-start(bf16[64,2176]{1,0:T(8,128)(2,1)S(1)} %constant_dynamic-update-slice_fusion.refs_0_), channel_id=1, source_target_pairs={{0,4},{4,0},{8,12},{12,8},{16,20},{20,16},{24,28},{28,24},{1,5},{5... | collective-permute-start | bytes 835592 | tf_op jit(solution)/shard_map/ppermute | solution.py:25
  26.6 11.7 %collective-permute-start.26 = (bf16[32,2176]{1,0:T(8,128)(2,1)S(1)}, bf16[32,2176]{1,0:T(8,128)(2,1)S(1)}, u32[]{:S(2)}, u32[]{:S(2)}) collective-permute-start(bf16[32,2176]{1,0:T(8,128)(2,1)S(1)} %slice.18), channel_id=1, source_target_pairs={{0,4},{4,0},{8,12},{12,8},{16,20},{20,16},{24,28},{28,24},{1,5},{5... | collective-permute-start | bytes 417800 | tf_op jit(solution)/shard_map/ppermute | solution.py:25
  31.0 9.0 %collective-permute-start.10 = (bf16[32,2176]{1,0:T(8,128)(2,1)S(1)}, bf16[32,2176]{1,0:T(8,128)(2,1)S(1)}, u32[]{:S(2)}, u32[]{:S(2)}) collective-permute-start(bf16[32,2176]{1,0:T(8,128)(2,1)S(1)} %slice.16), channel_id=1, source_target_pairs={{0,4},{4,0},{8,12},{12,8},{16,20},{20,16},{24,28},{28,24},{1,5},{5... | collective-permute-start | bytes 417800 | tf_op jit(solution)/shard_map/ppermute | solution.py:25
  32.7 11.3 %collective-permute-start.29 = (bf16[64,2176]{1,0:T(8,128)(2,1)S(1)}, bf16[64,2176]{1,0:T(8,128)(2,1)S(1)}, u32[]{:S(2)}, u32[]{:S(2)}) collective-permute-start(bf16[64,2176]{1,0:T(8,128)(2,1)S(1)} %collective-permute-done.24.refs_1_), channel_id=1, source_target_pairs={{0,1},{1,0},{2,3},{3,2},{4,5},{5,4},{6,7},{7,6},{8,9},{9,8},{10,11... | collective-permute-start | bytes 835592 | tf_op jit(solution)/shard_map/ppermute | solution.py:25
  35.4 9.0 %collective-permute-start.30 = (bf16[64,2176]{1,0:T(8,128)(2,1)S(1)}, bf16[64,2176]{1,0:T(8,128)(2,1)S(1)}, u32[]{:S(2)}, u32[]{:S(2)}) collective-permute-start(bf16[64,2176]{1,0:T(8,128)(2,1)S(1)} %collective-permute-done.25.refs_2_), channel_id=1, source_target_pairs={{0,1},{1,0},{2,3},{3,2},{4,5},{5,4},{6,7},{7,6},{8,9},{9,8},{10,11... | collective-permute-start | bytes 835592 | tf_op jit(solution)/shard_map/ppermute | solution.py:25
  48.5 14.4 %collective-permute-start.33 = (bf16[256,2048]{1,0:T(8,128)(2,1)S(1)}, bf16[256,2048]{1,0:T(8,128)(2,1)S(1)}, u32[]{:S(2)}, u32[]{:S(2)}) collective-permute-start(bf16[256,2048]{1,0:T(8,128)(2,1)S(1)} %experts.7), channel_id=1, source_target_pairs={{0,1},{1,0},{2,3},{3,2},{4,5},{5,4},{6,7},{7,6},{8,9},{9,8},{10,11... | collective-permute-start | bytes 3145736 | tf_op jit(solution)/shard_map/ppermute | solution.py:25
  51.4 13.5 %collective-permute-start.17 = (bf16[256,2048]{1,0:T(8,128)(2,1)S(1)}, bf16[256,2048]{1,0:T(8,128)(2,1)S(1)}, u32[]{:S(2)}, u32[]{:S(2)}) collective-permute-start(bf16[256,2048]{1,0:T(8,128)(2,1)S(1)} %experts.5), channel_id=1, source_target_pairs={{0,1},{1,0},{2,3},{3,2},{4,5},{5,4},{6,7},{7,6},{8,9},{9,8},{10,11... | collective-permute-start | bytes 3145736 | tf_op jit(solution)/shard_map/ppermute | solution.py:25
  53.8 26.0 %collective-permute-start.5 = (bf16[512,256]{1,0:T(8,128)(2,1)S(1)}, bf16[512,256]{1,0:T(8,128)(2,1)S(1)}, u32[]{:S(2)}, u32[]{:S(2)}) collective-permute-start(bf16[512,256]{1,0:T(8,128)(2,1)S(1)} %attend.3.refs_0_), channel_id=1, source_target_pairs={{0,2},{1,3},{2,0},{3,1},{4,6},{5,7},{6,4},{7,5},{8,10},{9,11},{10,... | collective-permute-start | bytes 786440 | tf_op jit(solution)/shard_map/ppermute | solution.py:25
  53.9 13.1 %collective-permute-start = (bf16[128,128]{1,0:T(8,128)(2,1)S(1)}, bf16[128,128]{1,0:T(8,128)(2,1)S(1)}, u32[]{:S(2)}, u32[]{:S(2)}) collective-permute-start(bf16[128,128]{1,0:T(8,128)(2,1)S(1)} %get-tuple-element.20), channel_id=1, source_target_pairs={{0,4},{4,8},{8,12},{12,16},{16,20},{20,24},{24,28},{1,5},{5,9},{9,... | collective-permute-start | bytes 98312 | tf_op jit(solution)/shard_map/ppermute | solution.py:21
  63.0 9.2 %collective-permute-start.34 = (bf16[64,2048]{1,0:T(8,128)(2,1)S(1)}, bf16[64,2048]{1,0:T(8,128)(2,1)S(1)}, u32[]{:S(2)}, u32[]{:S(2)}) collective-permute-start(bf16[64,2048]{1,0:T(8,128)(2,1)S(1)} %get-tuple-element.31), channel_id=1, source_target_pairs={{0,4},{4,0},{8,12},{12,8},{16,20},{20,16},{24,28},{28,24},{1,5},{5... | collective-permute-start | bytes 786440 | tf_op jit(solution)/shard_map/ppermute | solution.py:25
  63.1 10.8 %collective-permute-start.35 = (bf16[64,2048]{1,0:T(8,128)(2,1)S(1)}, bf16[64,2048]{1,0:T(8,128)(2,1)S(1)}, u32[]{:S(2)}, u32[]{:S(2)}) collective-permute-start(bf16[64,2048]{1,0:T(8,128)(2,1)S(1)} %get-tuple-element.32), channel_id=1, source_target_pairs={{0,2},{1,3},{2,0},{3,1},{4,6},{5,7},{6,4},{7,5},{8,10},{9,11},{10,... | collective-permute-start | bytes 786440 | tf_op jit(solution)/shard_map/ppermute | solution.py:25
  64.9 11.9 %collective-permute-start.18 = (bf16[64,2048]{1,0:T(8,128)(2,1)S(1)}, bf16[64,2048]{1,0:T(8,128)(2,1)S(1)}, u32[]{:S(2)}, u32[]{:S(2)}) collective-permute-start(bf16[64,2048]{1,0:T(8,128)(2,1)S(1)} %get-tuple-element.24), channel_id=1, source_target_pairs={{0,4},{4,0},{8,12},{12,8},{16,20},{20,16},{24,28},{28,24},{1,5},{5... | collective-permute-start | bytes 786440 | tf_op jit(solution)/shard_map/ppermute | solution.py:25
  67.0 11.0 %collective-permute-start.19 = (bf16[64,2048]{1,0:T(8,128)(2,1)S(1)}, bf16[64,2048]{1,0:T(8,128)(2,1)S(1)}, u32[]{:S(2)}, u32[]{:S(2)}) collective-permute-start(bf16[64,2048]{1,0:T(8,128)(2,1)S(1)} %get-tuple-element.25), channel_id=1, source_target_pairs={{0,2},{1,3},{2,0},{3,1},{4,6},{5,7},{6,4},{7,5},{8,10},{9,11},{10,... | collective-permute-start | bytes 786440 | tf_op jit(solution)/shard_map/ppermute | solution.py:25
  72.3 11.3 %collective-permute-start.2 = (bf16[512,256]{1,0:T(8,128)(2,1)S(1)}, bf16[512,256]{1,0:T(8,128)(2,1)S(1)}, u32[]{:S(2)}, u32[]{:S(2)}) collective-permute-start(bf16[512,256]{1,0:T(8,128)(2,1)S(1)} %attend.2.refs_0_), channel_id=1, source_target_pairs={{0,2},{1,3},{2,0},{3,1},{4,6},{5,7},{6,4},{7,5},{8,10},{9,11},{10,... | collective-permute-start | bytes 786440 | tf_op jit(solution)/shard_map/ppermute | solution.py:25
  74.0 12.4 %collective-permute-start.36 = (bf16[32,2048]{1,0:T(8,128)(2,1)S(1)}, bf16[32,2048]{1,0:T(8,128)(2,1)S(1)}, u32[]{:S(2)}, u32[]{:S(2)}) collective-permute-start(bf16[32,2048]{1,0:T(8,128)(2,1)S(1)} %get-tuple-element.33), channel_id=1, source_target_pairs={{0,2},{1,3},{2,0},{3,1},{4,6},{5,7},{6,4},{7,5},{8,10},{9,11},{10,... | collective-permute-start | bytes 393224 | tf_op jit(solution)/shard_map/ppermute | solution.py:25
  76.8 9.6 %collective-permute-start.37 = (bf16[32,2048]{1,0:T(8,128)(2,1)S(1)}, bf16[32,2048]{1,0:T(8,128)(2,1)S(1)}, u32[]{:S(2)}, u32[]{:S(2)}) collective-permute-start(bf16[32,2048]{1,0:T(8,128)(2,1)S(1)} %get-tuple-element.34), channel_id=1, source_target_pairs={{0,4},{4,0},{8,12},{12,8},{16,20},{20,16},{24,28},{28,24},{1,5},{5... | collective-permute-start | bytes 393224 | tf_op jit(solution)/shard_map/ppermute | solution.py:25
  78.1 10.0 %collective-permute-start.20 = (bf16[32,2048]{1,0:T(8,128)(2,1)S(1)}, bf16[32,2048]{1,0:T(8,128)(2,1)S(1)}, u32[]{:S(2)}, u32[]{:S(2)}) collective-permute-start(bf16[32,2048]{1,0:T(8,128)(2,1)S(1)} %get-tuple-element.26), channel_id=1, source_target_pairs={{0,2},{1,3},{2,0},{3,1},{4,6},{5,7},{6,4},{7,5},{8,10},{9,11},{10,... | collective-permute-start | bytes 393224 | tf_op jit(solution)/shard_map/ppermute | solution.py:25
  79.8 13.5 %collective-permute-start.4 = (bf16[512,256]{1,0:T(8,128)(2,1)S(1)}, bf16[512,256]{1,0:T(8,128)(2,1)S(1)}, u32[]{:S(2)}, u32[]{:S(2)}) collective-permute-start(bf16[512,256]{1,0:T(8,128)(2,1)S(1)} %attend.3.refs_0_), channel_id=1, source_target_pairs={{0,1},{1,0},{2,3},{3,2},{4,5},{5,4},{6,7},{7,6},{8,9},{9,8},{10,11... | collective-permute-start | bytes 786440 | tf_op jit(solution)/shard_map/ppermute | solution.py:25
  83.6 12.6 %collective-permute-start.6 = (bf16[512,256]{1,0:T(8,128)(2,1)S(1)}, bf16[512,256]{1,0:T(8,128)(2,1)S(1)}, u32[]{:S(2)}, u32[]{:S(2)}) collective-permute-start(bf16[512,256]{1,0:T(8,128)(2,1)S(1)} %collective-permute-done.5.refs_2_), channel_id=1, source_target_pairs={{0,1},{1,0},{2,3},{3,2},{4,5},{5,4},{6,7},{7,6},{8,9},{9,8},{10,11... | collective-permute-start | bytes 786440 | tf_op jit(solution)/shard_map/ppermute | solution.py:25
  86.4 13.4 %collective-permute-start.1 = (bf16[512,256]{1,0:T(8,128)(2,1)S(1)}, bf16[512,256]{1,0:T(8,128)(2,1)S(1)}, u32[]{:S(2)}, u32[]{:S(2)}) collective-permute-start(bf16[512,256]{1,0:T(8,128)(2,1)S(1)} %attend.2.refs_0_), channel_id=1, source_target_pairs={{0,1},{1,0},{2,3},{3,2},{4,5},{5,4},{6,7},{7,6},{8,9},{9,8},{10,11... | collective-permute-start | bytes 786440 | tf_op jit(solution)/shard_map/ppermute | solution.py:25
  86.4 13.4 %collective-permute-start.3 = (bf16[512,256]{1,0:T(8,128)(2,1)S(1)}, bf16[512,256]{1,0:T(8,128)(2,1)S(1)}, u32[]{:S(2)}, u32[]{:S(2)}) collective-permute-start(bf16[512,256]{1,0:T(8,128)(2,1)S(1)} %collective-permute-done.2.refs_2_), channel_id=1, source_target_pairs={{0,1},{1,0},{2,3},{3,2},{4,5},{5,4},{6,7},{7,6},{8,9},{9,8},{10,11... | collective-permute-start | bytes 786440 | tf_op jit(solution)/shard_map/ppermute | solution.py:25
  93.3 11.7 %collective-permute-start.39 = (bf16[32,2048]{1,0:T(8,128)(2,1)S(1)}, bf16[32,2048]{1,0:T(8,128)(2,1)S(1)}, u32[]{:S(2)}, u32[]{:S(2)}) collective-permute-start(bf16[32,2048]{1,0:T(8,128)(2,1)S(1)} %get-tuple-element.36), channel_id=1, source_target_pairs={{0,16},{4,20},{8,24},{12,28},{16,0},{20,4},{24,8},{28,12},{1,17},{... | collective-permute-start | bytes 393224 | tf_op jit(solution)/shard_map/ppermute | solution.py:25
  (26 other events, 226.7 us)
